TPU v7x, 32 devices: a whole 2x2x4 slice. The times are simulated.
32 devices in a mesh: sp: 8 (over z, x), tp: 4 (over y, core).
Axes of the slice: x: 2, y: 2, z: 4, core: 2. Of those that a mesh axis runs over, the one named last changes fastest.
Arguments:
- latent: bfloat16 [4096, 2048], P(('sp', 'tp')), may hold values from -6 to 6
- context: bfloat16 [512, 2048], P('sp'), may hold values from -6 to 6
- conditioning: float32 [2048], P('sp'), may hold values from -6 to 6
- context_conditioning: float32 [2048], P('sp'), may hold values from -6 to 6
- shift_weight: bfloat16 [2048, 2048], P('sp', 'tp'), may hold values from -0.25 to 0.25
- scale_weight: bfloat16 [2048, 2048], P('sp', 'tp'), may hold values from -0.25 to 0.25
- gate_weight: bfloat16 [2048, 2048], P('sp', 'tp'), may hold values from -0.25 to 0.25
- norm_gain: float32 [2048], replicated, may hold values from 0.1 to 1.9
- query_weight: bfloat16 [2048, 2048], P(None, 'tp'), may hold values from -0.125 to 0.125
- key_weight: bfloat16 [2048, 1024], P(None, 'tp'), may hold values from -0.125 to 0.125
- value_weight: bfloat16 [2048, 1024], P(None, 'tp'), may hold values from -0.125 to 0.125
- query_gain: float32 [64], replicated, may hold values from 2 to 64, as said below
- key_gain: float32 [64], replicated, may hold values from 0.1 to 1.9
- context_lift: float32 [32], P('tp'), may hold values from 1.5 to 3
- output_weight: bfloat16 [2048, 2048], P('tp'), may hold values from -0.125 to 0.125
Outputs:
- mixed: bfloat16 [4096, 2048], P(('sp', 'tp'))
Inputs may be any that keep to these rules, and one draw needn't show every extreme that they name: `query_gain`: one gain for each channel of a head.
All inputs are finite; a program needn't handle non-finite values.
Results may differ from a plain program's by a relative error of at most 0.018.
The roundings to bfloat16 on the way count: a program that leaves them out, or rounds other values in their place, can miss the bound.
Values may be sent and summed in bfloat16 or wider, within the bound.
No kernel may reach another device: no remote copies, remote signals or barrier semaphores. Data moves between devices by JAX's collectives and lax.ppermute only.
A program may use at most 128 MiB of HBM per device.

v0:
```python
import functools

import jax
import jax.numpy as jnp
from jax import lax
from jax.experimental import pallas as pl
from jax.experimental.pallas import tpu as pltpu
from jax.sharding import PartitionSpec as P


HEAD = 64
GRID = 64
TILE = 128
EPSILON = 1e-06
ROTARY_BASE = 10000.0
F32 = jnp.float32
BF16 = jnp.bfloat16


VMEM_LIMIT = 20 << 20
IN_VMEM = pl.BlockSpec(memory_space=pltpu.VMEM)

NT = (((1,), (1,)), ((), ()))


def dot(a, b):
    return jnp.dot(a, b, preferred_element_type=F32)


def cost(flops, nbytes):
    return pl.CostEstimate(flops=int(flops), bytes_accessed=int(nbytes), transcendentals=0)


def swap(value, axis, size, mask):
    return lax.ppermute(value, axis, [(i, i ^ mask) for i in range(size)])


def modulation_kernel(cond, ccond, shift, scale, gate, out):
    def signal(ref):
        v = ref[...]
        return (v / (1.0 + jnp.exp(-v))).astype(BF16)

    both = jnp.concatenate([signal(cond), signal(ccond)], axis=0)
    both = jnp.concatenate([both, jnp.zeros((6,) + both.shape[1:], F32).astype(BF16)], axis=0)
    s = dot(both, shift[...])
    c = dot(both, scale[...])
    g = dot(both, gate[...])
    out[0:1, :] = s[0:1]
    out[1:2, :] = c[0:1]
    out[2:3, :] = g[0:1]
    out[3:4, :] = s[1:2]
    out[4:5, :] = c[1:2]
    out[5:8, :] = jnp.zeros((3, out.shape[1]), F32)


def modulation_partial(cond, ccond, shift, scale, gate):
    width = shift.shape[1]
    depth = cond.shape[0]
    return pl.pallas_call(
        modulation_kernel,
        out_shape=jax.ShapeDtypeStruct((8, width), F32),
        cost_estimate=cost(6 * 8 * depth * width, 6 * depth * width),
        name="modulation",
    )(cond.reshape(1, depth), ccond.reshape(1, depth), shift, scale, gate)


def head_scale(x):
    width = x.shape[1]
    square = x * x
    high = square.astype(BF16)
    low = (square - high.astype(F32)).astype(BF16)
    rows = lax.broadcasted_iota(jnp.int32, (width, width), 0) // HEAD
    cols = lax.broadcasted_iota(jnp.int32, (width, width), 1) // HEAD
    ones = jnp.where(rows == cols, 1.0, 0.0).astype(BF16)
    mean = (dot(high, ones) + dot(low, ones)) * (1.0 / HEAD)
    return lax.rsqrt(mean + EPSILON)


def turn(x, tables):
    width = x.shape[1]
    left = pltpu.roll(x, width - 1, 1)
    right = pltpu.roll(x, 1, 1)
    return x * tables[0] + left * tables[1] + right * tables[2]


def pieces_of(x, width):
    return [x[:, i : i + width] for i in range(0, x.shape[1], width)]


def finish_heads(x, gain, tables):
    out = []
    step = TILE if x.shape[1] % TILE == 0 else HEAD
    tables = [t[:, :step] for t in tables]
    gain = jnp.concatenate([gain] * (step // HEAD), axis=1)
    for part in pieces_of(x, step):
        out.append(turn(part * head_scale(part) * gain, tables))
    return [h for part in out for h in pieces_of(part, HEAD)]


def modulate(x, gain, shift, dest, row):
    rows = x.shape[0]
    x = x.astype(F32)
    inverse = lax.rsqrt(jnp.mean(x * x, axis=1, keepdims=True) + EPSILON)
    dest[row : row + rows, :] = (x * inverse * gain + shift).astype(BF16)


def kv_kernel(count, *refs):
    pieces = refs[:count]
    context, mod, gains, weight, cos, sin_e, sin_o = refs[count : count + 7]
    hidden, packed = refs[count + 7 :]
    norm_gain = gains[:, : context.shape[1]]
    key_gain = gains[:, context.shape[1] : context.shape[1] + HEAD]
    parts = mod.shape[0] // 8

    def vector(index):
        return jnp.concatenate([mod[8 * t + index : 8 * t + index + 1, :] for t in range(parts)], axis=1)

    gain = norm_gain * (1.0 + vector(1))
    shift = vector(0)
    row = 0
    for piece in pieces:
        modulate(piece[...], gain, shift, hidden, row)
        row += piece.shape[0]
    modulate(context[...], norm_gain * (1.0 + vector(4)), vector(3), hidden, row)
    h = hidden[...]
    width = weight.shape[1] // 2
    keys = dot(h, weight[:, :width])
    values = dot(h, weight[:, width:])
    tables = (cos[...], sin_e[...], sin_o[...])
    heads = finish_heads(keys, key_gain, tables)
    for k, key in enumerate(heads):
        packed[:, k * TILE : (k + 1) * TILE] = jnp.concatenate(
            [key, values[:, k * HEAD : (k + 1) * HEAD]], axis=1
        ).astype(BF16)


def keys_values(pieces, context, mod, gains, weight, tables):
    rows = sum(p.shape[0] for p in pieces) + context.shape[0]
    depth = context.shape[1]
    width = weight.shape[1] // 2
    return pl.pallas_call(
        functools.partial(kv_kernel, len(pieces)),
        out_shape=(
            jax.ShapeDtypeStruct((rows, depth), BF16),
            jax.ShapeDtypeStruct((rows, 2 * width), BF16),
        ),
        in_specs=[IN_VMEM] * (len(pieces) + 7),
        out_specs=(IN_VMEM, IN_VMEM),
        compiler_params=pltpu.CompilerParams(vmem_limit_bytes=VMEM_LIMIT),
        cost_estimate=cost(4 * rows * depth * width, 4 * rows * depth + 4 * depth * width),
        name="keys_values",
    )(*pieces, context, mod, gains, weight, *tables)


def query_kernel(hidden, weight, gains, cos, sin_e, sin_o, out):
    rows = out.shape[1]
    tables = (cos[0:rows, :], sin_e[0:rows, :], sin_o[0:rows, :])
    width = weight.shape[1]
    gain = gains[:, hidden.shape[1] + HEAD :]
    step = min(width, 2 * TILE)
    for start in range(0, width, step):
        x = dot(hidden[0:rows, :], weight[:, start : start + step])
        for i, head in enumerate(finish_heads(x, gain, tables)):
            head = (head * (HEAD**-0.5)).astype(BF16)
            out[start // HEAD + i] = jnp.concatenate([head, jnp.zeros_like(head)], axis=1)


def queries_of(hidden, weight, gains, tables, rows):
    depth, width = weight.shape
    return pl.pallas_call(
        query_kernel,
        in_specs=[IN_VMEM] * 6,
        out_specs=IN_VMEM,
        out_shape=jax.ShapeDtypeStruct((width // HEAD, rows, TILE), BF16),
        compiler_params=pltpu.CompilerParams(vmem_limit_bytes=VMEM_LIMIT),
        cost_estimate=cost(2 * rows * depth * width, 2 * rows * depth + 2 * depth * width),
        name="queries",
    )(hidden, weight, gains, *tables)


STATE = HEAD + 16


def attention_kernel(spans, lifted, has_state, final, group, chunk, *refs):
    refs = list(refs)
    q_ref = refs.pop(0)
    blocks = [refs.pop(0) for _ in spans]
    lift = refs.pop(0) if lifted else None
    state = refs.pop(0) if has_state else None
    value_rows, held = refs[-3], refs[-2:]
    outs = refs[:-3]
    rows = q_ref.shape[1]
    kv_heads = q_ref.shape[0] // group
    sizes = [end - first for first, _, end in spans]
    starts = [sum(sizes[:i]) for i in range(len(sizes))]
    plain = [(st, middle - first) for st, (first, middle, _) in zip(starts, spans) if middle > first]
    raised = [
        (st + middle - first, end - middle)
        for st, (first, middle, end) in zip(starts, spans)
        if end > middle
    ]

    def tile(ref, span, k):
        return ref[span[0] : span[2], pl.ds(pl.multiple_of(k * TILE, TILE), TILE)]

    for k in range(kv_heads):
        for ref, span, start, size in zip(blocks, spans, starts, sizes):
            value_rows[k, 0:HEAD, start : start + size] = tile(ref, span, k).T[HEAD:]
            value_rows[k, HEAD:, start : start + size] = jnp.ones((16, size), BF16)

    work = [(g, r) for r in range(0, rows, chunk) for g in range(group)]

    def scores(k, item, slot):
        g, r = item
        q = q_ref[k * group + g, r : r + chunk, :]
        for ref, span, start, size in zip(blocks, spans, starts, sizes):
            held[slot][start : start + size, :] = lax.dot_general(
                tile(ref, span, k), q, NT, preferred_element_type=F32
            )

    def absorb(k, item, slot):
        g, r = item
        h = k * group + g
        parts = [(st, held[slot][st : st + n, :]) for st, n in plain]
        parts += [(st, held[slot][st : st + n, :] + lift[h]) for st, n in raised]
        top = functools.reduce(
            jnp.maximum, [jnp.max(x, axis=0, keepdims=True) for _, x in parts]
        )
        if has_state:
            before = state[h, HEAD + 8 : HEAD + 9, r : r + chunk]
            top = jnp.maximum(top, before)
        parts.sort(key=lambda part: part[0])
        weights = jnp.concatenate([jnp.exp(x - top).astype(BF16) for _, x in parts], axis=0)
        total = dot(value_rows[k], weights)
        if has_state:
            total = total + state[h, :, r : r + chunk] * jnp.exp(before - top)
        if not final:
            outs[0][h, 0 : HEAD + 8, r : r + chunk] = total[: HEAD + 8]
            outs[0][h, HEAD + 8 :, r : r + chunk] = jnp.broadcast_to(top, (8, chunk))
            return None
        return total[:HEAD] / total[HEAD : HEAD + 1]

    scores(0, work[0], 0)

    @pl.loop(0, kv_heads)
    def _(k):
        done = {}
        for i, item in enumerate(work):
            if i + 1 < len(work):
                scores(k, work[i + 1], (i + 1) % 2)
            else:
                scores(jnp.minimum(k + 1, kv_heads - 1), work[0], (i + 1) % 2)
            g, r = item
            done[g] = absorb(k, item, i % 2)
            if final and g == group - 1:
                whole = jnp.concatenate([done[j] for j in range(group)], axis=0).T.astype(BF16)
                size = outs[0].shape[0]
                width = group * HEAD
                lanes = pl.ds(pl.multiple_of(k * width, width), width)
                for j in range(0, chunk, size):
                    outs[(r + j) // size][:, lanes] = whole[j : j + size]


def attention(queries, blocks, lift, state, group, pieces):
    heads, rows, _ = queries.shape
    kv_heads = heads // group
    chunk = min(rows, 256)
    final = pieces > 0
    spans = [b[1:] for b in blocks]
    keys = sum(end - first for first, _, end in spans)
    lifted = any(end > middle for _, middle, end in spans)
    args = [queries] + [b[0] for b in blocks]
    in_specs = [IN_VMEM] * len(args)
    if lifted:
        in_specs.append(pl.BlockSpec(memory_space=pltpu.SMEM))
        args.append(lift)
    if state is not None:
        in_specs.append(IN_VMEM)
        args.append(state)
    if final:
        out_shape = [jax.ShapeDtypeStruct((rows // pieces, heads * HEAD), BF16)] * pieces
    else:
        out_shape = [jax.ShapeDtypeStruct((heads, STATE, rows), F32)]
    out = pl.pallas_call(
        functools.partial(
            attention_kernel, spans, lifted, state is not None, final, group, chunk
        ),
        in_specs=in_specs,
        out_specs=[IN_VMEM] * len(out_shape),
        out_shape=out_shape,
        scratch_shapes=[
            pltpu.VMEM((kv_heads, STATE, keys), BF16),
            pltpu.VMEM((keys, chunk), F32),
            pltpu.VMEM((keys, chunk), F32),
        ],
        compiler_params=pltpu.CompilerParams(vmem_limit_bytes=VMEM_LIMIT),
        cost_estimate=cost(16 * heads * rows * keys * HEAD, 4 * heads * rows * TILE),
        name="attention",
    )(*args)
    return list(out) if final else out[0]


def output_kernel(count, *refs):
    attended = refs[:count]
    weights = refs[count : 2 * count]
    latent, mod, out = refs[2 * count :]
    step = mod.shape[1]
    for i in range(out.shape[1] // step):
        total = None
        for a, w in zip(attended, weights):
            term = dot(a[...], w[:, i * step : (i + 1) * step])
            total = term if total is None else total + term
        gate = mod[8 * i + 2 : 8 * i + 3, :]
        old = latent[:, i * step : (i + 1) * step].astype(F32)
        out[:, i * step : (i + 1) * step] = (old + gate * total).astype(BF16)


def project(attended, weights, latent, mod):
    count = len(attended)
    rows, depth = latent.shape
    inner = attended[0].shape[1]
    return pl.pallas_call(
        functools.partial(output_kernel, count),
        in_specs=[IN_VMEM] * (2 * count + 2),
        out_specs=IN_VMEM,
        out_shape=jax.ShapeDtypeStruct((rows, depth), BF16),
        compiler_params=pltpu.CompilerParams(vmem_limit_bytes=VMEM_LIMIT),
        cost_estimate=cost(2 * rows * depth * inner * count, 2 * depth * inner * count),
        name="output",
    )(*attended, *weights, latent, mod)


def rotary_tables(rank, tp, rows, context_rows):
    index = lax.broadcasted_iota(jnp.int32, (tp * rows + context_rows, TILE), 0)
    lane = lax.broadcasted_iota(jnp.int32, (tp * rows + context_rows, TILE), 1)
    piece = index // rows
    position = (rank // tp * tp + jnp.bitwise_xor(rank % tp, piece)) * rows + index % rows
    quarter = HEAD // 4
    pair = lane % HEAD // 2
    frequency = ROTARY_BASE ** (-(pair % quarter).astype(F32) / quarter)
    place = jnp.where(pair < quarter, position // GRID, position % GRID).astype(F32)
    angle = jnp.where(index < tp * rows, place, 0.0) * frequency
    sine = jnp.sin(angle)
    even = lane % 2 == 0
    return jnp.cos(angle), jnp.where(even, -sine, 0.0), jnp.where(even, 0.0, sine)


def shards(
    sp,
    tp,
    latent,
    context,
    conditioning,
    context_conditioning,
    shift_weight,
    scale_weight,
    gate_weight,
    norm_gain,
    query_weight,
    key_weight,
    value_weight,
    query_gain,
    key_gain,
    context_lift,
    output_weight,
):
    rows = latent.shape[0]
    length = rows * tp
    context_rows = context.shape[0]
    group = query_weight.shape[1] // key_weight.shape[1]
    tp_bits = [1 << b for b in reversed(range(tp.bit_length() - 1))]

    def spread(have, bit):
        have.update({j | bit: swap(v, "tp", tp, bit) for j, v in list(have.items())})

    def tie(*values):
        return lax.optimization_barrier(values)

    pieces = {0: latent}
    spread(pieces, tp_bits[0])
    partial = modulation_partial(
        conditioning, context_conditioning, shift_weight, scale_weight, gate_weight
    )
    rank = lax.axis_index("sp") * tp + lax.axis_index("tp")
    gains = [v.reshape(1, -1) for v in (norm_gain, key_gain, query_gain)]
    early = [
        (*rotary_tables(rank, tp, rows, context_rows), jnp.concatenate(gains, axis=1)),
        (jnp.concatenate([key_weight, value_weight], axis=1),),
    ]
    ready = []
    bits = [1 << b for b in range(sp.bit_length() - 1)]
    for i in range(0, len(bits), 2):
        pair = bits[i : i + 2]
        masks = pair + [sum(pair)] if len(pair) == 2 else pair
        arrived = [swap(partial, "sp", sp, m) for m in masks]
        extra = early.pop(0) if early else ()
        tied = tie(*arrived, *extra)
        partial = sum(tied[: len(arrived)], partial)
        ready += tied[len(arrived) :]
    for extra in early:
        ready += extra
    *tables, gains, kv_weight = ready
    partial, pieces[tp_bits[0]] = tie(partial, pieces[tp_bits[0]])
    for bit in tp_bits[1:]:
        spread(pieces, bit)
    mod = lax.all_gather(partial, "tp", axis=0, tiled=True)

    hidden, packed = keys_values(
        [pieces[j] for j in range(tp)], context, mod, gains, kv_weight, tables
    )

    order = list(range(0, sp, 2)) + list(range(sp - 1, 0, -2))
    ahead = [(order[i], order[(i + 1) % sp]) for i in range(sp)]
    back = [(b, a) for a, b in ahead]
    across = [(order[i], order[(i + sp // 2) % sp]) for i in range(sp)]
    up, down = packed, packed
    waiting = [(packed, 0, length, length + context_rows)]
    state = None
    for step in range(1, sp // 2):
        up = lax.ppermute(up, "sp", ahead)
        down = lax.ppermute(down, "sp", back)
        if step == 1:
            queries = queries_of(hidden, query_weight, gains, tables, length)
            far_context = lax.ppermute(packed[length:], "sp", across)
            output_weight, _ = tie(output_weight, packed)
            weights = {0: output_weight}
            spread(weights, tp_bits[0])
        state = attention(queries, waiting, context_lift, state, group, 0)
        if step == 1:
            up, down, state, far_context = tie(up, down, state, far_context)
        else:
            up, down, state = tie(up, down, state)
        waiting = [(b, 0, length, length + context_rows) for b in (up, down)]
        if step == 2:
            waiting.append((far_context, 0, 0, context_rows))
    half = length // 2
    up = lax.ppermute(up[:half], "sp", ahead)
    down = lax.ppermute(down[half:length], "sp", back)
    state = attention(queries, waiting, context_lift, state, group, 0)
    first = tp_bits[0]
    up, down, state, weights[first] = tie(up, down, state, weights[first])
    for bit in tp_bits[1:]:
        spread(weights, bit)
    attended = attention(
        queries, [(up, 0, half, half), (down, 0, half, half)], context_lift, state, group, tp
    )
    for bit in tp_bits:
        attended = [swap(a, "tp", tp, bit) if j & bit else a for j, a in enumerate(attended)]
    return project(attended, [weights[j] for j in range(tp)], latent, mod)


def solution(mesh):
    in_specs = (
        P(("sp", "tp"), None),
        P("sp", None),
        P("sp"),
        P("sp"),
        P("sp", "tp"),
        P("sp", "tp"),
        P("sp", "tp"),
        P(),
        P(None, "tp"),
        P(None, "tp"),
        P(None, "tp"),
        P(),
        P(),
        P("tp"),
        P("tp", None),
    )
    return jax.shard_map(
        functools.partial(shards, mesh.shape["sp"], mesh.shape["tp"]),
        mesh=mesh,
        in_specs=in_specs,
        out_specs=P(("sp", "tp"), None),
        check_vma=False,
    )
```

profile of v0, /device:TPU:0, one launch (start us, length us, event | category | flops | bytes accessed | tf_op | source)
XLA Modules:
  0.0 103.3 jit_solution(15690546510296039250)
XLA Ops:
  0.0 2.1 %modulation.1 = f32[8,512]{1,0:T(8,128)} custom-call(f32[1,256]{1,0:T(1,128)} %bitcast.6, f32[1,256]{1,0:T(1,128)} %bitcast.7, bf16[256,512]{1,0:T(8,128)(2,1)} %shift.1, bf16[256,512]{1,0:T(8,128)(2,1)} %scale.1, bf16[256,512]{1,0:T(8,128)(2,1)} %gate.1), custom_call_target="tpu_custom_call" | custom-call | flops 6291456 | bytes 786432 | tf_op jit(solution)/shard_map/modulation/pallas_call | solution.py:59
  2.1 3.0 %collective-permute-start.1 = (f32[8,512]{1,0:T(8,128)}, f32[8,512]{1,0:T(8,128)S(1)}, u32[]{:S(2)}, u32[]{:S(2)}) collective-permute-start(f32[8,512]{1,0:T(8,128)} %modulation.1), channel_id=1, source_target_pairs={{0,4},{4,0},{8,12},{12,8},{16,20},{20,16},{24,28},{28,24},{1,5},{5... | collective-permute-start | bytes 49160 | tf_op jit(solution)/shard_map/ppermute | solution.py:35
  5.0 1.6 %collective-permute-start.2 = (f32[8,512]{1,0:T(8,128)}, f32[8,512]{1,0:T(8,128)S(1)}, u32[]{:S(2)}, u32[]{:S(2)}) collective-permute-start(f32[8,512]{1,0:T(8,128)} %modulation.1), channel_id=1, source_target_pairs={{0,8},{4,12},{8,0},{12,4},{16,24},{20,28},{24,16},{28,20},{1,9},{5... | collective-permute-start | bytes 49160 | tf_op jit(solution)/shard_map/ppermute | solution.py:35
  6.6 0.0 collective-permute-start.3
  6.6 0.0 collective-permute-start
  6.6 1.9 %collective-permute-start.5 = (bf16[128,2048]{1,0:T(8,128)(2,1)}, bf16[128,2048]{1,0:T(8,128)(2,1)S(1)}, u32[]{:S(2)}, u32[]{:S(2)}) collective-permute-start(bf16[128,2048]{1,0:T(8,128)(2,1)} %refs_8_.1), channel_id=1, source_target_pairs={{0,2},{1,3},{2,0},{3,1},{4,6},{5,7},{6,4},{7,5},{8,10},{9,11},{10,... | collective-permute-start | bytes 1572872 | tf_op jit(solution)/shard_map/ppermute | solution.py:35
  8.6 1.6 %fusion.13 = (f32[576,128]{1,0:T(8,128)S(1)}, f32[576,128]{1,0:T(8,128)S(1)}, f32[576,128]{1,0:T(8,128)S(1)}) fusion(s32[128]{0:T(128)S(1)} %get-tuple-element.80, s32[128]{0:T(128)S(1)} %get-tuple-element.82, pred[128]{0:T(512)(128)(4,1)S(1)} %get-tuple-element.78, s32[576]{0:T(1024)S(1)} %get-tuple-element.73, s32[576]{0:T(1024)S(1)} %get-tuple-element.74, ...), kind=kLoop, calls=%fused_computation.31 | loop fusion | flops 4792320 | bytes 897992 | tf_op jit(solution)/shard_map/jit(_where)/select_n | solution.py:345
  10.3 0.8 concatenate.6.refs_6_.gains
  11.1 0.0 collective-permute-done.1
  11.1 0.0 collective-permute-done.2
  11.1 0.4 collective-permute-done.3
  11.4 0.7 add_add_fusion
  12.2 2.7 %collective-permute-start.4 = (f32[8,512]{1,0:T(8,128)S(1)}, f32[8,512]{1,0:T(8,128)S(1)}, u32[]{:S(2)}, u32[]{:S(2)}) collective-permute-start(f32[8,512]{1,0:T(8,128)S(1)} %add_add_fusion), channel_id=1, source_target_pairs={{0,16},{4,20},{8,24},{12,28},{16,0},{20,4},{24,8},{28,12},{1,17},{... | collective-permute-start | bytes 49160 | tf_op jit(solution)/shard_map/ppermute | solution.py:35
  14.8 0.0 copy-done.5
  14.8 1.4 %pad_maximum_fusion.refs_7_ = bf16[2048,512]{1,0:T(8,128)(2,1)S(1)} fusion(bf16[2048,256]{1,0:T(8,128)(2,1)S(1)} %copy-done.5, bf16[2048,256]{1,0:T(8,128)(2,1)} %param.24), kind=kLoop, calls=%fused_computation | loop fusion | flops 4194304 | bytes 4194304 | tf_op jit(solution)/shard_map/concatenate | solution.py:388
  16.2 0.7 collective-permute-done.4
  17.0 4.4 %collective-permute-done.5.refs_2_ = bf16[128,2048]{1,0:T(8,128)(2,1)S(1)} collective-permute-done((bf16[128,2048]{1,0:T(8,128)(2,1)}, bf16[128,2048]{1,0:T(8,128)(2,1)S(1)}, u32[]{:S(2)}, u32[]{:S(2)}) %collective-permute-start.5) | collective-permute-done | bytes 524320 | tf_op jit(solution)/shard_map/ppermute | solution.py:35
  21.3 0.0 collective-permute-start.6
  21.4 5.4 %all_gather.3.refs_5_.refs_9_ = f32[32,512]{1,0:T(8,128)S(1)} all-gather(f32[8,512]{1,0:T(8,128)S(1)} %add.75), channel_id=1, replica_groups=mesh['sp'=8,'tp'=4] {'tp'}, dimensions={0}, use_global_device_ids=true | all-gather | bytes 81920 | tf_op jit(solution)/shard_map/all_gather | solution.py:406
  26.8 0.0 collective-permute-done.refs_1_
  26.8 0.0 collective-permute-done.6.refs_3_
  26.8 0.0 copy-done.2
  26.8 0.0 copy-done.3
  26.8 2.5 %keys_values.1 = (bf16[576,2048]{1,0:T(8,128)(2,1)S(1)}, bf16[576,512]{1,0:T(8,128)(2,1)S(1)}) custom-call(bf16[128,2048]{1,0:T(8,128)(2,1)S(1)} %copy-done.2, bf16[128,2048]{1,0:T(8,128)(2,1)S(1)} %collective-permute-done.refs_1_, bf16[128,2048]{1,0:T(8,128)(2,1)S(1)} %collective-permute-done.5.refs_2_, ...), custom_call_target="tpu_custom_call" | custom-call | flops 1207959552 | bytes 6815744 | tf_op jit(solution)/shard_map/keys_values/pallas_call | solution.py:141
  29.4 1.6 %collective-permute-start.7 = (bf16[576,512]{1,0:T(8,128)(2,1)S(1)}, bf16[576,512]{1,0:T(8,128)(2,1)S(1)}, u32[]{:S(2)}, u32[]{:S(2)}) collective-permute-start(bf16[576,512]{1,0:T(8,128)(2,1)S(1)} %get-tuple-element.49.refs_1_), channel_id=1, source_target_pairs={{0,8},{8,16},{16,24},{24,28},{28,20},{20,12},{12,4},{4,0},{1,9},{9... | collective-permute-start | bytes 1769480 | tf_op jit(solution)/shard_map/ppermute | solution.py:420
  31.0 0.4 collective-permute-start.8
  31.4 0.0 copy-done
  31.4 1.5 %collective-permute-start.16 = (bf16[512,2048]{1,0:T(8,128)(2,1)S(1)}, bf16[512,2048]{1,0:T(8,128)(2,1)S(1)}, u32[]{:S(2)}, u32[]{:S(2)}) collective-permute-start(bf16[512,2048]{1,0:T(8,128)(2,1)S(1)} %copy-done), channel_id=1, source_target_pairs={{0,2},{1,3},{2,0},{3,1},{4,6},{5,7},{6,4},{7,5},{8,10},{9,11},{10,... | collective-permute-start | bytes 6291464 | tf_op jit(solution)/shard_map/ppermute | solution.py:35
  33.0 4.5 %collective-permute-start.9 = (bf16[64,512]{1,0:T(8,128)(2,1)S(1)}, bf16[64,512]{1,0:T(8,128)(2,1)S(1)}, u32[]{:S(2)}, u32[]{:S(2)}) collective-permute-start(bf16[64,512]{1,0:T(8,128)(2,1)S(1)} %slice.9), channel_id=1, source_target_pairs={{0,28},{8,20},{16,12},{24,4},{28,0},{20,8},{12,16},{4,24},{1,29},{... | collective-permute-start | bytes 196616 | tf_op jit(solution)/shard_map/ppermute | solution.py:424
  37.5 3.3 %queries.1.refs_0_ = bf16[8,512,128]{2,1,0:T(8,128)(2,1)S(1)} custom-call(bf16[576,2048]{1,0:T(8,128)(2,1)S(1)} %get-tuple-element.48.hidden, bf16[2048,512]{1,0:T(8,128)(2,1)S(1)} %copy-done.1, f32[1,2176]{1,0:T(1,128)S(1)} %concatenate.6.refs_6_.gains, f32[576,128]{1,0:T(8,128)S(1)} %get-tuple-element.45.refs_8_.cos, ...), custom_call_target="tpu_custom_call" | custom-call | flops 1073741824 | bytes 4194304 | tf_op jit(solution)/shard_map/queries/pallas_call | solution.py:170
  40.8 5.2 %attention.5.refs_4_ = f32[8,80,512]{2,1,0:T(8,128)S(1)} custom-call(bf16[8,512,128]{2,1,0:T(8,128)(2,1)S(1)} %queries.1.refs_0_, bf16[576,512]{1,0:T(8,128)(2,1)S(1)} %get-tuple-element.49.refs_1_, f32[8]{0:T(128)S(1)} %copy-done.4), custom_call_target="tpu_custom_call" | custom-call | flops 2415919104 | bytes 2097152 | tf_op jit(solution)/shard_map/attention/pallas_call | solution.py:284
  46.0 3.5 %collective-permute-done.9.refs_3_ = bf16[64,512]{1,0:T(8,128)(2,1)S(1)} collective-permute-done((bf16[64,512]{1,0:T(8,128)(2,1)S(1)}, bf16[64,512]{1,0:T(8,128)(2,1)S(1)}, u32[]{:S(2)}, u32[]{:S(2)}) %collective-permute-start.9) | collective-permute-done | bytes 65568 | tf_op jit(solution)/shard_map/ppermute | solution.py:424
  49.5 0.0 collective-permute-done.7.refs_1_
  49.5 0.0 collective-permute-done.8.refs_2_
  49.5 0.9 collective-permute-start.10
  50.3 1.2 %collective-permute-start.11 = (bf16[576,512]{1,0:T(8,128)(2,1)S(1)}, bf16[576,512]{1,0:T(8,128)(2,1)S(1)}, u32[]{:S(2)}, u32[]{:S(2)}) collective-permute-start(bf16[576,512]{1,0:T(8,128)(2,1)S(1)} %collective-permute-done.8.refs_2_), channel_id=1, source_target_pairs={{8,0},{16,8},{24,16},{28,24},{20,28},{12,20},{4,12},{0,4},{9,1},{1... | collective-permute-start | bytes 1769480 | tf_op jit(solution)/shard_map/ppermute | solution.py:421
  51.5 7.1 %attention.6.refs_5_ = f32[8,80,512]{2,1,0:T(8,128)S(1)} custom-call(bf16[8,512,128]{2,1,0:T(8,128)(2,1)S(1)} %queries.1.refs_0_, bf16[576,512]{1,0:T(8,128)(2,1)S(1)} %collective-permute-done.7.refs_1_, bf16[576,512]{1,0:T(8,128)(2,1)S(1)} %collective-permute-done.8.refs_2_, f32[8]{0:T(128)S(1)} %copy-done.4, f32[8,80,512]{2,1,0:T(8,128)S(1)} %attention.5.refs_4_), custom_call_target="tpu_custom_call" | custom-call | flops 4831838208 | bytes 2097152 | tf_op jit(solution)/shard_map/attention/pallas_call | solution.py:284
  58.6 5.5 %collective-permute-done.10.refs_1_ = bf16[576,512]{1,0:T(8,128)(2,1)S(1)} collective-permute-done((bf16[576,512]{1,0:T(8,128)(2,1)S(1)}, bf16[576,512]{1,0:T(8,128)(2,1)S(1)}, u32[]{:S(2)}, u32[]{:S(2)}) %collective-permute-start.10) | collective-permute-done | bytes 589856 | tf_op jit(solution)/shard_map/ppermute | solution.py:420
  64.1 0.1 collective-permute-done.11.refs_2_
  64.2 1.7 %collective-permute-start.12 = (bf16[576,512]{1,0:T(8,128)(2,1)S(1)}, bf16[576,512]{1,0:T(8,128)(2,1)S(1)}, u32[]{:S(2)}, u32[]{:S(2)}) collective-permute-start(bf16[576,512]{1,0:T(8,128)(2,1)S(1)} %collective-permute-done.10.refs_1_), channel_id=1, source_target_pairs={{0,8},{8,16},{16,24},{24,28},{28,20},{20,12},{12,4},{4,0},{1,9},{9... | collective-permute-start | bytes 1769480 | tf_op jit(solution)/shard_map/ppermute | solution.py:420
  66.0 0.3 collective-permute-start.13
  66.2 0.0 collective-permute-start.21
  66.2 7.3 %attention.7.refs_4_ = f32[8,80,512]{2,1,0:T(8,128)S(1)} custom-call(bf16[8,512,128]{2,1,0:T(8,128)(2,1)S(1)} %queries.1.refs_0_, bf16[576,512]{1,0:T(8,128)(2,1)S(1)} %collective-permute-done.10.refs_1_, bf16[576,512]{1,0:T(8,128)(2,1)S(1)} %collective-permute-done.11.refs_2_, bf16[64,512]{1,0:T(8,128)(2,1)S(1)} %collective-permute-done.9.refs_3_, ...), custom_call_target="tpu_custom_call" | custom-call | flops 5100273664 | bytes 2097152 | tf_op jit(solution)/shard_map/attention/pallas_call | solution.py:284
  73.5 4.4 %collective-permute-done.12.refs_1_ = bf16[576,512]{1,0:T(8,128)(2,1)S(1)} collective-permute-done((bf16[576,512]{1,0:T(8,128)(2,1)S(1)}, bf16[576,512]{1,0:T(8,128)(2,1)S(1)}, u32[]{:S(2)}, u32[]{:S(2)}) %collective-permute-start.12) | collective-permute-done | bytes 589856 | tf_op jit(solution)/shard_map/ppermute | solution.py:420
  77.9 0.9 collective-permute-done.13.refs_2_
  78.8 0.5 collective-permute-start.14
  79.3 1.6 %collective-permute-start.15 = (bf16[256,512]{1,0:T(8,128)(2,1)S(1)}, bf16[256,512]{1,0:T(8,128)(2,1)S(1)}, u32[]{:S(2)}, u32[]{:S(2)}) collective-permute-start(bf16[256,512]{1,0:T(8,128)(2,1)S(1)} %slice.11), channel_id=1, source_target_pairs={{8,0},{16,8},{24,16},{28,24},{20,28},{12,20},{4,12},{0,4},{9,1},{1... | collective-permute-start | bytes 786440 | tf_op jit(solution)/shard_map/ppermute | solution.py:438
  81.0 7.1 %attention.8.refs_3_ = f32[8,80,512]{2,1,0:T(8,128)S(1)} custom-call(bf16[8,512,128]{2,1,0:T(8,128)(2,1)S(1)} %queries.1.refs_0_, bf16[576,512]{1,0:T(8,128)(2,1)S(1)} %collective-permute-done.12.refs_1_, bf16[576,512]{1,0:T(8,128)(2,1)S(1)} %collective-permute-done.13.refs_2_, f32[8]{0:T(128)S(1)} %copy-done.4, f32[8,80,512]{2,1,0:T(8,128)S(1)} %attention.7.refs_4_), custom_call_target="tpu_custom_call" | custom-call | flops 4831838208 | bytes 2097152 | tf_op jit(solution)/shard_map/attention/pallas_call | solution.py:284
  88.1 0.0 collective-permute-done.14.refs_1_
  88.1 0.0 collective-permute-done.15.refs_2_
  88.1 0.0 collective-permute-done.16.refs_6_
  88.1 0.1 collective-permute-start.22
  88.2 4.2 %attention.9 = (bf16[128,512]{1,0:T(8,128)(2,1)S(1)}, bf16[128,512]{1,0:T(8,128)(2,1)S(1)}, bf16[128,512]{1,0:T(8,128)(2,1)S(1)}, bf16[128,512]{1,0:T(8,128)(2,1)S(1)}) custom-call(bf16[8,512,128]{2,1,0:T(8,128)(2,1)S(1)} %queries.1.refs_0_, bf16[256,512]{1,0:T(8,128)(2,1)S(1)} %collective-permute-done.14.refs_1_, ...), custom_call_target="tpu_custom_call" | custom-call | flops 2147483648 | bytes 2097152 | tf_op jit(solution)/shard_map/attention/pallas_call | solution.py:284
  92.4 1.6 %collective-permute-start.19 = (bf16[128,512]{1,0:T(8,128)(2,1)S(1)}, bf16[128,512]{1,0:T(8,128)(2,1)S(1)}, u32[]{:S(2)}, u32[]{:S(2)}) collective-permute-start(bf16[128,512]{1,0:T(8,128)(2,1)S(1)} %get-tuple-element.67), channel_id=1, source_target_pairs={{0,2},{1,3},{2,0},{3,1},{4,6},{5,7},{6,4},{7,5},{8,10},{9,11},{10,... | collective-permute-start | bytes 393224 | tf_op jit(solution)/shard_map/ppermute | solution.py:35
  94.0 0.2 collective-permute-start.17
  94.2 0.5 collective-permute-start.18
  94.7 4.1 %collective-permute-done.19 = bf16[128,512]{1,0:T(8,128)(2,1)S(1)} collective-permute-done((bf16[128,512]{1,0:T(8,128)(2,1)S(1)}, bf16[128,512]{1,0:T(8,128)(2,1)S(1)}, u32[]{:S(2)}, u32[]{:S(2)}) %collective-permute-start.19) | collective-permute-done | bytes 131104 | tf_op jit(solution)/shard_map/ppermute | solution.py:35
  98.8 0.0 collective-permute-start.20
  98.8 0.0 collective-permute-done.21.refs_5_
  98.8 0.0 collective-permute-done.17.refs_1_
  98.8 2.3 %collective-permute-done.18.refs_2_ = bf16[128,512]{1,0:T(8,128)(2,1)S(1)} collective-permute-done((bf16[128,512]{1,0:T(8,128)(2,1)S(1)}, bf16[128,512]{1,0:T(8,128)(2,1)S(1)}, u32[]{:S(2)}, u32[]{:S(2)}) %collective-permute-start.18) | collective-permute-done | bytes 131104 | tf_op jit(solution)/shard_map/ppermute | solution.py:35
  101.2 0.0 collective-permute-done.20.refs_3_
  101.2 0.0 collective-permute-done.22.refs_7_
  101.2 2.1 %output.1 = bf16[128,2048]{1,0:T(8,128)(2,1)} custom-call(bf16[128,512]{1,0:T(8,128)(2,1)S(1)} %get-tuple-element.64.refs_0_, bf16[128,512]{1,0:T(8,128)(2,1)S(1)} %collective-permute-done.17.refs_1_, bf16[128,512]{1,0:T(8,128)(2,1)S(1)} %collective-permute-done.18.refs_2_, bf16[128,512]{1,0:T(8,128)(2,1)S(1)} %collective-permute-done.20.refs_3_, ...), custom_call_target="tpu_custom_call" | custom-call | flops 1073741824 | bytes 8388608 | tf_op jit(solution)/shard_map/output/pallas_call | solution.py:322
  (19 shorter events, 0.1 us)
Async XLA Ops:
  0.0 14.8 %copy-start.5 = (bf16[2048,256]{1,0:T(8,128)(2,1)S(1)}, bf16[2048,256]{1,0:T(8,128)(2,1)}, u32[]{:S(2)}) copy-start(bf16[2048,256]{1,0:T(8,128)(2,1)} %param.25) | copy-start | bytes 3145732
  2.1 9.0 %collective-permute-start.1 = (f32[8,512]{1,0:T(8,128)}, f32[8,512]{1,0:T(8,128)S(1)}, u32[]{:S(2)}, u32[]{:S(2)}) collective-permute-start(f32[8,512]{1,0:T(8,128)} %modulation.1), channel_id=1, source_target_pairs={{0,4},{4,0},{8,12},{12,8},{16,20},{20,16},{24,28},{28,24},{1,5},{5... | collective-permute-start | bytes 49160 | tf_op jit(solution)/shard_map/ppermute | solution.py:35
  5.0 6.0 %collective-permute-start.2 = (f32[8,512]{1,0:T(8,128)}, f32[8,512]{1,0:T(8,128)S(1)}, u32[]{:S(2)}, u32[]{:S(2)}) collective-permute-start(f32[8,512]{1,0:T(8,128)} %modulation.1), channel_id=1, source_target_pairs={{0,8},{4,12},{8,0},{12,4},{16,24},{20,28},{24,16},{28,20},{1,9},{5... | collective-permute-start | bytes 49160 | tf_op jit(solution)/shard_map/ppermute | solution.py:35
  6.6 4.8 %collective-permute-start.3 = (f32[8,512]{1,0:T(8,128)}, f32[8,512]{1,0:T(8,128)S(1)}, u32[]{:S(2)}, u32[]{:S(2)}) collective-permute-start(f32[8,512]{1,0:T(8,128)} %modulation.1), channel_id=1, source_target_pairs={{0,12},{4,8},{8,4},{12,0},{16,28},{20,24},{24,20},{28,16},{1,13},{... | collective-permute-start | bytes 49160 | tf_op jit(solution)/shard_map/ppermute | solution.py:35
  6.6 20.2 %collective-permute-start = (bf16[128,2048]{1,0:T(8,128)(2,1)}, bf16[128,2048]{1,0:T(8,128)(2,1)S(1)}, u32[]{:S(2)}, u32[]{:S(2)}) collective-permute-start(bf16[128,2048]{1,0:T(8,128)(2,1)} %refs_8_.1), channel_id=1, source_target_pairs={{0,1},{1,0},{2,3},{3,2},{4,5},{5,4},{6,7},{7,6},{8,9},{9,8},{10,11... | collective-permute-start | bytes 1572872 | tf_op jit(solution)/shard_map/ppermute | solution.py:35
  6.6 14.7 %collective-permute-start.5 = (bf16[128,2048]{1,0:T(8,128)(2,1)}, bf16[128,2048]{1,0:T(8,128)(2,1)S(1)}, u32[]{:S(2)}, u32[]{:S(2)}) collective-permute-start(bf16[128,2048]{1,0:T(8,128)(2,1)} %refs_8_.1), channel_id=1, source_target_pairs={{0,2},{1,3},{2,0},{3,1},{4,6},{5,7},{6,4},{7,5},{8,10},{9,11},{10,... | collective-permute-start | bytes 1572872 | tf_op jit(solution)/shard_map/ppermute | solution.py:35
  12.2 14.6 %copy-start.2 = (bf16[128,2048]{1,0:T(8,128)(2,1)S(1)}, bf16[128,2048]{1,0:T(8,128)(2,1)}, u32[]{:S(2)}) copy-start(bf16[128,2048]{1,0:T(8,128)(2,1)} %refs_8_.1) | copy-start | bytes 1572868
  12.2 14.6 %copy-start.3 = (bf16[64,2048]{1,0:T(8,128)(2,1)S(1)}, bf16[64,2048]{1,0:T(8,128)(2,1)}, u32[]{:S(2)}) copy-start(bf16[64,2048]{1,0:T(8,128)(2,1)} %refs_4_.2) | copy-start | bytes 786436
  12.2 4.8 %collective-permute-start.4 = (f32[8,512]{1,0:T(8,128)S(1)}, f32[8,512]{1,0:T(8,128)S(1)}, u32[]{:S(2)}, u32[]{:S(2)}) collective-permute-start(f32[8,512]{1,0:T(8,128)S(1)} %add_add_fusion), channel_id=1, source_target_pairs={{0,16},{4,20},{8,24},{12,28},{16,0},{20,4},{24,8},{28,12},{1,17},{... | collective-permute-start | bytes 49160 | tf_op jit(solution)/shard_map/ppermute | solution.py:35
  21.3 5.4 %collective-permute-start.6 = (bf16[128,2048]{1,0:T(8,128)(2,1)S(1)}, bf16[128,2048]{1,0:T(8,128)(2,1)S(1)}, u32[]{:S(2)}, u32[]{:S(2)}) collective-permute-start(bf16[128,2048]{1,0:T(8,128)(2,1)S(1)} %collective-permute-done.5.refs_2_), channel_id=1, source_target_pairs={{0,1},{1,0},{2,3},{3,2},{4,5},{5,4},{6,7},{7,6},{8,9},{9,8},{10,11... | collective-permute-start | bytes 1572872 | tf_op jit(solution)/shard_map/ppermute | solution.py:35
  26.8 4.7 %copy-start = (bf16[512,2048]{1,0:T(8,128)(2,1)S(1)}, bf16[512,2048]{1,0:T(8,128)(2,1)}, u32[]{:S(2)}) copy-start(bf16[512,2048]{1,0:T(8,128)(2,1)} %refs_4_.4) | copy-start | bytes 6291460
  26.8 10.7 %copy-start.1 = (bf16[2048,512]{1,0:T(8,128)(2,1)S(1)}, bf16[2048,512]{1,0:T(8,128)(2,1)}, u32[]{:S(2)}) copy-start(bf16[2048,512]{1,0:T(8,128)(2,1)} %weight.1) | copy-start | bytes 6291460
  29.4 20.1 %collective-permute-start.7 = (bf16[576,512]{1,0:T(8,128)(2,1)S(1)}, bf16[576,512]{1,0:T(8,128)(2,1)S(1)}, u32[]{:S(2)}, u32[]{:S(2)}) collective-permute-start(bf16[576,512]{1,0:T(8,128)(2,1)S(1)} %get-tuple-element.49.refs_1_), channel_id=1, source_target_pairs={{0,8},{8,16},{16,24},{24,28},{28,20},{20,12},{12,4},{4,0},{1,9},{9... | collective-permute-start | bytes 1769480 | tf_op jit(solution)/shard_map/ppermute | solution.py:420
  31.0 18.5 %collective-permute-start.8 = (bf16[576,512]{1,0:T(8,128)(2,1)S(1)}, bf16[576,512]{1,0:T(8,128)(2,1)S(1)}, u32[]{:S(2)}, u32[]{:S(2)}) collective-permute-start(bf16[576,512]{1,0:T(8,128)(2,1)S(1)} %get-tuple-element.49.refs_1_), channel_id=1, source_target_pairs={{8,0},{16,8},{24,16},{28,24},{20,28},{12,20},{4,12},{0,4},{9,1},{1... | collective-permute-start | bytes 1769480 | tf_op jit(solution)/shard_map/ppermute | solution.py:421
  31.4 56.6 %collective-permute-start.16 = (bf16[512,2048]{1,0:T(8,128)(2,1)S(1)}, bf16[512,2048]{1,0:T(8,128)(2,1)S(1)}, u32[]{:S(2)}, u32[]{:S(2)}) collective-permute-start(bf16[512,2048]{1,0:T(8,128)(2,1)S(1)} %copy-done), channel_id=1, source_target_pairs={{0,2},{1,3},{2,0},{3,1},{4,6},{5,7},{6,4},{7,5},{8,10},{9,11},{10,... | collective-permute-start | bytes 6291464 | tf_op jit(solution)/shard_map/ppermute | solution.py:35
  33.0 16.5 %collective-permute-start.9 = (bf16[64,512]{1,0:T(8,128)(2,1)S(1)}, bf16[64,512]{1,0:T(8,128)(2,1)S(1)}, u32[]{:S(2)}, u32[]{:S(2)}) collective-permute-start(bf16[64,512]{1,0:T(8,128)(2,1)S(1)} %slice.9), channel_id=1, source_target_pairs={{0,28},{8,20},{16,12},{24,4},{28,0},{20,8},{12,16},{4,24},{1,29},{... | collective-permute-start | bytes 196616 | tf_op jit(solution)/shard_map/ppermute | solution.py:424
  37.5 3.3 %copy-start.4 = (f32[8]{0:T(128)S(1)}, f32[8]{0:T(128)}, u32[]{:S(2)}) copy-start(f32[8]{0:T(128)} %refs_3_.3) | copy-start | bytes 100
  49.5 14.6 %collective-permute-start.10 = (bf16[576,512]{1,0:T(8,128)(2,1)S(1)}, bf16[576,512]{1,0:T(8,128)(2,1)S(1)}, u32[]{:S(2)}, u32[]{:S(2)}) collective-permute-start(bf16[576,512]{1,0:T(8,128)(2,1)S(1)} %collective-permute-done.7.refs_1_), channel_id=1, source_target_pairs={{0,8},{8,16},{16,24},{24,28},{28,20},{20,12},{12,4},{4,0},{1,9},{9... | collective-permute-start | bytes 1769480 | tf_op jit(solution)/shard_map/ppermute | solution.py:420
  50.3 13.9 %collective-permute-start.11 = (bf16[576,512]{1,0:T(8,128)(2,1)S(1)}, bf16[576,512]{1,0:T(8,128)(2,1)S(1)}, u32[]{:S(2)}, u32[]{:S(2)}) collective-permute-start(bf16[576,512]{1,0:T(8,128)(2,1)S(1)} %collective-permute-done.8.refs_2_), channel_id=1, source_target_pairs={{8,0},{16,8},{24,16},{28,24},{20,28},{12,20},{4,12},{0,4},{9,1},{1... | collective-permute-start | bytes 1769480 | tf_op jit(solution)/shard_map/ppermute | solution.py:421
  64.2 13.7 %collective-permute-start.12 = (bf16[576,512]{1,0:T(8,128)(2,1)S(1)}, bf16[576,512]{1,0:T(8,128)(2,1)S(1)}, u32[]{:S(2)}, u32[]{:S(2)}) collective-permute-start(bf16[576,512]{1,0:T(8,128)(2,1)S(1)} %collective-permute-done.10.refs_1_), channel_id=1, source_target_pairs={{0,8},{8,16},{16,24},{24,28},{28,20},{20,12},{12,4},{4,0},{1,9},{9... | collective-permute-start | bytes 1769480 | tf_op jit(solution)/shard_map/ppermute | solution.py:420
  66.0 12.8 %collective-permute-start.13 = (bf16[576,512]{1,0:T(8,128)(2,1)S(1)}, bf16[576,512]{1,0:T(8,128)(2,1)S(1)}, u32[]{:S(2)}, u32[]{:S(2)}) collective-permute-start(bf16[576,512]{1,0:T(8,128)(2,1)S(1)} %collective-permute-done.11.refs_2_), channel_id=1, source_target_pairs={{8,0},{16,8},{24,16},{28,24},{20,28},{12,20},{4,12},{0,4},{9,1},{1... | collective-permute-start | bytes 1769480 | tf_op jit(solution)/shard_map/ppermute | solution.py:421
  66.2 32.6 %collective-permute-start.21 = (bf16[512,2048]{1,0:T(8,128)(2,1)S(1)}, bf16[512,2048]{1,0:T(8,128)(2,1)S(1)}, u32[]{:S(2)}, u32[]{:S(2)}) collective-permute-start(bf16[512,2048]{1,0:T(8,128)(2,1)S(1)} %copy-done), channel_id=1, source_target_pairs={{0,1},{1,0},{2,3},{3,2},{4,5},{5,4},{6,7},{7,6},{8,9},{9,8},{10,11... | collective-permute-start | bytes 6291464 | tf_op jit(solution)/shard_map/ppermute | solution.py:35
  78.8 9.2 %collective-permute-start.14 = (bf16[256,512]{1,0:T(8,128)(2,1)S(1)}, bf16[256,512]{1,0:T(8,128)(2,1)S(1)}, u32[]{:S(2)}, u32[]{:S(2)}) collective-permute-start(bf16[256,512]{1,0:T(8,128)(2,1)S(1)} %slice.10), channel_id=1, source_target_pairs={{0,8},{8,16},{16,24},{24,28},{28,20},{20,12},{12,4},{4,0},{1,9},{9... | collective-permute-start | bytes 786440 | tf_op jit(solution)/shard_map/ppermute | solution.py:437
  79.3 8.7 %collective-permute-start.15 = (bf16[256,512]{1,0:T(8,128)(2,1)S(1)}, bf16[256,512]{1,0:T(8,128)(2,1)S(1)}, u32[]{:S(2)}, u32[]{:S(2)}) collective-permute-start(bf16[256,512]{1,0:T(8,128)(2,1)S(1)} %slice.11), channel_id=1, source_target_pairs={{8,0},{16,8},{24,16},{28,24},{20,28},{12,20},{4,12},{0,4},{9,1},{1... | collective-permute-start | bytes 786440 | tf_op jit(solution)/shard_map/ppermute | solution.py:438
  88.1 13.1 %collective-permute-start.22 = (bf16[512,2048]{1,0:T(8,128)(2,1)S(1)}, bf16[512,2048]{1,0:T(8,128)(2,1)S(1)}, u32[]{:S(2)}, u32[]{:S(2)}) collective-permute-start(bf16[512,2048]{1,0:T(8,128)(2,1)S(1)} %collective-permute-done.16.refs_6_), channel_id=1, source_target_pairs={{0,1},{1,0},{2,3},{3,2},{4,5},{5,4},{6,7},{7,6},{8,9},{9,8},{10,11... | collective-permute-start | bytes 6291464 | tf_op jit(solution)/shard_map/ppermute | solution.py:35
  92.4 6.4 %collective-permute-start.19 = (bf16[128,512]{1,0:T(8,128)(2,1)S(1)}, bf16[128,512]{1,0:T(8,128)(2,1)S(1)}, u32[]{:S(2)}, u32[]{:S(2)}) collective-permute-start(bf16[128,512]{1,0:T(8,128)(2,1)S(1)} %get-tuple-element.67), channel_id=1, source_target_pairs={{0,2},{1,3},{2,0},{3,1},{4,6},{5,7},{6,4},{7,5},{8,10},{9,11},{10,... | collective-permute-start | bytes 393224 | tf_op jit(solution)/shard_map/ppermute | solution.py:35
  94.0 4.9 %collective-permute-start.17 = (bf16[128,512]{1,0:T(8,128)(2,1)S(1)}, bf16[128,512]{1,0:T(8,128)(2,1)S(1)}, u32[]{:S(2)}, u32[]{:S(2)}) collective-permute-start(bf16[128,512]{1,0:T(8,128)(2,1)S(1)} %get-tuple-element.65), channel_id=1, source_target_pairs={{0,1},{1,0},{2,3},{3,2},{4,5},{5,4},{6,7},{7,6},{8,9},{9,8},{10,11... | collective-permute-start | bytes 393224 | tf_op jit(solution)/shard_map/ppermute | solution.py:35
  94.2 7.0 %collective-permute-start.18 = (bf16[128,512]{1,0:T(8,128)(2,1)S(1)}, bf16[128,512]{1,0:T(8,128)(2,1)S(1)}, u32[]{:S(2)}, u32[]{:S(2)}) collective-permute-start(bf16[128,512]{1,0:T(8,128)(2,1)S(1)} %get-tuple-element.66), channel_id=1, source_target_pairs={{0,2},{1,3},{2,0},{3,1},{4,6},{5,7},{6,4},{7,5},{8,10},{9,11},{10,... | collective-permute-start | bytes 393224 | tf_op jit(solution)/shard_map/ppermute | solution.py:35
  98.8 2.3 %collective-permute-start.20 = (bf16[128,512]{1,0:T(8,128)(2,1)S(1)}, bf16[128,512]{1,0:T(8,128)(2,1)S(1)}, u32[]{:S(2)}, u32[]{:S(2)}) collective-permute-start(bf16[128,512]{1,0:T(8,128)(2,1)S(1)} %collective-permute-done.19), channel_id=1, source_target_pairs={{0,1},{1,0},{2,3},{3,2},{4,5},{5,4},{6,7},{7,6},{8,9},{9,8},{10,11... | collective-permute-start | bytes 393224 | tf_op jit(solution)/shard_map/ppermute | solution.py:35
where the time goes:
time: 104 us; the launch traced here: 103 us
  Pallas kernels  40.8 us (39%)
  waiting for transfers between devices  26.4 us (25%)
  starting transfers between devices  25.9 us (25%)
  blocking collectives  5.43 us (5%)
  other arithmetic  3.75 us (4%)
    pallas_call x5, Pallas kernels, attention(): pl.pallas_call(functools.partial(attention_kernel, spans, lifted, state i...  30.8 us
    ppermute x14, starting transfers between devices, swap(): return lax.ppermute(value, axis, [(i, i ^ mask) for i in range(size)])  13.1 us
    ppermute x14, waiting for transfers between devices, swap(): return lax.ppermute(value, axis, [(i, i ^ mask) for i in range(size)])  12 us
    ppermute x3, waiting for transfers between devices, shards(): up = lax.ppermute(up, 'sp', ahead)  9.88 us
    all_gather x1, blocking collectives, shards(): mod = lax.all_gather(partial, 'tp', axis=0, tiled=True)  5.43 us
    ppermute x1, starting transfers between devices, shards(): far_context = lax.ppermute(packed[length:], 'sp', across)  4.53 us
    ppermute x3, starting transfers between devices, shards(): up = lax.ppermute(up, 'sp', ahead)  4.24 us
    ppermute x1, waiting for transfers between devices, shards(): far_context = lax.ppermute(packed[length:], 'sp', across)  3.48 us
  transfers between devices with their start and end apart: 23, of which 10 were waited for; matrix products, arithmetic and copies ran while one was open for 4% of the time, Pallas kernels for 33%

commit v1 on v0

--- a/solution.py
+++ b/solution.py
@@ -107,7 +107,8 @@
 def kv_kernel(count, *refs):
     pieces = refs[:count]
     context, mod, gains, weight, cos, sin_e, sin_o = refs[count : count + 7]
-    hidden, packed = refs[count + 7 :]
+    hidden, first, second = refs[count + 7 :]
+    half = first.shape[0]
     norm_gain = gains[:, : context.shape[1]]
     key_gain = gains[:, context.shape[1] : context.shape[1] + HEAD]
     parts = mod.shape[0] // 8
@@ -129,23 +130,25 @@
     tables = (cos[...], sin_e[...], sin_o[...])
     heads = finish_heads(keys, key_gain, tables)
     for k, key in enumerate(heads):
-        packed[:, k * TILE : (k + 1) * TILE] = jnp.concatenate(
-            [key, values[:, k * HEAD : (k + 1) * HEAD]], axis=1
-        ).astype(BF16)
+        tile = jnp.concatenate([key, values[:, k * HEAD : (k + 1) * HEAD]], axis=1).astype(BF16)
+        first[:, k * TILE : (k + 1) * TILE] = tile[:half]
+        second[:, k * TILE : (k + 1) * TILE] = tile[half:]
 
 
 def keys_values(pieces, context, mod, gains, weight, tables):
     rows = sum(p.shape[0] for p in pieces) + context.shape[0]
     depth = context.shape[1]
     width = weight.shape[1] // 2
+    half = (rows - context.shape[0]) // 2
     return pl.pallas_call(
         functools.partial(kv_kernel, len(pieces)),
         out_shape=(
             jax.ShapeDtypeStruct((rows, depth), BF16),
-            jax.ShapeDtypeStruct((rows, 2 * width), BF16),
+            jax.ShapeDtypeStruct((half, 2 * width), BF16),
+            jax.ShapeDtypeStruct((rows - half, 2 * width), BF16),
         ),
         in_specs=[IN_VMEM] * (len(pieces) + 7),
-        out_specs=(IN_VMEM, IN_VMEM),
+        out_specs=(IN_VMEM, IN_VMEM, IN_VMEM),
         compiler_params=pltpu.CompilerParams(vmem_limit_bytes=VMEM_LIMIT),
         cost_estimate=cost(4 * rows * depth * width, 4 * rows * depth + 4 * depth * width),
         name="keys_values",
@@ -181,7 +184,7 @@
 STATE = HEAD + 16
 
 
-def attention_kernel(spans, lifted, has_state, final, group, chunk, *refs):
+def attention_kernel(spans, lifted, has_state, final, group, chunk, window, unrolled, *refs):
     refs = list(refs)
     q_ref = refs.pop(0)
     blocks = [refs.pop(0) for _ in spans]
@@ -189,7 +192,7 @@
     state = refs.pop(0) if has_state else None
     value_rows, held = refs[-3], refs[-2:]
     outs = refs[:-3]
-    rows = q_ref.shape[1]
+    low, high = window
     kv_heads = q_ref.shape[0] // group
     sizes = [end - first for first, _, end in spans]
     starts = [sum(sizes[:i]) for i in range(len(sizes))]
@@ -200,71 +203,91 @@
         if end > middle
     ]
 
+    def aligned(k, width):
+        return k * width if isinstance(k, int) else pl.multiple_of(k * width, width)
+
     def tile(ref, span, k):
-        return ref[span[0] : span[2], pl.ds(pl.multiple_of(k * TILE, TILE), TILE)]
+        return ref[span[0] : span[2], pl.ds(aligned(k, TILE), TILE)]
 
     for k in range(kv_heads):
         for ref, span, start, size in zip(blocks, spans, starts, sizes):
             value_rows[k, 0:HEAD, start : start + size] = tile(ref, span, k).T[HEAD:]
             value_rows[k, HEAD:, start : start + size] = jnp.ones((16, size), BF16)
 
-    work = [(g, r) for r in range(0, rows, chunk) for g in range(group)]
-
-    def scores(k, item, slot):
-        g, r = item
-        q = q_ref[k * group + g, r : r + chunk, :]
+    work = list(range(low, high, chunk))
+
+    def scores(k, r, slot):
+        q = q_ref[pl.ds(k * group, group), r : r + chunk, :].reshape(group * chunk, TILE)
         for ref, span, start, size in zip(blocks, spans, starts, sizes):
             held[slot][start : start + size, :] = lax.dot_general(
                 tile(ref, span, k), q, NT, preferred_element_type=F32
             )
 
-    def absorb(k, item, slot):
-        g, r = item
-        h = k * group + g
+    def both(k, value):
+        return jnp.concatenate(
+            [jnp.full((1, chunk), value[k * group + g], F32) for g in range(group)], axis=1
+        )
+
+    def absorb(k, r, slot):
         parts = [(st, held[slot][st : st + n, :]) for st, n in plain]
-        parts += [(st, held[slot][st : st + n, :] + lift[h]) for st, n in raised]
+        if raised:
+            extra = both(k, lift)
+            parts += [(st, held[slot][st : st + n, :] + extra) for st, n in raised]
         top = functools.reduce(
             jnp.maximum, [jnp.max(x, axis=0, keepdims=True) for _, x in parts]
         )
         if has_state:
-            before = state[h, HEAD + 8 : HEAD + 9, r : r + chunk]
+            old = [state[k * group + g, :, r : r + chunk] for g in range(group)]
+            old = jnp.concatenate(old, axis=1)
+            before = old[HEAD + 8 : HEAD + 9]
             top = jnp.maximum(top, before)
         parts.sort(key=lambda part: part[0])
         weights = jnp.concatenate([jnp.exp(x - top).astype(BF16) for _, x in parts], axis=0)
         total = dot(value_rows[k], weights)
         if has_state:
-            total = total + state[h, :, r : r + chunk] * jnp.exp(before - top)
+            total = total + old * jnp.exp(before - top)
         if not final:
-            outs[0][h, 0 : HEAD + 8, r : r + chunk] = total[: HEAD + 8]
-            outs[0][h, HEAD + 8 :, r : r + chunk] = jnp.broadcast_to(top, (8, chunk))
-            return None
-        return total[:HEAD] / total[HEAD : HEAD + 1]
+            for g in range(group):
+                lanes = slice(g * chunk, (g + 1) * chunk)
+                out = outs[0].at[k * group + g]
+                out[0 : HEAD + 8, r : r + chunk] = total[: HEAD + 8, lanes]
+                out[HEAD + 8 :, r : r + chunk] = jnp.broadcast_to(top[:, lanes], (8, chunk))
+            return
+        value = total[:HEAD] / total[HEAD : HEAD + 1]
+        whole = [value[:, g * chunk : (g + 1) * chunk] for g in range(group)]
+        whole = jnp.concatenate(whole, axis=0).T.astype(BF16)
+        size = outs[0].shape[0]
+        width = group * HEAD
+        for j in range(0, chunk, size):
+            outs[(r - low + j) // size][:, pl.ds(aligned(k, width), width)] = whole[j : j + size]
 
     scores(0, work[0], 0)
 
-    @pl.loop(0, kv_heads)
-    def _(k):
-        done = {}
-        for i, item in enumerate(work):
+    def slot_of(k, i):
+        return (k * len(work) + i) % 2 if isinstance(k, int) else i % 2
+
+    def one_head(k):
+        for i, r in enumerate(work):
             if i + 1 < len(work):
-                scores(k, work[i + 1], (i + 1) % 2)
-            else:
-                scores(jnp.minimum(k + 1, kv_heads - 1), work[0], (i + 1) % 2)
-            g, r = item
-            done[g] = absorb(k, item, i % 2)
-            if final and g == group - 1:
-                whole = jnp.concatenate([done[j] for j in range(group)], axis=0).T.astype(BF16)
-                size = outs[0].shape[0]
-                width = group * HEAD
-                lanes = pl.ds(pl.multiple_of(k * width, width), width)
-                for j in range(0, chunk, size):
-                    outs[(r + j) // size][:, lanes] = whole[j : j + size]
-
-
-def attention(queries, blocks, lift, state, group, pieces):
+                scores(k, work[i + 1], slot_of(k, i + 1))
+            elif not isinstance(k, int):
+                scores(jnp.minimum(k + 1, kv_heads - 1), work[0], slot_of(k, i + 1))
+            elif k + 1 < kv_heads:
+                scores(k + 1, work[0], slot_of(k, i + 1))
+            absorb(k, r, slot_of(k, i))
+
+    if unrolled or len(work) % 2:
+        for k in range(kv_heads):
+            one_head(k)
+    else:
+        pl.loop(0, kv_heads)(one_head)
+
+
+def attention(queries, blocks, lift, state, group, pieces, window=None):
     heads, rows, _ = queries.shape
     kv_heads = heads // group
-    chunk = min(rows, 256)
+    low, high = window or (0, rows)
+    chunk = min(high - low, 256)
     final = pieces > 0
     spans = [b[1:] for b in blocks]
     keys = sum(end - first for first, _, end in spans)
@@ -278,20 +301,20 @@
         in_specs.append(IN_VMEM)
         args.append(state)
     if final:
-        out_shape = [jax.ShapeDtypeStruct((rows // pieces, heads * HEAD), BF16)] * pieces
+        out_shape = [jax.ShapeDtypeStruct(((high - low) // pieces, heads * HEAD), BF16)] * pieces
     else:
         out_shape = [jax.ShapeDtypeStruct((heads, STATE, rows), F32)]
     out = pl.pallas_call(
         functools.partial(
-            attention_kernel, spans, lifted, state is not None, final, group, chunk
+            attention_kernel, spans, lifted, state is not None, final, group, chunk, (low, high), True
         ),
         in_specs=in_specs,
         out_specs=[IN_VMEM] * len(out_shape),
         out_shape=out_shape,
         scratch_shapes=[
             pltpu.VMEM((kv_heads, STATE, keys), BF16),
-            pltpu.VMEM((keys, chunk), F32),
-            pltpu.VMEM((keys, chunk), F32),
+            pltpu.VMEM((keys, group * chunk), F32),
+            pltpu.VMEM((keys, group * chunk), F32),
         ],
         compiler_params=pltpu.CompilerParams(vmem_limit_bytes=VMEM_LIMIT),
         cost_estimate=cost(16 * heads * rows * keys * HEAD, 4 * heads * rows * TILE),
@@ -303,31 +326,34 @@
 def output_kernel(count, *refs):
     attended = refs[:count]
     weights = refs[count : 2 * count]
-    latent, mod, out = refs[2 * count :]
-    step = mod.shape[1]
-    for i in range(out.shape[1] // step):
+    rest, out = refs[2 * count : -1], refs[-1]
+    step = min(out.shape[1], 4 * TILE)
+    for i in range(0, out.shape[1], step):
         total = None
         for a, w in zip(attended, weights):
-            term = dot(a[...], w[:, i * step : (i + 1) * step])
+            term = dot(a[...], w[:, i : i + step])
             total = term if total is None else total + term
-        gate = mod[8 * i + 2 : 8 * i + 3, :]
-        old = latent[:, i * step : (i + 1) * step].astype(F32)
-        out[:, i * step : (i + 1) * step] = (old + gate * total).astype(BF16)
-
-
-def project(attended, weights, latent, mod):
+        if rest:
+            begun, latent, mod = rest
+            gate = [mod[8 * t + 2 : 8 * t + 3, :] for t in range(mod.shape[0] // 8)]
+            gate = jnp.concatenate(gate, axis=1)[:, i : i + step]
+            total = latent[:, i : i + step].astype(F32) + gate * (begun[:, i : i + step] + total)
+        out[:, i : i + step] = total.astype(out.dtype)
+
+
+def project(attended, weights, begun, latent, mod, depth):
     count = len(attended)
-    rows, depth = latent.shape
-    inner = attended[0].shape[1]
+    rows, inner = attended[0].shape
+    rest = [] if begun is None else [begun, latent, mod]
     return pl.pallas_call(
         functools.partial(output_kernel, count),
-        in_specs=[IN_VMEM] * (2 * count + 2),
+        in_specs=[IN_VMEM] * (2 * count + len(rest)),
         out_specs=IN_VMEM,
-        out_shape=jax.ShapeDtypeStruct((rows, depth), BF16),
+        out_shape=jax.ShapeDtypeStruct((rows, depth), BF16 if rest else F32),
         compiler_params=pltpu.CompilerParams(vmem_limit_bytes=VMEM_LIMIT),
         cost_estimate=cost(2 * rows * depth * inner * count, 2 * depth * inner * count),
         name="output",
-    )(*attended, *weights, latent, mod)
+    )(*attended, *weights, *rest)
 
 
 def rotary_tables(rank, tp, rows, context_rows):
@@ -405,48 +431,46 @@
         spread(pieces, bit)
     mod = lax.all_gather(partial, "tp", axis=0, tiled=True)
 
-    hidden, packed = keys_values(
+    hidden, first, second = keys_values(
         [pieces[j] for j in range(tp)], context, mod, gains, kv_weight, tables
     )
 
+    half = length // 2
     order = list(range(0, sp, 2)) + list(range(sp - 1, 0, -2))
     ahead = [(order[i], order[(i + 1) % sp]) for i in range(sp)]
     back = [(b, a) for a, b in ahead]
-    across = [(order[i], order[(i + sp // 2) % sp]) for i in range(sp)]
-    up, down = packed, packed
-    waiting = [(packed, 0, length, length + context_rows)]
+
+    def hop(pair):
+        return lax.ppermute(pair[0], "sp", ahead), lax.ppermute(pair[1], "sp", back)
+
+    def as_blocks(pair):
+        return [(b, 0, half, half if b.shape[0] == half else half + context_rows) for b in pair]
+
+    flight = [hop((first, second))]
+    flight.append(hop((second, first)))
+    queries = queries_of(hidden, query_weight, gains, tables, length)
+    output_weight, _ = tie(output_weight, first)
+    weights = {0: output_weight}
+    spread(weights, tp_bits[0])
+    waiting = as_blocks((first, second))
     state = None
-    for step in range(1, sp // 2):
-        up = lax.ppermute(up, "sp", ahead)
-        down = lax.ppermute(down, "sp", back)
-        if step == 1:
-            queries = queries_of(hidden, query_weight, gains, tables, length)
-            far_context = lax.ppermute(packed[length:], "sp", across)
-            output_weight, _ = tie(output_weight, packed)
-            weights = {0: output_weight}
-            spread(weights, tp_bits[0])
+    for i in range(sp - 1):
         state = attention(queries, waiting, context_lift, state, group, 0)
-        if step == 1:
-            up, down, state, far_context = tie(up, down, state, far_context)
-        else:
-            up, down, state = tie(up, down, state)
-        waiting = [(b, 0, length, length + context_rows) for b in (up, down)]
-        if step == 2:
-            waiting.append((far_context, 0, 0, context_rows))
-    half = length // 2
-    up = lax.ppermute(up[:half], "sp", ahead)
-    down = lax.ppermute(down[half:length], "sp", back)
-    state = attention(queries, waiting, context_lift, state, group, 0)
-    first = tp_bits[0]
-    up, down, state, weights[first] = tie(up, down, state, weights[first])
+        up, down, state = tie(*flight.pop(0), state)
+        if i < sp - 3:
+            flight.append(hop((up, down)))
+        waiting = as_blocks((up, down))
+    far = attention(queries, waiting, context_lift, state, group, tp // 2, (half, length))
+    top_bit = tp_bits[0]
+    weights[top_bit], state, *_ = tie(weights[top_bit], state, *far)
     for bit in tp_bits[1:]:
         spread(weights, bit)
-    attended = attention(
-        queries, [(up, 0, half, half), (down, 0, half, half)], context_lift, state, group, tp
-    )
-    for bit in tp_bits:
-        attended = [swap(a, "tp", tp, bit) if j & bit else a for j, a in enumerate(attended)]
-    return project(attended, [weights[j] for j in range(tp)], latent, mod)
+    far = [swap(a, "tp", tp, tp // 2 + j) for j, a in enumerate(far)]
+    near = attention(queries, waiting, context_lift, state, group, tp // 2, (0, half))
+    near = near[:1] + [swap(a, "tp", tp, j) for j, a in enumerate(near) if j]
+    weights = [weights[j] for j in range(tp)]
+    begun = project(near, weights[: tp // 2], None, None, None, latent.shape[1])
+    return project(far, weights[tp // 2 :], begun, latent, mod, latent.shape[1])
 
 
 def solution(mesh):

time: 104 us -> 92.6 us (0.89)
  waiting for transfers between devices: 26.4 us -> 9.74 us
  Pallas kernels: 40.8 us -> 44.8 us
  starting transfers between devices: 25.9 us -> 27.5 us
    ppermute x9 -> x14, waiting for transfers between devices: 14.4 us -> 0.25 us  [the longest x7 0.21 us: hop(): lax.ppermute(pair[1], 'sp', back)]
    pallas_call x5 -> x9, Pallas kernels: 30.8 us -> 34.5 us  [attention(): pl.pallas_call(functools.partial(attention_kernel, spans, lifted, state i...]
    ppermute x14 -> x13, waiting for transfers between devices: 12 us -> 9.49 us  [swap(): return lax.ppermute(value, axis, [(i, i ^ mask) for i in range(size)])]
    ppermute x9 -> x14, starting transfers between devices: 12.8 us -> 14.4 us  [the longest x7 7.49 us: hop(): lax.ppermute(pair[1], 'sp', back)]
    pallas_call x1 -> x2, Pallas kernels: 2.12 us -> 2.39 us  [project(): pl.pallas_call(functools.partial(output_kernel, count), in_specs=[IN_VMEM...]
    ppermute x14 -> x13, starting transfers between devices: 13.1 us -> 13.1 us  [swap(): return lax.ppermute(value, axis, [(i, i ^ mask) for i in range(size)])]
  transfers between devices with their start and end apart: 23 -> 27, of which waited for: 10 -> 6; matrix products, arithmetic and copies ran while one was open for 4% -> 5% of each run, Pallas kernels for 33% -> 42%
where the time goes in v1:
time: 92.6 us; the launch traced here: 92.3 us
  Pallas kernels  44.8 us (48%)
  starting transfers between devices  27.5 us (30%)
  waiting for transfers between devices  9.74 us (11%)
  blocking collectives  5.34 us (6%)
  other arithmetic  3.75 us (4%)
    pallas_call x9, Pallas kernels, attention(): pl.pallas_call(functools.partial(attention_kernel, spans, lifted, state i...  34.5 us
    ppermute x13, starting transfers between devices, swap(): return lax.ppermute(value, axis, [(i, i ^ mask) for i in range(size)])  13.1 us
    ppermute x13, waiting for transfers between devices, swap(): return lax.ppermute(value, axis, [(i, i ^ mask) for i in range(size)])  9.49 us
    ppermute x7, starting transfers between devices, hop(): lax.ppermute(pair[1], 'sp', back)  7.49 us
    ppermute x7, starting transfers between devices, hop(): lax.ppermute(pair[0], 'sp', ahead)  6.96 us
    all_gather x1, blocking collectives, shards(): mod = lax.all_gather(partial, 'tp', axis=0, tiled=True)  5.34 us
    pallas_call x1, Pallas kernels, queries_of(): pl.pallas_call(query_kernel, in_specs=[IN_VMEM] * 6, out_specs=IN_VMEM, o...  3.25 us
    pallas_call x1, Pallas kernels, keys_values(): pl.pallas_call(functools.partial(kv_kernel, len(pieces)), out_shape=(jax....  2.55 us
  transfers between devices with their start and end apart: 27, of which 6 were waited for; matrix products, arithmetic and copies ran while one was open for 5% of the time, Pallas kernels for 42%

profile of v1, /device:TPU:0, one launch (start us, length us, event | category | flops | bytes accessed | tf_op | source)
XLA Modules:
  0.0 92.3 jit_solution(4144671747481775069)
XLA Ops:
  0.0 2.1 %modulation.1 = f32[8,512]{1,0:T(8,128)} custom-call(f32[1,256]{1,0:T(1,128)} %bitcast.6, f32[1,256]{1,0:T(1,128)} %bitcast.7, bf16[256,512]{1,0:T(8,128)(2,1)} %shift.1, bf16[256,512]{1,0:T(8,128)(2,1)} %scale.1, bf16[256,512]{1,0:T(8,128)(2,1)} %gate.1), custom_call_target="tpu_custom_call" | custom-call | flops 6291456 | bytes 786432 | tf_op jit(solution)/shard_map/modulation/pallas_call | solution.py:59
  2.1 3.0 %collective-permute-start.1 = (f32[8,512]{1,0:T(8,128)}, f32[8,512]{1,0:T(8,128)S(1)}, u32[]{:S(2)}, u32[]{:S(2)}) collective-permute-start(f32[8,512]{1,0:T(8,128)} %modulation.1), channel_id=1, source_target_pairs={{0,4},{4,0},{8,12},{12,8},{16,20},{20,16},{24,28},{28,24},{1,5},{5... | collective-permute-start | bytes 49160 | tf_op jit(solution)/shard_map/ppermute | solution.py:35
  5.0 1.6 %collective-permute-start.2 = (f32[8,512]{1,0:T(8,128)}, f32[8,512]{1,0:T(8,128)S(1)}, u32[]{:S(2)}, u32[]{:S(2)}) collective-permute-start(f32[8,512]{1,0:T(8,128)} %modulation.1), channel_id=1, source_target_pairs={{0,8},{4,12},{8,0},{12,4},{16,24},{20,28},{24,16},{28,20},{1,9},{5... | collective-permute-start | bytes 49160 | tf_op jit(solution)/shard_map/ppermute | solution.py:35
  6.6 0.0 collective-permute-start.3
  6.6 1.9 %collective-permute-start.5 = (bf16[128,2048]{1,0:T(8,128)(2,1)}, bf16[128,2048]{1,0:T(8,128)(2,1)S(1)}, u32[]{:S(2)}, u32[]{:S(2)}) collective-permute-start(bf16[128,2048]{1,0:T(8,128)(2,1)} %refs_5_.1), channel_id=1, source_target_pairs={{0,2},{1,3},{2,0},{3,1},{4,6},{5,7},{6,4},{7,5},{8,10},{9,11},{10,... | collective-permute-start | bytes 1572872 | tf_op jit(solution)/shard_map/ppermute | solution.py:35
  8.6 1.6 %fusion.13 = (f32[576,128]{1,0:T(8,128)S(1)}, f32[576,128]{1,0:T(8,128)S(1)}, f32[576,128]{1,0:T(8,128)S(1)}) fusion(s32[128]{0:T(128)S(1)} %get-tuple-element.100, s32[128]{0:T(128)S(1)} %get-tuple-element.102, pred[128]{0:T(512)(128)(4,1)S(1)} %get-tuple-element.98, s32[576]{0:T(1024)S(1)} %get-tuple-element.93, s32[576]{0:T(1024)S(1)} %get-tuple-element.94, ...), kind=kLoop, calls=%fused_computation.31 | loop fusion | flops 4792320 | bytes 897992 | tf_op jit(solution)/shard_map/jit(_where)/select_n | solution.py:371
  10.3 0.8 concatenate.6.refs_6_.gains
  11.1 0.0 collective-permute-done.1
  11.1 0.0 collective-permute-done.2
  11.1 0.4 collective-permute-done.3
  11.4 0.7 add_add_fusion
  12.2 2.7 %collective-permute-start.4 = (f32[8,512]{1,0:T(8,128)S(1)}, f32[8,512]{1,0:T(8,128)S(1)}, u32[]{:S(2)}, u32[]{:S(2)}) collective-permute-start(f32[8,512]{1,0:T(8,128)S(1)} %add_add_fusion), channel_id=1, source_target_pairs={{0,16},{4,20},{8,24},{12,28},{16,0},{20,4},{24,8},{28,12},{1,17},{... | collective-permute-start | bytes 49160 | tf_op jit(solution)/shard_map/ppermute | solution.py:35
  14.8 1.4 %pad_maximum_fusion.refs_7_ = bf16[2048,512]{1,0:T(8,128)(2,1)S(1)} fusion(bf16[2048,256]{1,0:T(8,128)(2,1)S(1)} %copy-done.5, bf16[2048,256]{1,0:T(8,128)(2,1)} %param.24), kind=kLoop, calls=%fused_computation | loop fusion | flops 4194304 | bytes 4194304 | tf_op jit(solution)/shard_map/concatenate | solution.py:414
  16.2 0.7 collective-permute-done.4
  16.9 3.0 %collective-permute-done.5.refs_2_ = bf16[128,2048]{1,0:T(8,128)(2,1)S(1)} collective-permute-done((bf16[128,2048]{1,0:T(8,128)(2,1)}, bf16[128,2048]{1,0:T(8,128)(2,1)S(1)}, u32[]{:S(2)}, u32[]{:S(2)}) %collective-permute-start.5) | collective-permute-done | bytes 524320 | tf_op jit(solution)/shard_map/ppermute | solution.py:35
  19.9 5.3 %all_gather.3.refs_5_.refs_6_ = f32[32,512]{1,0:T(8,128)S(1)} all-gather(f32[8,512]{1,0:T(8,128)S(1)} %add.75), channel_id=1, replica_groups=mesh['sp'=8,'tp'=4] {'tp'}, dimensions={0}, use_global_device_ids=true | all-gather | bytes 81920 | tf_op jit(solution)/shard_map/all_gather | solution.py:432
  25.3 0.0 collective-permute-done.refs_1_
  25.3 0.0 collective-permute-done.6.refs_3_
  25.3 2.5 %keys_values.1 = (bf16[576,2048]{1,0:T(8,128)(2,1)S(1)}, bf16[256,512]{1,0:T(8,128)(2,1)S(1)}, bf16[320,512]{1,0:T(8,128)(2,1)S(1)}) custom-call(bf16[128,2048]{1,0:T(8,128)(2,1)S(1)} %copy-done.2, bf16[128,2048]{1,0:T(8,128)(2,1)S(1)} %collective-permute-done.refs_1_, bf16[128,2048]{1,0:T(8,128)(2,1)S(1)} %collective-permute-done.5.refs_2_, ...), custom_call_target="tpu_custom_call" | custom-call | flops 1207959552 | bytes 6815744 | tf_op jit(solution)/shard_map/keys_values/pallas_call | solution.py:143
  27.9 1.6 %collective-permute-start.23 = (bf16[512,2048]{1,0:T(8,128)(2,1)S(1)}, bf16[512,2048]{1,0:T(8,128)(2,1)S(1)}, u32[]{:S(2)}, u32[]{:S(2)}) collective-permute-start(bf16[512,2048]{1,0:T(8,128)(2,1)S(1)} %copy-done.1), channel_id=1, source_target_pairs={{0,2},{1,3},{2,0},{3,1},{4,6},{5,7},{6,4},{7,5},{8,10},{9,11},{10,... | collective-permute-start | bytes 6291464 | tf_op jit(solution)/shard_map/ppermute | solution.py:35
  29.5 1.5 %collective-permute-start.8 = (bf16[320,512]{1,0:T(8,128)(2,1)S(1)}, bf16[320,512]{1,0:T(8,128)(2,1)S(1)}, u32[]{:S(2)}, u32[]{:S(2)}) collective-permute-start(bf16[320,512]{1,0:T(8,128)(2,1)S(1)} %get-tuple-element.60.refs_2_), channel_id=1, source_target_pairs={{8,0},{16,8},{24,16},{28,24},{20,28},{12,20},{4,12},{0,4},{9,1},{1... | collective-permute-start | bytes 983048 | tf_op jit(solution)/shard_map/ppermute | solution.py:444
  31.0 0.5 collective-permute-start.7
  31.5 1.6 %collective-permute-start.11 = (bf16[320,512]{1,0:T(8,128)(2,1)S(1)}, bf16[320,512]{1,0:T(8,128)(2,1)S(1)}, u32[]{:S(2)}, u32[]{:S(2)}) collective-permute-start(bf16[320,512]{1,0:T(8,128)(2,1)S(1)} %get-tuple-element.60.refs_2_), channel_id=1, source_target_pairs={{0,8},{8,16},{16,24},{24,28},{28,20},{20,12},{12,4},{4,0},{1,9},{9... | collective-permute-start | bytes 983048 | tf_op jit(solution)/shard_map/ppermute | solution.py:444
  33.1 0.4 collective-permute-start.12
  33.5 3.2 %queries.1.refs_0_ = bf16[8,512,128]{2,1,0:T(8,128)(2,1)S(1)} custom-call(bf16[576,2048]{1,0:T(8,128)(2,1)S(1)} %get-tuple-element.58.hidden, bf16[2048,512]{1,0:T(8,128)(2,1)S(1)} %copy-done, f32[1,2176]{1,0:T(1,128)S(1)} %concatenate.6.refs_6_.gains, f32[576,128]{1,0:T(8,128)S(1)} %get-tuple-element.55.refs_8_.cos, ...), custom_call_target="tpu_custom_call" | custom-call | flops 1073741824 | bytes 4194304 | tf_op jit(solution)/shard_map/queries/pallas_call | solution.py:173
  36.8 4.1 %attention.9.refs_4_ = f32[8,80,512]{2,1,0:T(8,128)S(1)} custom-call(bf16[8,512,128]{2,1,0:T(8,128)(2,1)S(1)} %queries.1.refs_0_, bf16[256,512]{1,0:T(8,128)(2,1)S(1)} %get-tuple-element.59.refs_1_, bf16[320,512]{1,0:T(8,128)(2,1)S(1)} %get-tuple-element.60.refs_2_, f32[8]{0:T(128)S(1)} %copy-done.4), custom_call_target="tpu_custom_call" | custom-call | flops 2415919104 | bytes 2097152 | tf_op jit(solution)/shard_map/attention/pallas_call | solution.py:307
  40.9 0.0 collective-permute-done.7.refs_1_
  40.9 1.5 %collective-permute-start.10 = (bf16[320,512]{1,0:T(8,128)(2,1)S(1)}, bf16[320,512]{1,0:T(8,128)(2,1)S(1)}, u32[]{:S(2)}, u32[]{:S(2)}) collective-permute-start(bf16[320,512]{1,0:T(8,128)(2,1)S(1)} %collective-permute-done.8.refs_2_), channel_id=1, source_target_pairs={{8,0},{16,8},{24,16},{28,24},{20,28},{12,20},{4,12},{0,4},{9,1},{1... | collective-permute-start | bytes 983048 | tf_op jit(solution)/shard_map/ppermute | solution.py:444
  42.4 0.5 collective-permute-start.9
  43.0 4.2 %attention.10.refs_4_ = f32[8,80,512]{2,1,0:T(8,128)S(1)} custom-call(bf16[8,512,128]{2,1,0:T(8,128)(2,1)S(1)} %queries.1.refs_0_, bf16[256,512]{1,0:T(8,128)(2,1)S(1)} %collective-permute-done.7.refs_1_, bf16[320,512]{1,0:T(8,128)(2,1)S(1)} %collective-permute-done.8.refs_2_, f32[8]{0:T(128)S(1)} %copy-done.4, f32[8,80,512]{2,1,0:T(8,128)S(1)} %attention.9.refs_4_), custom_call_target="tpu_custom_call" | custom-call | flops 2415919104 | bytes 2097152 | tf_op jit(solution)/shard_map/attention/pallas_call | solution.py:307
  47.2 1.6 %collective-permute-start.15 = (bf16[320,512]{1,0:T(8,128)(2,1)S(1)}, bf16[320,512]{1,0:T(8,128)(2,1)S(1)}, u32[]{:S(2)}, u32[]{:S(2)}) collective-permute-start(bf16[320,512]{1,0:T(8,128)(2,1)S(1)} %collective-permute-done.11.refs_1_), channel_id=1, source_target_pairs={{0,8},{8,16},{16,24},{24,28},{28,20},{20,12},{12,4},{4,0},{1,9},{9... | collective-permute-start | bytes 983048 | tf_op jit(solution)/shard_map/ppermute | solution.py:444
  48.9 0.5 collective-permute-start.16
  49.3 4.2 %attention.11.refs_4_ = f32[8,80,512]{2,1,0:T(8,128)S(1)} custom-call(bf16[8,512,128]{2,1,0:T(8,128)(2,1)S(1)} %queries.1.refs_0_, bf16[320,512]{1,0:T(8,128)(2,1)S(1)} %collective-permute-done.11.refs_1_, bf16[256,512]{1,0:T(8,128)(2,1)S(1)} %collective-permute-done.12.refs_2_, f32[8]{0:T(128)S(1)} %copy-done.4, f32[8,80,512]{2,1,0:T(8,128)S(1)} %attention.10.refs_4_), custom_call_target="tpu_custom_call" | custom-call | flops 2415919104 | bytes 2097152 | tf_op jit(solution)/shard_map/attention/pallas_call | solution.py:307
  53.5 0.0 collective-permute-done.9.refs_1_
  53.5 0.0 collective-permute-done.10.refs_2_
  53.6 1.5 %collective-permute-start.14 = (bf16[320,512]{1,0:T(8,128)(2,1)S(1)}, bf16[320,512]{1,0:T(8,128)(2,1)S(1)}, u32[]{:S(2)}, u32[]{:S(2)}) collective-permute-start(bf16[320,512]{1,0:T(8,128)(2,1)S(1)} %collective-permute-done.10.refs_2_), channel_id=1, source_target_pairs={{8,0},{16,8},{24,16},{28,24},{20,28},{12,20},{4,12},{0,4},{9,1},{1... | collective-permute-start | bytes 983048 | tf_op jit(solution)/shard_map/ppermute | solution.py:444
  55.1 0.5 collective-permute-start.13
  55.6 4.2 %attention.12.refs_4_ = f32[8,80,512]{2,1,0:T(8,128)S(1)} custom-call(bf16[8,512,128]{2,1,0:T(8,128)(2,1)S(1)} %queries.1.refs_0_, bf16[256,512]{1,0:T(8,128)(2,1)S(1)} %collective-permute-done.9.refs_1_, bf16[320,512]{1,0:T(8,128)(2,1)S(1)} %collective-permute-done.10.refs_2_, f32[8]{0:T(128)S(1)} %copy-done.4, f32[8,80,512]{2,1,0:T(8,128)S(1)} %attention.11.refs_4_), custom_call_target="tpu_custom_call" | custom-call | flops 2415919104 | bytes 2097152 | tf_op jit(solution)/shard_map/attention/pallas_call | solution.py:307
  59.9 1.6 %collective-permute-start.19 = (bf16[320,512]{1,0:T(8,128)(2,1)S(1)}, bf16[320,512]{1,0:T(8,128)(2,1)S(1)}, u32[]{:S(2)}, u32[]{:S(2)}) collective-permute-start(bf16[320,512]{1,0:T(8,128)(2,1)S(1)} %collective-permute-done.15.refs_1_), channel_id=1, source_target_pairs={{0,8},{8,16},{16,24},{24,28},{28,20},{20,12},{12,4},{4,0},{1,9},{9... | collective-permute-start | bytes 983048 | tf_op jit(solution)/shard_map/ppermute | solution.py:444
  61.5 0.5 collective-permute-start.20
  62.0 4.2 %attention.13.refs_4_ = f32[8,80,512]{2,1,0:T(8,128)S(1)} custom-call(bf16[8,512,128]{2,1,0:T(8,128)(2,1)S(1)} %queries.1.refs_0_, bf16[320,512]{1,0:T(8,128)(2,1)S(1)} %collective-permute-done.15.refs_1_, bf16[256,512]{1,0:T(8,128)(2,1)S(1)} %collective-permute-done.16.refs_2_, f32[8]{0:T(128)S(1)} %copy-done.4, f32[8,80,512]{2,1,0:T(8,128)S(1)} %attention.12.refs_4_), custom_call_target="tpu_custom_call" | custom-call | flops 2415919104 | bytes 2097152 | tf_op jit(solution)/shard_map/attention/pallas_call | solution.py:307
  66.2 0.0 collective-permute-done.13.refs_1_
  66.2 0.0 collective-permute-done.14.refs_2_
  66.2 1.5 %collective-permute-start.18 = (bf16[320,512]{1,0:T(8,128)(2,1)S(1)}, bf16[320,512]{1,0:T(8,128)(2,1)S(1)}, u32[]{:S(2)}, u32[]{:S(2)}) collective-permute-start(bf16[320,512]{1,0:T(8,128)(2,1)S(1)} %collective-permute-done.14.refs_2_), channel_id=1, source_target_pairs={{8,0},{16,8},{24,16},{28,24},{20,28},{12,20},{4,12},{0,4},{9,1},{1... | collective-permute-start | bytes 983048 | tf_op jit(solution)/shard_map/ppermute | solution.py:444
  67.7 0.5 collective-permute-start.17
  68.3 4.2 %attention.14.refs_4_ = f32[8,80,512]{2,1,0:T(8,128)S(1)} custom-call(bf16[8,512,128]{2,1,0:T(8,128)(2,1)S(1)} %queries.1.refs_0_, bf16[256,512]{1,0:T(8,128)(2,1)S(1)} %collective-permute-done.13.refs_1_, bf16[320,512]{1,0:T(8,128)(2,1)S(1)} %collective-permute-done.14.refs_2_, f32[8]{0:T(128)S(1)} %copy-done.4, f32[8,80,512]{2,1,0:T(8,128)S(1)} %attention.13.refs_4_), custom_call_target="tpu_custom_call" | custom-call | flops 2415919104 | bytes 2097152 | tf_op jit(solution)/shard_map/attention/pallas_call | solution.py:307
  72.5 0.0 collective-permute-done.20.refs_2_
  72.5 0.1 collective-permute-start.26
  72.6 0.0 collective-permute-done.19.refs_1_
  72.6 4.2 %attention.15.refs_4_ = f32[8,80,512]{2,1,0:T(8,128)S(1)} custom-call(bf16[8,512,128]{2,1,0:T(8,128)(2,1)S(1)} %queries.1.refs_0_, bf16[320,512]{1,0:T(8,128)(2,1)S(1)} %collective-permute-done.19.refs_1_, bf16[256,512]{1,0:T(8,128)(2,1)S(1)} %collective-permute-done.20.refs_2_, f32[8]{0:T(128)S(1)} %copy-done.4, f32[8,80,512]{2,1,0:T(8,128)S(1)} %attention.14.refs_4_), custom_call_target="tpu_custom_call" | custom-call | flops 2415919104 | bytes 2097152 | tf_op jit(solution)/shard_map/attention/pallas_call | solution.py:307
  76.9 0.0 collective-permute-done.17.refs_1_
  76.9 0.2 collective-permute-done.18.refs_2_
  77.1 2.6 %attention.16 = (bf16[128,512]{1,0:T(8,128)(2,1)S(1)}, bf16[128,512]{1,0:T(8,128)(2,1)S(1)}) custom-call(bf16[8,512,128]{2,1,0:T(8,128)(2,1)S(1)} %queries.1.refs_0_, bf16[256,512]{1,0:T(8,128)(2,1)S(1)} %collective-permute-done.17.refs_1_, bf16[320,512]{1,0:T(8,128)(2,1)S(1)} %collective-permute-done.18.refs_2_, f32[8]{0:T(128)S(1)} %copy-done.4, ...), custom_call_target="tpu_custom_call" | custom-call | flops 2415919104 | bytes 2097152 | tf_op jit(solution)/shard_map/attention/pallas_call | solution.py:307
  79.6 0.0 collective-permute-done.23.refs_2_
  79.6 0.3 collective-permute-start.24
  80.0 2.6 %attention.17 = (bf16[128,512]{1,0:T(8,128)(2,1)S(1)}, bf16[128,512]{1,0:T(8,128)(2,1)S(1)}) custom-call(bf16[8,512,128]{2,1,0:T(8,128)(2,1)S(1)} %queries.1.refs_0_, bf16[256,512]{1,0:T(8,128)(2,1)S(1)} %collective-permute-done.17.refs_1_, bf16[320,512]{1,0:T(8,128)(2,1)S(1)} %collective-permute-done.18.refs_2_, f32[8]{0:T(128)S(1)} %copy-done.4, ...), custom_call_target="tpu_custom_call" | custom-call | flops 2415919104 | bytes 2097152 | tf_op jit(solution)/shard_map/attention/pallas_call | solution.py:307
  82.6 0.3 collective-permute-start.25
  82.8 0.5 collective-permute-start.21
  83.3 1.1 %collective-permute-start.22 = (bf16[128,512]{1,0:T(8,128)(2,1)S(1)}, bf16[128,512]{1,0:T(8,128)(2,1)S(1)}, u32[]{:S(2)}, u32[]{:S(2)}) collective-permute-start(bf16[128,512]{1,0:T(8,128)(2,1)S(1)} %get-tuple-element.83), channel_id=1, source_target_pairs={{0,3},{1,2},{2,1},{3,0},{4,7},{5,6},{6,5},{7,4},{8,11},{9,10},{10,... | collective-permute-start | bytes 393224 | tf_op jit(solution)/shard_map/ppermute | solution.py:35
  84.5 0.7 output.2.refs_4_
  85.2 4.0 %collective-permute-done.21.refs_0_ = bf16[128,512]{1,0:T(8,128)(2,1)S(1)} collective-permute-done((bf16[128,512]{1,0:T(8,128)(2,1)S(1)}, bf16[128,512]{1,0:T(8,128)(2,1)S(1)}, u32[]{:S(2)}, u32[]{:S(2)}) %collective-permute-start.21) | collective-permute-done | bytes 131104 | tf_op jit(solution)/shard_map/ppermute | solution.py:35
  89.2 1.4 %collective-permute-done.22.refs_1_ = bf16[128,512]{1,0:T(8,128)(2,1)S(1)} collective-permute-done((bf16[128,512]{1,0:T(8,128)(2,1)S(1)}, bf16[128,512]{1,0:T(8,128)(2,1)S(1)}, u32[]{:S(2)}, u32[]{:S(2)}) %collective-permute-start.22) | collective-permute-done | bytes 131104 | tf_op jit(solution)/shard_map/ppermute | solution.py:35
  90.6 0.0 collective-permute-done.24.refs_3_
  90.7 1.6 %output.3 = bf16[128,2048]{1,0:T(8,128)(2,1)} custom-call(bf16[128,512]{1,0:T(8,128)(2,1)S(1)} %collective-permute-done.21.refs_0_, bf16[128,512]{1,0:T(8,128)(2,1)S(1)} %collective-permute-done.22.refs_1_, bf16[512,2048]{1,0:T(8,128)(2,1)S(1)} %collective-permute-done.23.refs_2_, bf16[512,2048]{1,0:T(8,128)(2,1)S(1)} %collective-permute-done.24.refs_3_, ...), custom_call_target="tpu_custom_call" | custom-call | flops 536870912 | bytes 4194304 | tf_op jit(solution)/shard_map/output/pallas_call | solution.py:348
  (29 shorter events, 0.1 us)
Async XLA Ops:
  0.0 14.8 %copy-start.5 = (bf16[2048,256]{1,0:T(8,128)(2,1)S(1)}, bf16[2048,256]{1,0:T(8,128)(2,1)}, u32[]{:S(2)}) copy-start(bf16[2048,256]{1,0:T(8,128)(2,1)} %param.25) | copy-start | bytes 3145732
  2.1 9.0 %collective-permute-start.1 = (f32[8,512]{1,0:T(8,128)}, f32[8,512]{1,0:T(8,128)S(1)}, u32[]{:S(2)}, u32[]{:S(2)}) collective-permute-start(f32[8,512]{1,0:T(8,128)} %modulation.1), channel_id=1, source_target_pairs={{0,4},{4,0},{8,12},{12,8},{16,20},{20,16},{24,28},{28,24},{1,5},{5... | collective-permute-start | bytes 49160 | tf_op jit(solution)/shard_map/ppermute | solution.py:35
  5.0 6.0 %collective-permute-start.2 = (f32[8,512]{1,0:T(8,128)}, f32[8,512]{1,0:T(8,128)S(1)}, u32[]{:S(2)}, u32[]{:S(2)}) collective-permute-start(f32[8,512]{1,0:T(8,128)} %modulation.1), channel_id=1, source_target_pairs={{0,8},{4,12},{8,0},{12,4},{16,24},{20,28},{24,16},{28,20},{1,9},{5... | collective-permute-start | bytes 49160 | tf_op jit(solution)/shard_map/ppermute | solution.py:35
  6.6 4.8 %collective-permute-start.3 = (f32[8,512]{1,0:T(8,128)}, f32[8,512]{1,0:T(8,128)S(1)}, u32[]{:S(2)}, u32[]{:S(2)}) collective-permute-start(f32[8,512]{1,0:T(8,128)} %modulation.1), channel_id=1, source_target_pairs={{0,12},{4,8},{8,4},{12,0},{16,28},{20,24},{24,20},{28,16},{1,13},{... | collective-permute-start | bytes 49160 | tf_op jit(solution)/shard_map/ppermute | solution.py:35
  6.6 13.3 %collective-permute-start.5 = (bf16[128,2048]{1,0:T(8,128)(2,1)}, bf16[128,2048]{1,0:T(8,128)(2,1)S(1)}, u32[]{:S(2)}, u32[]{:S(2)}) collective-permute-start(bf16[128,2048]{1,0:T(8,128)(2,1)} %refs_5_.1), channel_id=1, source_target_pairs={{0,2},{1,3},{2,0},{3,1},{4,6},{5,7},{6,4},{7,5},{8,10},{9,11},{10,... | collective-permute-start | bytes 1572872 | tf_op jit(solution)/shard_map/ppermute | solution.py:35
  8.5 16.7 %collective-permute-start = (bf16[128,2048]{1,0:T(8,128)(2,1)}, bf16[128,2048]{1,0:T(8,128)(2,1)S(1)}, u32[]{:S(2)}, u32[]{:S(2)}) collective-permute-start(bf16[128,2048]{1,0:T(8,128)(2,1)} %refs_5_.1), channel_id=1, source_target_pairs={{0,1},{1,0},{2,3},{3,2},{4,5},{5,4},{6,7},{7,6},{8,9},{9,8},{10,11... | collective-permute-start | bytes 1572872 | tf_op jit(solution)/shard_map/ppermute | solution.py:35
  12.2 13.1 %copy-start.2 = (bf16[128,2048]{1,0:T(8,128)(2,1)S(1)}, bf16[128,2048]{1,0:T(8,128)(2,1)}, u32[]{:S(2)}) copy-start(bf16[128,2048]{1,0:T(8,128)(2,1)} %refs_5_.1) | copy-start | bytes 1572868
  12.2 13.1 %copy-start.3 = (bf16[64,2048]{1,0:T(8,128)(2,1)S(1)}, bf16[64,2048]{1,0:T(8,128)(2,1)}, u32[]{:S(2)}) copy-start(bf16[64,2048]{1,0:T(8,128)(2,1)} %refs_4_.1) | copy-start | bytes 786436
  12.2 4.7 %collective-permute-start.4 = (f32[8,512]{1,0:T(8,128)S(1)}, f32[8,512]{1,0:T(8,128)S(1)}, u32[]{:S(2)}, u32[]{:S(2)}) collective-permute-start(f32[8,512]{1,0:T(8,128)S(1)} %add_add_fusion), channel_id=1, source_target_pairs={{0,16},{4,20},{8,24},{12,28},{16,0},{20,4},{24,8},{28,12},{1,17},{... | collective-permute-start | bytes 49160 | tf_op jit(solution)/shard_map/ppermute | solution.py:35
  19.9 5.4 %collective-permute-start.6 = (bf16[128,2048]{1,0:T(8,128)(2,1)S(1)}, bf16[128,2048]{1,0:T(8,128)(2,1)S(1)}, u32[]{:S(2)}, u32[]{:S(2)}) collective-permute-start(bf16[128,2048]{1,0:T(8,128)(2,1)S(1)} %collective-permute-done.5.refs_2_), channel_id=1, source_target_pairs={{0,1},{1,0},{2,3},{3,2},{4,5},{5,4},{6,7},{7,6},{8,9},{9,8},{10,11... | collective-permute-start | bytes 1572872 | tf_op jit(solution)/shard_map/ppermute | solution.py:35
  25.3 2.6 %copy-start.1 = (bf16[512,2048]{1,0:T(8,128)(2,1)S(1)}, bf16[512,2048]{1,0:T(8,128)(2,1)}, u32[]{:S(2)}) copy-start(bf16[512,2048]{1,0:T(8,128)(2,1)} %refs_2_) | copy-start | bytes 6291460
  25.3 8.3 %copy-start = (bf16[2048,512]{1,0:T(8,128)(2,1)S(1)}, bf16[2048,512]{1,0:T(8,128)(2,1)}, u32[]{:S(2)}) copy-start(bf16[2048,512]{1,0:T(8,128)(2,1)} %weight.1) | copy-start | bytes 6291460
  27.9 51.8 %collective-permute-start.23 = (bf16[512,2048]{1,0:T(8,128)(2,1)S(1)}, bf16[512,2048]{1,0:T(8,128)(2,1)S(1)}, u32[]{:S(2)}, u32[]{:S(2)}) collective-permute-start(bf16[512,2048]{1,0:T(8,128)(2,1)S(1)} %copy-done.1), channel_id=1, source_target_pairs={{0,2},{1,3},{2,0},{3,1},{4,6},{5,7},{6,4},{7,5},{8,10},{9,11},{10,... | collective-permute-start | bytes 6291464 | tf_op jit(solution)/shard_map/ppermute | solution.py:35
  29.5 11.4 %collective-permute-start.8 = (bf16[320,512]{1,0:T(8,128)(2,1)S(1)}, bf16[320,512]{1,0:T(8,128)(2,1)S(1)}, u32[]{:S(2)}, u32[]{:S(2)}) collective-permute-start(bf16[320,512]{1,0:T(8,128)(2,1)S(1)} %get-tuple-element.60.refs_2_), channel_id=1, source_target_pairs={{8,0},{16,8},{24,16},{28,24},{20,28},{12,20},{4,12},{0,4},{9,1},{1... | collective-permute-start | bytes 983048 | tf_op jit(solution)/shard_map/ppermute | solution.py:444
  31.0 9.9 %collective-permute-start.7 = (bf16[256,512]{1,0:T(8,128)(2,1)S(1)}, bf16[256,512]{1,0:T(8,128)(2,1)S(1)}, u32[]{:S(2)}, u32[]{:S(2)}) collective-permute-start(bf16[256,512]{1,0:T(8,128)(2,1)S(1)} %get-tuple-element.59.refs_1_), channel_id=1, source_target_pairs={{0,8},{8,16},{16,24},{24,28},{28,20},{20,12},{12,4},{4,0},{1,9},{9... | collective-permute-start | bytes 786440 | tf_op jit(solution)/shard_map/ppermute | solution.py:444
  31.5 15.7 %collective-permute-start.11 = (bf16[320,512]{1,0:T(8,128)(2,1)S(1)}, bf16[320,512]{1,0:T(8,128)(2,1)S(1)}, u32[]{:S(2)}, u32[]{:S(2)}) collective-permute-start(bf16[320,512]{1,0:T(8,128)(2,1)S(1)} %get-tuple-element.60.refs_2_), channel_id=1, source_target_pairs={{0,8},{8,16},{16,24},{24,28},{28,20},{20,12},{12,4},{4,0},{1,9},{9... | collective-permute-start | bytes 983048 | tf_op jit(solution)/shard_map/ppermute | solution.py:444
  33.1 14.1 %collective-permute-start.12 = (bf16[256,512]{1,0:T(8,128)(2,1)S(1)}, bf16[256,512]{1,0:T(8,128)(2,1)S(1)}, u32[]{:S(2)}, u32[]{:S(2)}) collective-permute-start(bf16[256,512]{1,0:T(8,128)(2,1)S(1)} %get-tuple-element.59.refs_1_), channel_id=1, source_target_pairs={{8,0},{16,8},{24,16},{28,24},{20,28},{12,20},{4,12},{0,4},{9,1},{1... | collective-permute-start | bytes 786440 | tf_op jit(solution)/shard_map/ppermute | solution.py:444
  33.5 3.3 %copy-start.4 = (f32[8]{0:T(128)S(1)}, f32[8]{0:T(128)}, u32[]{:S(2)}) copy-start(f32[8]{0:T(128)} %refs_3_.17) | copy-start | bytes 100
  40.9 12.6 %collective-permute-start.10 = (bf16[320,512]{1,0:T(8,128)(2,1)S(1)}, bf16[320,512]{1,0:T(8,128)(2,1)S(1)}, u32[]{:S(2)}, u32[]{:S(2)}) collective-permute-start(bf16[320,512]{1,0:T(8,128)(2,1)S(1)} %collective-permute-done.8.refs_2_), channel_id=1, source_target_pairs={{8,0},{16,8},{24,16},{28,24},{20,28},{12,20},{4,12},{0,4},{9,1},{1... | collective-permute-start | bytes 983048 | tf_op jit(solution)/shard_map/ppermute | solution.py:444
  42.4 11.1 %collective-permute-start.9 = (bf16[256,512]{1,0:T(8,128)(2,1)S(1)}, bf16[256,512]{1,0:T(8,128)(2,1)S(1)}, u32[]{:S(2)}, u32[]{:S(2)}) collective-permute-start(bf16[256,512]{1,0:T(8,128)(2,1)S(1)} %collective-permute-done.7.refs_1_), channel_id=1, source_target_pairs={{0,8},{8,16},{16,24},{24,28},{28,20},{20,12},{12,4},{4,0},{1,9},{9... | collective-permute-start | bytes 786440 | tf_op jit(solution)/shard_map/ppermute | solution.py:444
  47.2 12.6 %collective-permute-start.15 = (bf16[320,512]{1,0:T(8,128)(2,1)S(1)}, bf16[320,512]{1,0:T(8,128)(2,1)S(1)}, u32[]{:S(2)}, u32[]{:S(2)}) collective-permute-start(bf16[320,512]{1,0:T(8,128)(2,1)S(1)} %collective-permute-done.11.refs_1_), channel_id=1, source_target_pairs={{0,8},{8,16},{16,24},{24,28},{28,20},{20,12},{12,4},{4,0},{1,9},{9... | collective-permute-start | bytes 983048 | tf_op jit(solution)/shard_map/ppermute | solution.py:444
  48.9 11.0 %collective-permute-start.16 = (bf16[256,512]{1,0:T(8,128)(2,1)S(1)}, bf16[256,512]{1,0:T(8,128)(2,1)S(1)}, u32[]{:S(2)}, u32[]{:S(2)}) collective-permute-start(bf16[256,512]{1,0:T(8,128)(2,1)S(1)} %collective-permute-done.12.refs_2_), channel_id=1, source_target_pairs={{8,0},{16,8},{24,16},{28,24},{20,28},{12,20},{4,12},{0,4},{9,1},{1... | collective-permute-start | bytes 786440 | tf_op jit(solution)/shard_map/ppermute | solution.py:444
  53.6 12.6 %collective-permute-start.14 = (bf16[320,512]{1,0:T(8,128)(2,1)S(1)}, bf16[320,512]{1,0:T(8,128)(2,1)S(1)}, u32[]{:S(2)}, u32[]{:S(2)}) collective-permute-start(bf16[320,512]{1,0:T(8,128)(2,1)S(1)} %collective-permute-done.10.refs_2_), channel_id=1, source_target_pairs={{8,0},{16,8},{24,16},{28,24},{20,28},{12,20},{4,12},{0,4},{9,1},{1... | collective-permute-start | bytes 983048 | tf_op jit(solution)/shard_map/ppermute | solution.py:444
  55.1 11.1 %collective-permute-start.13 = (bf16[256,512]{1,0:T(8,128)(2,1)S(1)}, bf16[256,512]{1,0:T(8,128)(2,1)S(1)}, u32[]{:S(2)}, u32[]{:S(2)}) collective-permute-start(bf16[256,512]{1,0:T(8,128)(2,1)S(1)} %collective-permute-done.9.refs_1_), channel_id=1, source_target_pairs={{0,8},{8,16},{16,24},{24,28},{28,20},{20,12},{12,4},{4,0},{1,9},{9... | collective-permute-start | bytes 786440 | tf_op jit(solution)/shard_map/ppermute | solution.py:444
  59.9 12.7 %collective-permute-start.19 = (bf16[320,512]{1,0:T(8,128)(2,1)S(1)}, bf16[320,512]{1,0:T(8,128)(2,1)S(1)}, u32[]{:S(2)}, u32[]{:S(2)}) collective-permute-start(bf16[320,512]{1,0:T(8,128)(2,1)S(1)} %collective-permute-done.15.refs_1_), channel_id=1, source_target_pairs={{0,8},{8,16},{16,24},{24,28},{28,20},{20,12},{12,4},{4,0},{1,9},{9... | collective-permute-start | bytes 983048 | tf_op jit(solution)/shard_map/ppermute | solution.py:444
  61.5 11.0 %collective-permute-start.20 = (bf16[256,512]{1,0:T(8,128)(2,1)S(1)}, bf16[256,512]{1,0:T(8,128)(2,1)S(1)}, u32[]{:S(2)}, u32[]{:S(2)}) collective-permute-start(bf16[256,512]{1,0:T(8,128)(2,1)S(1)} %collective-permute-done.16.refs_2_), channel_id=1, source_target_pairs={{8,0},{16,8},{24,16},{28,24},{20,28},{12,20},{4,12},{0,4},{9,1},{1... | collective-permute-start | bytes 786440 | tf_op jit(solution)/shard_map/ppermute | solution.py:444
  66.2 10.9 %collective-permute-start.18 = (bf16[320,512]{1,0:T(8,128)(2,1)S(1)}, bf16[320,512]{1,0:T(8,128)(2,1)S(1)}, u32[]{:S(2)}, u32[]{:S(2)}) collective-permute-start(bf16[320,512]{1,0:T(8,128)(2,1)S(1)} %collective-permute-done.14.refs_2_), channel_id=1, source_target_pairs={{8,0},{16,8},{24,16},{28,24},{20,28},{12,20},{4,12},{0,4},{9,1},{1... | collective-permute-start | bytes 983048 | tf_op jit(solution)/shard_map/ppermute | solution.py:444
  67.7 9.1 %collective-permute-start.17 = (bf16[256,512]{1,0:T(8,128)(2,1)S(1)}, bf16[256,512]{1,0:T(8,128)(2,1)S(1)}, u32[]{:S(2)}, u32[]{:S(2)}) collective-permute-start(bf16[256,512]{1,0:T(8,128)(2,1)S(1)} %collective-permute-done.13.refs_1_), channel_id=1, source_target_pairs={{0,8},{8,16},{16,24},{24,28},{28,20},{20,12},{12,4},{4,0},{1,9},{9... | collective-permute-start | bytes 786440 | tf_op jit(solution)/shard_map/ppermute | solution.py:444
  72.5 11.9 %collective-permute-start.26 = (bf16[512,2048]{1,0:T(8,128)(2,1)S(1)}, bf16[512,2048]{1,0:T(8,128)(2,1)S(1)}, u32[]{:S(2)}, u32[]{:S(2)}) collective-permute-start(bf16[512,2048]{1,0:T(8,128)(2,1)S(1)} %copy-done.1), channel_id=1, source_target_pairs={{0,1},{1,0},{2,3},{3,2},{4,5},{5,4},{6,7},{7,6},{8,9},{9,8},{10,11... | collective-permute-start | bytes 6291464 | tf_op jit(solution)/shard_map/ppermute | solution.py:35
  79.6 11.0 %collective-permute-start.24 = (bf16[512,2048]{1,0:T(8,128)(2,1)S(1)}, bf16[512,2048]{1,0:T(8,128)(2,1)S(1)}, u32[]{:S(2)}, u32[]{:S(2)}) collective-permute-start(bf16[512,2048]{1,0:T(8,128)(2,1)S(1)} %collective-permute-done.23.refs_2_), channel_id=1, source_target_pairs={{0,1},{1,0},{2,3},{3,2},{4,5},{5,4},{6,7},{7,6},{8,9},{9,8},{10,11... | collective-permute-start | bytes 6291464 | tf_op jit(solution)/shard_map/ppermute | solution.py:35
  82.6 1.9 %collective-permute-start.25 = (bf16[128,512]{1,0:T(8,128)(2,1)S(1)}, bf16[128,512]{1,0:T(8,128)(2,1)S(1)}, u32[]{:S(2)}, u32[]{:S(2)}) collective-permute-start(bf16[128,512]{1,0:T(8,128)(2,1)S(1)} %get-tuple-element.88), channel_id=1, source_target_pairs={{0,1},{1,0},{2,3},{3,2},{4,5},{5,4},{6,7},{7,6},{8,9},{9,8},{10,11... | collective-permute-start | bytes 393224 | tf_op jit(solution)/shard_map/ppermute | solution.py:35
  82.8 6.4 %collective-permute-start.21 = (bf16[128,512]{1,0:T(8,128)(2,1)S(1)}, bf16[128,512]{1,0:T(8,128)(2,1)S(1)}, u32[]{:S(2)}, u32[]{:S(2)}) collective-permute-start(bf16[128,512]{1,0:T(8,128)(2,1)S(1)} %get-tuple-element.82), channel_id=1, source_target_pairs={{0,2},{1,3},{2,0},{3,1},{4,6},{5,7},{6,4},{7,5},{8,10},{9,11},{10,... | collective-permute-start | bytes 393224 | tf_op jit(solution)/shard_map/ppermute | solution.py:35
  83.3 7.3 %collective-permute-start.22 = (bf16[128,512]{1,0:T(8,128)(2,1)S(1)}, bf16[128,512]{1,0:T(8,128)(2,1)S(1)}, u32[]{:S(2)}, u32[]{:S(2)}) collective-permute-start(bf16[128,512]{1,0:T(8,128)(2,1)S(1)} %get-tuple-element.83), channel_id=1, source_target_pairs={{0,3},{1,2},{2,1},{3,0},{4,7},{5,6},{6,5},{7,4},{8,11},{9,10},{10,... | collective-permute-start | bytes 393224 | tf_op jit(solution)/shard_map/ppermute | solution.py:35

commit v2 on v1

--- a/solution.py
+++ b/solution.py
@@ -108,7 +108,8 @@
     pieces = refs[:count]
     context, mod, gains, weight, cos, sin_e, sin_o = refs[count : count + 7]
     hidden, first, second = refs[count + 7 :]
-    half = first.shape[0]
+    extra = context.shape[0] // 2
+    half = first.shape[0] - extra
     norm_gain = gains[:, : context.shape[1]]
     key_gain = gains[:, context.shape[1] : context.shape[1] + HEAD]
     parts = mod.shape[0] // 8
@@ -131,21 +132,23 @@
     heads = finish_heads(keys, key_gain, tables)
     for k, key in enumerate(heads):
         tile = jnp.concatenate([key, values[:, k * HEAD : (k + 1) * HEAD]], axis=1).astype(BF16)
-        first[:, k * TILE : (k + 1) * TILE] = tile[:half]
-        second[:, k * TILE : (k + 1) * TILE] = tile[half:]
+        lanes = slice(k * TILE, (k + 1) * TILE)
+        first[:half, lanes] = tile[:half]
+        first[half:, lanes] = tile[2 * half : 2 * half + extra]
+        second[:half, lanes] = tile[half : 2 * half]
+        second[half:, lanes] = tile[2 * half + extra :]
 
 
 def keys_values(pieces, context, mod, gains, weight, tables):
     rows = sum(p.shape[0] for p in pieces) + context.shape[0]
     depth = context.shape[1]
     width = weight.shape[1] // 2
-    half = (rows - context.shape[0]) // 2
     return pl.pallas_call(
         functools.partial(kv_kernel, len(pieces)),
         out_shape=(
             jax.ShapeDtypeStruct((rows, depth), BF16),
-            jax.ShapeDtypeStruct((half, 2 * width), BF16),
-            jax.ShapeDtypeStruct((rows - half, 2 * width), BF16),
+            jax.ShapeDtypeStruct((rows // 2, 2 * width), BF16),
+            jax.ShapeDtypeStruct((rows // 2, 2 * width), BF16),
         ),
         in_specs=[IN_VMEM] * (len(pieces) + 7),
         out_specs=(IN_VMEM, IN_VMEM, IN_VMEM),
@@ -158,14 +161,11 @@
 def query_kernel(hidden, weight, gains, cos, sin_e, sin_o, out):
     rows = out.shape[1]
     tables = (cos[0:rows, :], sin_e[0:rows, :], sin_o[0:rows, :])
-    width = weight.shape[1]
     gain = gains[:, hidden.shape[1] + HEAD :]
-    step = min(width, 2 * TILE)
-    for start in range(0, width, step):
-        x = dot(hidden[0:rows, :], weight[:, start : start + step])
-        for i, head in enumerate(finish_heads(x, gain, tables)):
-            head = (head * (HEAD**-0.5)).astype(BF16)
-            out[start // HEAD + i] = jnp.concatenate([head, jnp.zeros_like(head)], axis=1)
+    x = dot(hidden[0:rows, :], weight[...])
+    for i, head in enumerate(finish_heads(x, gain, tables)):
+        head = (head * (HEAD**-0.5)).astype(BF16)
+        out[i] = jnp.concatenate([head, jnp.zeros_like(head)], axis=1)
 
 
 def queries_of(hidden, weight, gains, tables, rows):
@@ -223,15 +223,14 @@
                 tile(ref, span, k), q, NT, preferred_element_type=F32
             )
 
-    def both(k, value):
-        return jnp.concatenate(
-            [jnp.full((1, chunk), value[k * group + g], F32) for g in range(group)], axis=1
-        )
+    def raises(k):
+        heads = [lift[k * group + g, 0:1, :] for g in range(group)]
+        return jnp.concatenate([h for h in heads for _ in range(chunk // TILE)], axis=1)
 
     def absorb(k, r, slot):
         parts = [(st, held[slot][st : st + n, :]) for st, n in plain]
         if raised:
-            extra = both(k, lift)
+            extra = raises(k)
             parts += [(st, held[slot][st : st + n, :] + extra) for st, n in raised]
         top = functools.reduce(
             jnp.maximum, [jnp.max(x, axis=0, keepdims=True) for _, x in parts]
@@ -295,7 +294,7 @@
     args = [queries] + [b[0] for b in blocks]
     in_specs = [IN_VMEM] * len(args)
     if lifted:
-        in_specs.append(pl.BlockSpec(memory_space=pltpu.SMEM))
+        in_specs.append(IN_VMEM)
         args.append(lift)
     if state is not None:
         in_specs.append(IN_VMEM)
@@ -326,8 +325,10 @@
 def output_kernel(count, *refs):
     attended = refs[:count]
     weights = refs[count : 2 * count]
-    rest, out = refs[2 * count : -1], refs[-1]
+    rest = refs[2 * count : -3] if len(refs) > 2 * count + 1 else ()
+    out = refs[-3] if rest else refs[-1]
     step = min(out.shape[1], 4 * TILE)
+    copies = []
     for i in range(0, out.shape[1], step):
         total = None
         for a, w in zip(attended, weights):
@@ -338,7 +339,16 @@
             gate = [mod[8 * t + 2 : 8 * t + 3, :] for t in range(mod.shape[0] // 8)]
             gate = jnp.concatenate(gate, axis=1)[:, i : i + step]
             total = latent[:, i : i + step].astype(F32) + gate * (begun[:, i : i + step] + total)
-        out[:, i : i + step] = total.astype(out.dtype)
+            made, sems = refs[-2:]
+            made[:, i : i + step] = total.astype(out.dtype)
+            lanes = pl.ds(i, step)
+            copy = pltpu.make_async_copy(made.at[:, lanes], out.at[:, lanes], sems.at[i // step])
+            copy.start()
+            copies.append(copy)
+        else:
+            out[:, i : i + step] = total
+    for copy in copies:
+        copy.wait()
 
 
 def project(attended, weights, begun, latent, mod, depth):
@@ -348,8 +358,14 @@
     return pl.pallas_call(
         functools.partial(output_kernel, count),
         in_specs=[IN_VMEM] * (2 * count + len(rest)),
-        out_specs=IN_VMEM,
+        out_specs=pl.BlockSpec(memory_space=pltpu.HBM) if rest else IN_VMEM,
         out_shape=jax.ShapeDtypeStruct((rows, depth), BF16 if rest else F32),
+        scratch_shapes=[
+            pltpu.VMEM((rows, depth), BF16),
+            pltpu.SemaphoreType.DMA((pl.cdiv(depth, 4 * TILE),)),
+        ]
+        if rest
+        else [],
         compiler_params=pltpu.CompilerParams(vmem_limit_bytes=VMEM_LIMIT),
         cost_estimate=cost(2 * rows * depth * inner * count, 2 * depth * inner * count),
         name="output",
@@ -411,21 +427,26 @@
     gains = [v.reshape(1, -1) for v in (norm_gain, key_gain, query_gain)]
     early = [
         (*rotary_tables(rank, tp, rows, context_rows), jnp.concatenate(gains, axis=1)),
-        (jnp.concatenate([key_weight, value_weight], axis=1),),
+        (
+            jnp.concatenate([key_weight, value_weight], axis=1),
+            jnp.broadcast_to(context_lift[:, None, None], context_lift.shape + (8, TILE)),
+        ),
     ]
     ready = []
     bits = [1 << b for b in range(sp.bit_length() - 1)]
     for i in range(0, len(bits), 2):
         pair = bits[i : i + 2]
         masks = pair + [sum(pair)] if len(pair) == 2 else pair
-        arrived = [swap(partial, "sp", sp, m) for m in masks]
+        arrived = []
+        for m in masks:
+            arrived.append(swap(partial, "sp", sp, m))
         extra = early.pop(0) if early else ()
         tied = tie(*arrived, *extra)
         partial = sum(tied[: len(arrived)], partial)
         ready += tied[len(arrived) :]
     for extra in early:
         ready += extra
-    *tables, gains, kv_weight = ready
+    *tables, gains, kv_weight, lifts = ready
     partial, pieces[tp_bits[0]] = tie(partial, pieces[tp_bits[0]])
     for bit in tp_bits[1:]:
         spread(pieces, bit)
@@ -444,7 +465,7 @@
         return lax.ppermute(pair[0], "sp", ahead), lax.ppermute(pair[1], "sp", back)
 
     def as_blocks(pair):
-        return [(b, 0, half, half if b.shape[0] == half else half + context_rows) for b in pair]
+        return [(b, 0, half, b.shape[0]) for b in pair]
 
     flight = [hop((first, second))]
     flight.append(hop((second, first)))
@@ -455,18 +476,18 @@
     waiting = as_blocks((first, second))
     state = None
     for i in range(sp - 1):
-        state = attention(queries, waiting, context_lift, state, group, 0)
+        state = attention(queries, waiting, lifts, state, group, 0)
         up, down, state = tie(*flight.pop(0), state)
         if i < sp - 3:
             flight.append(hop((up, down)))
         waiting = as_blocks((up, down))
-    far = attention(queries, waiting, context_lift, state, group, tp // 2, (half, length))
+    far = attention(queries, waiting, lifts, state, group, tp // 2, (half, length))
     top_bit = tp_bits[0]
     weights[top_bit], state, *_ = tie(weights[top_bit], state, *far)
     for bit in tp_bits[1:]:
         spread(weights, bit)
     far = [swap(a, "tp", tp, tp // 2 + j) for j, a in enumerate(far)]
-    near = attention(queries, waiting, context_lift, state, group, tp // 2, (0, half))
+    near = attention(queries, waiting, lifts, state, group, tp // 2, (0, half))
     near = near[:1] + [swap(a, "tp", tp, j) for j, a in enumerate(near) if j]
     weights = [weights[j] for j in range(tp)]
     begun = project(near, weights[: tp // 2], None, None, None, latent.shape[1])

time: 92.6 us -> 92 us (level)
  Pallas kernels: 44.8 us -> 38.4 us
  waiting for transfers between devices: 9.74 us -> 15.6 us
    ppermute x7, waiting for transfers between devices: 0.21 us -> 6.02 us  [hop(): lax.ppermute(pair[1], 'sp', back)]
    pallas_call x9, Pallas kernels: 34.5 us -> 29.4 us  [attention(): pl.pallas_call(functools.partial(attention_kernel, spans, lifted, state i...]
    ppermute x7, starting transfers between devices: 7.49 us -> 3.14 us  [hop(): lax.ppermute(pair[1], 'sp', back)]
    ppermute x7, starting transfers between devices: 6.96 us -> 11 us  [hop(): lax.ppermute(pair[0], 'sp', ahead)]
    pallas_call x1, Pallas kernels: 3.25 us -> 2.17 us  [queries_of(): pl.pallas_call(query_kernel, in_specs=[IN_VMEM] * 6, out_specs=IN_VMEM, o...]
  transfers between devices with their start and end apart: 27 -> 27, of which waited for: 6 -> 15; matrix products, arithmetic and copies ran while one was open for 5% -> 5% of each run, Pallas kernels for 42% -> 35%
where the time goes in v2:
time: 92 us; the launch traced here: 91.5 us
  Pallas kernels  38.4 us (42%)
  starting transfers between devices  27.1 us (29%)
  waiting for transfers between devices  15.6 us (17%)
  blocking collectives  5.34 us (6%)
  other arithmetic  3.75 us (4%)
    pallas_call x9, Pallas kernels, attention(): pl.pallas_call(functools.partial(attention_kernel, spans, lifted, state i...  29.4 us
    ppermute x13, starting transfers between devices, swap(): return lax.ppermute(value, axis, [(i, i ^ mask) for i in range(size)])  12.9 us
    ppermute x7, starting transfers between devices, hop(): lax.ppermute(pair[0], 'sp', ahead)  11 us
    ppermute x13, waiting for transfers between devices, swap(): return lax.ppermute(value, axis, [(i, i ^ mask) for i in range(size)])  9.2 us
    ppermute x7, waiting for transfers between devices, hop(): lax.ppermute(pair[1], 'sp', back)  6.02 us
    all_gather x1, blocking collectives, shards(): mod = lax.all_gather(partial, 'tp', axis=0, tiled=True)  5.34 us
    ppermute x7, starting transfers between devices, hop(): lax.ppermute(pair[1], 'sp', back)  3.14 us
    pallas_call x1, Pallas kernels, keys_values(): pl.pallas_call(functools.partial(kv_kernel, len(pieces)), out_shape=(jax....  2.55 us
  transfers between devices with their start and end apart: 27, of which 15 were waited for; matrix products, arithmetic and copies ran while one was open for 5% of the time, Pallas kernels for 35%

profile of v2, /device:TPU:0, one launch (start us, length us, event | category | flops | bytes accessed | tf_op | source)
XLA Modules:
  0.0 91.5 jit_solution(18347181186455226553)
XLA Ops:
  0.0 2.1 %modulation.1 = f32[8,512]{1,0:T(8,128)} custom-call(f32[1,256]{1,0:T(1,128)} %bitcast.6, f32[1,256]{1,0:T(1,128)} %bitcast.7, bf16[256,512]{1,0:T(8,128)(2,1)} %shift.1, bf16[256,512]{1,0:T(8,128)(2,1)} %scale.1, bf16[256,512]{1,0:T(8,128)(2,1)} %gate.1), custom_call_target="tpu_custom_call" | custom-call | flops 6291456 | bytes 786432 | tf_op jit(solution)/shard_map/modulation/pallas_call | solution.py:59
  2.1 3.0 %collective-permute-start.1 = (f32[8,512]{1,0:T(8,128)}, f32[8,512]{1,0:T(8,128)S(1)}, u32[]{:S(2)}, u32[]{:S(2)}) collective-permute-start(f32[8,512]{1,0:T(8,128)} %modulation.1), channel_id=1, source_target_pairs={{0,4},{4,0},{8,12},{12,8},{16,20},{20,16},{24,28},{28,24},{1,5},{5... | collective-permute-start | bytes 49160 | tf_op jit(solution)/shard_map/ppermute | solution.py:35
  5.0 1.6 %collective-permute-start.2 = (f32[8,512]{1,0:T(8,128)}, f32[8,512]{1,0:T(8,128)S(1)}, u32[]{:S(2)}, u32[]{:S(2)}) collective-permute-start(f32[8,512]{1,0:T(8,128)} %modulation.1), channel_id=1, source_target_pairs={{0,8},{4,12},{8,0},{12,4},{16,24},{20,28},{24,16},{28,20},{1,9},{5... | collective-permute-start | bytes 49160 | tf_op jit(solution)/shard_map/ppermute | solution.py:35
  6.6 0.0 collective-permute-start.3
  6.6 1.9 %collective-permute-start.5 = (bf16[128,2048]{1,0:T(8,128)(2,1)}, bf16[128,2048]{1,0:T(8,128)(2,1)S(1)}, u32[]{:S(2)}, u32[]{:S(2)}) collective-permute-start(bf16[128,2048]{1,0:T(8,128)(2,1)} %refs_5_.1), channel_id=1, source_target_pairs={{0,2},{1,3},{2,0},{3,1},{4,6},{5,7},{6,4},{7,5},{8,10},{9,11},{10,... | collective-permute-start | bytes 1572872 | tf_op jit(solution)/shard_map/ppermute | solution.py:35
  8.6 1.6 %fusion.13 = (f32[576,128]{1,0:T(8,128)S(1)}, f32[576,128]{1,0:T(8,128)S(1)}, f32[576,128]{1,0:T(8,128)S(1)}) fusion(s32[128]{0:T(128)S(1)} %get-tuple-element.102, s32[128]{0:T(128)S(1)} %get-tuple-element.104, pred[128]{0:T(512)(128)(4,1)S(1)} %get-tuple-element.100, s32[576]{0:T(1024)S(1)} %get-tuple-element.95, s32[576]{0:T(1024)S(1)} %get-tuple-element.96, ...), kind=kLoop, calls=%fused_computation.31 | loop fusion | flops 4792320 | bytes 897992 | tf_op jit(solution)/shard_map/jit(_where)/select_n | solution.py:387
  10.3 0.8 concatenate.6.refs_6_.gains
  11.1 0.0 collective-permute-done.1
  11.1 0.0 collective-permute-done.2
  11.1 0.4 collective-permute-done.3
  11.4 0.7 add_add_fusion
  12.2 0.0 copy-start.3
  12.2 2.7 %collective-permute-start.4 = (f32[8,512]{1,0:T(8,128)S(1)}, f32[8,512]{1,0:T(8,128)S(1)}, u32[]{:S(2)}, u32[]{:S(2)}) collective-permute-start(f32[8,512]{1,0:T(8,128)S(1)} %add_add_fusion), channel_id=1, source_target_pairs={{0,16},{4,20},{8,24},{12,28},{16,0},{20,4},{24,8},{28,12},{1,17},{... | collective-permute-start | bytes 49160 | tf_op jit(solution)/shard_map/ppermute | solution.py:35
  14.9 1.4 %pad_maximum_fusion.refs_7_ = bf16[2048,512]{1,0:T(8,128)(2,1)S(1)} fusion(bf16[2048,256]{1,0:T(8,128)(2,1)S(1)} %copy-done.4, bf16[2048,256]{1,0:T(8,128)(2,1)} %param.24), kind=kLoop, calls=%fused_computation | loop fusion | flops 4194304 | bytes 4194304 | tf_op jit(solution)/shard_map/concatenate | solution.py:431
  16.2 0.7 collective-permute-done.4
  16.9 0.1 broadcast_in_dim.14.refs_3_
  17.0 2.9 %collective-permute-done.5.refs_2_ = bf16[128,2048]{1,0:T(8,128)(2,1)S(1)} collective-permute-done((bf16[128,2048]{1,0:T(8,128)(2,1)}, bf16[128,2048]{1,0:T(8,128)(2,1)S(1)}, u32[]{:S(2)}, u32[]{:S(2)}) %collective-permute-start.5) | collective-permute-done | bytes 524320 | tf_op jit(solution)/shard_map/ppermute | solution.py:35
  19.9 5.3 %all_gather.3.refs_5_.refs_6_ = f32[32,512]{1,0:T(8,128)S(1)} all-gather(f32[8,512]{1,0:T(8,128)S(1)} %add.75), channel_id=1, replica_groups=mesh['sp'=8,'tp'=4] {'tp'}, dimensions={0}, use_global_device_ids=true | all-gather | bytes 81920 | tf_op jit(solution)/shard_map/all_gather | solution.py:453
  25.3 0.0 collective-permute-done.refs_1_
  25.3 2.5 %keys_values.1 = (bf16[576,2048]{1,0:T(8,128)(2,1)S(1)}, bf16[288,512]{1,0:T(8,128)(2,1)S(1)}, bf16[288,512]{1,0:T(8,128)(2,1)S(1)}) custom-call(bf16[128,2048]{1,0:T(8,128)(2,1)S(1)} %copy-done.2, bf16[128,2048]{1,0:T(8,128)(2,1)S(1)} %collective-permute-done.refs_1_, bf16[128,2048]{1,0:T(8,128)(2,1)S(1)} %collective-permute-done.5.refs_2_, ...), custom_call_target="tpu_custom_call" | custom-call | flops 1207959552 | bytes 6815744 | tf_op jit(solution)/shard_map/keys_values/pallas_call | solution.py:146
  27.9 1.6 %collective-permute-start.23 = (bf16[512,2048]{1,0:T(8,128)(2,1)S(1)}, bf16[512,2048]{1,0:T(8,128)(2,1)S(1)}, u32[]{:S(2)}, u32[]{:S(2)}) collective-permute-start(bf16[512,2048]{1,0:T(8,128)(2,1)S(1)} %copy-done.1), channel_id=1, source_target_pairs={{0,2},{1,3},{2,0},{3,1},{4,6},{5,7},{6,4},{7,5},{8,10},{9,11},{10,... | collective-permute-start | bytes 6291464 | tf_op jit(solution)/shard_map/ppermute | solution.py:35
  29.5 1.6 %collective-permute-start.7 = (bf16[288,512]{1,0:T(8,128)(2,1)S(1)}, bf16[288,512]{1,0:T(8,128)(2,1)S(1)}, u32[]{:S(2)}, u32[]{:S(2)}) collective-permute-start(bf16[288,512]{1,0:T(8,128)(2,1)S(1)} %get-tuple-element.60.refs_1_), channel_id=1, source_target_pairs={{0,8},{8,16},{16,24},{24,28},{28,20},{20,12},{12,4},{4,0},{1,9},{9... | collective-permute-start | bytes 884744 | tf_op jit(solution)/shard_map/ppermute | solution.py:465
  31.0 0.4 collective-permute-start.8
  31.5 1.6 %collective-permute-start.11 = (bf16[288,512]{1,0:T(8,128)(2,1)S(1)}, bf16[288,512]{1,0:T(8,128)(2,1)S(1)}, u32[]{:S(2)}, u32[]{:S(2)}) collective-permute-start(bf16[288,512]{1,0:T(8,128)(2,1)S(1)} %get-tuple-element.61.refs_2_), channel_id=1, source_target_pairs={{0,8},{8,16},{16,24},{24,28},{28,20},{20,12},{12,4},{4,0},{1,9},{9... | collective-permute-start | bytes 884744 | tf_op jit(solution)/shard_map/ppermute | solution.py:465
  33.1 0.4 collective-permute-start.12
  33.5 2.2 %queries.1.refs_0_ = bf16[8,512,128]{2,1,0:T(8,128)(2,1)S(1)} custom-call(bf16[576,2048]{1,0:T(8,128)(2,1)S(1)} %get-tuple-element.59.hidden, bf16[2048,512]{1,0:T(8,128)(2,1)S(1)} %copy-done, f32[1,2176]{1,0:T(1,128)S(1)} %concatenate.6.refs_6_.gains, f32[576,128]{1,0:T(8,128)S(1)} %get-tuple-element.56.refs_8_.cos, ...), custom_call_target="tpu_custom_call" | custom-call | flops 1073741824 | bytes 4194304 | tf_op jit(solution)/shard_map/queries/pallas_call | solution.py:173
  35.7 3.5 %attention.9.refs_4_ = f32[8,80,512]{2,1,0:T(8,128)S(1)} custom-call(bf16[8,512,128]{2,1,0:T(8,128)(2,1)S(1)} %queries.1.refs_0_, bf16[288,512]{1,0:T(8,128)(2,1)S(1)} %get-tuple-element.60.refs_1_, bf16[288,512]{1,0:T(8,128)(2,1)S(1)} %get-tuple-element.61.refs_2_, f32[8,8,128]{2,1,0:T(8,128)S(1)} %broadcast_in_dim.14.refs_3_), custom_call_target="tpu_custom_call" | custom-call | flops 2415919104 | bytes 2097152 | tf_op jit(solution)/shard_map/attention/pallas_call | solution.py:306
  39.2 0.1 collective-permute-done.7.refs_1_
  39.3 1.6 %collective-permute-done.8.refs_2_ = bf16[288,512]{1,0:T(8,128)(2,1)S(1)} collective-permute-done((bf16[288,512]{1,0:T(8,128)(2,1)S(1)}, bf16[288,512]{1,0:T(8,128)(2,1)S(1)}, u32[]{:S(2)}, u32[]{:S(2)}) %collective-permute-start.8) | collective-permute-done | bytes 294944 | tf_op jit(solution)/shard_map/ppermute | solution.py:465
  40.9 0.4 collective-permute-start.10
  41.4 1.6 %collective-permute-start.9 = (bf16[288,512]{1,0:T(8,128)(2,1)S(1)}, bf16[288,512]{1,0:T(8,128)(2,1)S(1)}, u32[]{:S(2)}, u32[]{:S(2)}) collective-permute-start(bf16[288,512]{1,0:T(8,128)(2,1)S(1)} %collective-permute-done.7.refs_1_), channel_id=1, source_target_pairs={{0,8},{8,16},{16,24},{24,28},{28,20},{20,12},{12,4},{4,0},{1,9},{9... | collective-permute-start | bytes 884744 | tf_op jit(solution)/shard_map/ppermute | solution.py:465
  42.9 3.6 %attention.10.refs_4_ = f32[8,80,512]{2,1,0:T(8,128)S(1)} custom-call(bf16[8,512,128]{2,1,0:T(8,128)(2,1)S(1)} %queries.1.refs_0_, bf16[288,512]{1,0:T(8,128)(2,1)S(1)} %collective-permute-done.7.refs_1_, bf16[288,512]{1,0:T(8,128)(2,1)S(1)} %collective-permute-done.8.refs_2_, f32[8,8,128]{2,1,0:T(8,128)S(1)} %broadcast_in_dim.14.refs_3_, ...), custom_call_target="tpu_custom_call" | custom-call | flops 2415919104 | bytes 2097152 | tf_op jit(solution)/shard_map/attention/pallas_call | solution.py:306
  46.6 0.6 collective-permute-done.12.refs_2_
  47.2 1.6 %collective-permute-start.15 = (bf16[288,512]{1,0:T(8,128)(2,1)S(1)}, bf16[288,512]{1,0:T(8,128)(2,1)S(1)}, u32[]{:S(2)}, u32[]{:S(2)}) collective-permute-start(bf16[288,512]{1,0:T(8,128)(2,1)S(1)} %collective-permute-done.11.refs_1_), channel_id=1, source_target_pairs={{0,8},{8,16},{16,24},{24,28},{28,20},{20,12},{12,4},{4,0},{1,9},{9... | collective-permute-start | bytes 884744 | tf_op jit(solution)/shard_map/ppermute | solution.py:465
  48.8 0.4 collective-permute-start.16
  49.3 3.6 %attention.11.refs_4_ = f32[8,80,512]{2,1,0:T(8,128)S(1)} custom-call(bf16[8,512,128]{2,1,0:T(8,128)(2,1)S(1)} %queries.1.refs_0_, bf16[288,512]{1,0:T(8,128)(2,1)S(1)} %collective-permute-done.11.refs_1_, bf16[288,512]{1,0:T(8,128)(2,1)S(1)} %collective-permute-done.12.refs_2_, f32[8,8,128]{2,1,0:T(8,128)S(1)} %broadcast_in_dim.14.refs_3_, ...), custom_call_target="tpu_custom_call" | custom-call | flops 2415919104 | bytes 2097152 | tf_op jit(solution)/shard_map/attention/pallas_call | solution.py:306
  52.9 0.7 collective-permute-done.10.refs_2_
  53.6 1.6 %collective-permute-start.13 = (bf16[288,512]{1,0:T(8,128)(2,1)S(1)}, bf16[288,512]{1,0:T(8,128)(2,1)S(1)}, u32[]{:S(2)}, u32[]{:S(2)}) collective-permute-start(bf16[288,512]{1,0:T(8,128)(2,1)S(1)} %collective-permute-done.9.refs_1_), channel_id=1, source_target_pairs={{0,8},{8,16},{16,24},{24,28},{28,20},{20,12},{12,4},{4,0},{1,9},{9... | collective-permute-start | bytes 884744 | tf_op jit(solution)/shard_map/ppermute | solution.py:465
  55.1 0.4 collective-permute-start.14
  55.6 3.6 %attention.12.refs_4_ = f32[8,80,512]{2,1,0:T(8,128)S(1)} custom-call(bf16[8,512,128]{2,1,0:T(8,128)(2,1)S(1)} %queries.1.refs_0_, bf16[288,512]{1,0:T(8,128)(2,1)S(1)} %collective-permute-done.9.refs_1_, bf16[288,512]{1,0:T(8,128)(2,1)S(1)} %collective-permute-done.10.refs_2_, f32[8,8,128]{2,1,0:T(8,128)S(1)} %broadcast_in_dim.14.refs_3_, ...), custom_call_target="tpu_custom_call" | custom-call | flops 2415919104 | bytes 2097152 | tf_op jit(solution)/shard_map/attention/pallas_call | solution.py:306
  59.2 0.6 collective-permute-done.16.refs_2_
  59.9 1.6 %collective-permute-start.19 = (bf16[288,512]{1,0:T(8,128)(2,1)S(1)}, bf16[288,512]{1,0:T(8,128)(2,1)S(1)}, u32[]{:S(2)}, u32[]{:S(2)}) collective-permute-start(bf16[288,512]{1,0:T(8,128)(2,1)S(1)} %collective-permute-done.15.refs_1_), channel_id=1, source_target_pairs={{0,8},{8,16},{16,24},{24,28},{28,20},{20,12},{12,4},{4,0},{1,9},{9... | collective-permute-start | bytes 884744 | tf_op jit(solution)/shard_map/ppermute | solution.py:465
  61.5 0.4 collective-permute-start.20
  61.9 3.6 %attention.13.refs_4_ = f32[8,80,512]{2,1,0:T(8,128)S(1)} custom-call(bf16[8,512,128]{2,1,0:T(8,128)(2,1)S(1)} %queries.1.refs_0_, bf16[288,512]{1,0:T(8,128)(2,1)S(1)} %collective-permute-done.15.refs_1_, bf16[288,512]{1,0:T(8,128)(2,1)S(1)} %collective-permute-done.16.refs_2_, f32[8,8,128]{2,1,0:T(8,128)S(1)} %broadcast_in_dim.14.refs_3_, ...), custom_call_target="tpu_custom_call" | custom-call | flops 2415919104 | bytes 2097152 | tf_op jit(solution)/shard_map/attention/pallas_call | solution.py:306
  65.6 0.6 collective-permute-done.14.refs_2_
  66.2 1.6 %collective-permute-start.17 = (bf16[288,512]{1,0:T(8,128)(2,1)S(1)}, bf16[288,512]{1,0:T(8,128)(2,1)S(1)}, u32[]{:S(2)}, u32[]{:S(2)}) collective-permute-start(bf16[288,512]{1,0:T(8,128)(2,1)S(1)} %collective-permute-done.13.refs_1_), channel_id=1, source_target_pairs={{0,8},{8,16},{16,24},{24,28},{28,20},{20,12},{12,4},{4,0},{1,9},{9... | collective-permute-start | bytes 884744 | tf_op jit(solution)/shard_map/ppermute | solution.py:465
  67.8 0.4 collective-permute-start.18
  68.2 3.6 %attention.14.refs_4_ = f32[8,80,512]{2,1,0:T(8,128)S(1)} custom-call(bf16[8,512,128]{2,1,0:T(8,128)(2,1)S(1)} %queries.1.refs_0_, bf16[288,512]{1,0:T(8,128)(2,1)S(1)} %collective-permute-done.13.refs_1_, bf16[288,512]{1,0:T(8,128)(2,1)S(1)} %collective-permute-done.14.refs_2_, f32[8,8,128]{2,1,0:T(8,128)S(1)} %broadcast_in_dim.14.refs_3_, ...), custom_call_target="tpu_custom_call" | custom-call | flops 2415919104 | bytes 2097152 | tf_op jit(solution)/shard_map/attention/pallas_call | solution.py:306
  71.9 0.1 collective-permute-start.26
  72.0 0.6 collective-permute-done.20.refs_2_
  72.5 3.6 %attention.15.refs_4_ = f32[8,80,512]{2,1,0:T(8,128)S(1)} custom-call(bf16[8,512,128]{2,1,0:T(8,128)(2,1)S(1)} %queries.1.refs_0_, bf16[288,512]{1,0:T(8,128)(2,1)S(1)} %collective-permute-done.19.refs_1_, bf16[288,512]{1,0:T(8,128)(2,1)S(1)} %collective-permute-done.20.refs_2_, f32[8,8,128]{2,1,0:T(8,128)S(1)} %broadcast_in_dim.14.refs_3_, ...), custom_call_target="tpu_custom_call" | custom-call | flops 2415919104 | bytes 2097152 | tf_op jit(solution)/shard_map/attention/pallas_call | solution.py:306
  76.2 0.2 collective-permute-done.17.refs_1_
  76.4 1.3 %collective-permute-done.18.refs_2_ = bf16[288,512]{1,0:T(8,128)(2,1)S(1)} collective-permute-done((bf16[288,512]{1,0:T(8,128)(2,1)S(1)}, bf16[288,512]{1,0:T(8,128)(2,1)S(1)}, u32[]{:S(2)}, u32[]{:S(2)}) %collective-permute-start.18) | collective-permute-done | bytes 294944 | tf_op jit(solution)/shard_map/ppermute | solution.py:465
  77.7 2.0 %attention.16 = (bf16[128,512]{1,0:T(8,128)(2,1)S(1)}, bf16[128,512]{1,0:T(8,128)(2,1)S(1)}) custom-call(bf16[8,512,128]{2,1,0:T(8,128)(2,1)S(1)} %queries.1.refs_0_, bf16[288,512]{1,0:T(8,128)(2,1)S(1)} %collective-permute-done.17.refs_1_, bf16[288,512]{1,0:T(8,128)(2,1)S(1)} %collective-permute-done.18.refs_2_, f32[8,8,128]{2,1,0:T(8,128)S(1)} %broadcast_in_dim.14.refs_3_, ...), custom_call_target="tpu_custom_call" | custom-call | flops 2415919104 | bytes 2097152 | tf_op jit(solution)/shard_map/attention/pallas_call | solution.py:306
  79.7 0.1 collective-permute-start.24
  79.8 2.0 %attention.17 = (bf16[128,512]{1,0:T(8,128)(2,1)S(1)}, bf16[128,512]{1,0:T(8,128)(2,1)S(1)}) custom-call(bf16[8,512,128]{2,1,0:T(8,128)(2,1)S(1)} %queries.1.refs_0_, bf16[288,512]{1,0:T(8,128)(2,1)S(1)} %collective-permute-done.17.refs_1_, bf16[288,512]{1,0:T(8,128)(2,1)S(1)} %collective-permute-done.18.refs_2_, f32[8,8,128]{2,1,0:T(8,128)S(1)} %broadcast_in_dim.14.refs_3_, ...), custom_call_target="tpu_custom_call" | custom-call | flops 2415919104 | bytes 2097152 | tf_op jit(solution)/shard_map/attention/pallas_call | solution.py:306
  81.8 0.6 collective-permute-start.25
  82.4 0.5 collective-permute-start.21
  82.9 0.9 %collective-permute-start.22 = (bf16[128,512]{1,0:T(8,128)(2,1)S(1)}, bf16[128,512]{1,0:T(8,128)(2,1)S(1)}, u32[]{:S(2)}, u32[]{:S(2)}) collective-permute-start(bf16[128,512]{1,0:T(8,128)(2,1)S(1)} %get-tuple-element.85), channel_id=1, source_target_pairs={{0,3},{1,2},{2,1},{3,0},{4,7},{5,6},{6,5},{7,4},{8,11},{9,10},{10,... | collective-permute-start | bytes 393224 | tf_op jit(solution)/shard_map/ppermute | solution.py:35
  83.8 0.3 collective-permute-done.25.refs_1_
  84.1 0.7 output.2.refs_4_
  84.9 3.9 %collective-permute-done.21.refs_0_ = bf16[128,512]{1,0:T(8,128)(2,1)S(1)} collective-permute-done((bf16[128,512]{1,0:T(8,128)(2,1)S(1)}, bf16[128,512]{1,0:T(8,128)(2,1)S(1)}, u32[]{:S(2)}, u32[]{:S(2)}) %collective-permute-start.21) | collective-permute-done | bytes 131104 | tf_op jit(solution)/shard_map/ppermute | solution.py:35
  88.8 1.0 %collective-permute-done.22.refs_1_ = bf16[128,512]{1,0:T(8,128)(2,1)S(1)} collective-permute-done((bf16[128,512]{1,0:T(8,128)(2,1)S(1)}, bf16[128,512]{1,0:T(8,128)(2,1)S(1)}, u32[]{:S(2)}, u32[]{:S(2)}) %collective-permute-start.22) | collective-permute-done | bytes 131104 | tf_op jit(solution)/shard_map/ppermute | solution.py:35
  89.8 1.5 %output.3 = bf16[128,2048]{1,0:T(8,128)(2,1)} custom-call(bf16[128,512]{1,0:T(8,128)(2,1)S(1)} %collective-permute-done.21.refs_0_, bf16[128,512]{1,0:T(8,128)(2,1)S(1)} %collective-permute-done.22.refs_1_, bf16[512,2048]{1,0:T(8,128)(2,1)S(1)} %collective-permute-done.23.refs_2_, bf16[512,2048]{1,0:T(8,128)(2,1)S(1)} %collective-permute-done.24.refs_3_, ...), custom_call_target="tpu_custom_call" | custom-call | flops 536870912 | bytes 4194304 | tf_op jit(solution)/shard_map/output/pallas_call | solution.py:358
  (30 shorter events, 0.1 us)
Async XLA Ops:
  0.0 14.9 %copy-start.4 = (bf16[2048,256]{1,0:T(8,128)(2,1)S(1)}, bf16[2048,256]{1,0:T(8,128)(2,1)}, u32[]{:S(2)}) copy-start(bf16[2048,256]{1,0:T(8,128)(2,1)} %param.25) | copy-start | bytes 3145732
  2.1 9.0 %collective-permute-start.1 = (f32[8,512]{1,0:T(8,128)}, f32[8,512]{1,0:T(8,128)S(1)}, u32[]{:S(2)}, u32[]{:S(2)}) collective-permute-start(f32[8,512]{1,0:T(8,128)} %modulation.1), channel_id=1, source_target_pairs={{0,4},{4,0},{8,12},{12,8},{16,20},{20,16},{24,28},{28,24},{1,5},{5... | collective-permute-start | bytes 49160 | tf_op jit(solution)/shard_map/ppermute | solution.py:35
  5.0 6.0 %collective-permute-start.2 = (f32[8,512]{1,0:T(8,128)}, f32[8,512]{1,0:T(8,128)S(1)}, u32[]{:S(2)}, u32[]{:S(2)}) collective-permute-start(f32[8,512]{1,0:T(8,128)} %modulation.1), channel_id=1, source_target_pairs={{0,8},{4,12},{8,0},{12,4},{16,24},{20,28},{24,16},{28,20},{1,9},{5... | collective-permute-start | bytes 49160 | tf_op jit(solution)/shard_map/ppermute | solution.py:35
  6.6 4.8 %collective-permute-start.3 = (f32[8,512]{1,0:T(8,128)}, f32[8,512]{1,0:T(8,128)S(1)}, u32[]{:S(2)}, u32[]{:S(2)}) collective-permute-start(f32[8,512]{1,0:T(8,128)} %modulation.1), channel_id=1, source_target_pairs={{0,12},{4,8},{8,4},{12,0},{16,28},{20,24},{24,20},{28,16},{1,13},{... | collective-permute-start | bytes 49160 | tf_op jit(solution)/shard_map/ppermute | solution.py:35
  6.6 13.3 %collective-permute-start.5 = (bf16[128,2048]{1,0:T(8,128)(2,1)}, bf16[128,2048]{1,0:T(8,128)(2,1)S(1)}, u32[]{:S(2)}, u32[]{:S(2)}) collective-permute-start(bf16[128,2048]{1,0:T(8,128)(2,1)} %refs_5_.1), channel_id=1, source_target_pairs={{0,2},{1,3},{2,0},{3,1},{4,6},{5,7},{6,4},{7,5},{8,10},{9,11},{10,... | collective-permute-start | bytes 1572872 | tf_op jit(solution)/shard_map/ppermute | solution.py:35
  8.5 16.7 %collective-permute-start = (bf16[128,2048]{1,0:T(8,128)(2,1)}, bf16[128,2048]{1,0:T(8,128)(2,1)S(1)}, u32[]{:S(2)}, u32[]{:S(2)}) collective-permute-start(bf16[128,2048]{1,0:T(8,128)(2,1)} %refs_5_.1), channel_id=1, source_target_pairs={{0,1},{1,0},{2,3},{3,2},{4,5},{5,4},{6,7},{7,6},{8,9},{9,8},{10,11... | collective-permute-start | bytes 1572872 | tf_op jit(solution)/shard_map/ppermute | solution.py:35
  12.2 4.7 %copy-start.5 = (f32[8]{0:T(128)S(1)}, f32[8]{0:T(128)}, u32[]{:S(2)}) copy-start(f32[8]{0:T(128)} %param.28) | copy-start | bytes 100
  12.2 13.1 %copy-start.2 = (bf16[128,2048]{1,0:T(8,128)(2,1)S(1)}, bf16[128,2048]{1,0:T(8,128)(2,1)}, u32[]{:S(2)}) copy-start(bf16[128,2048]{1,0:T(8,128)(2,1)} %refs_5_.1) | copy-start | bytes 1572868
  12.2 13.1 %copy-start.3 = (bf16[64,2048]{1,0:T(8,128)(2,1)S(1)}, bf16[64,2048]{1,0:T(8,128)(2,1)}, u32[]{:S(2)}) copy-start(bf16[64,2048]{1,0:T(8,128)(2,1)} %refs_4_.1) | copy-start | bytes 786436
  12.2 4.7 %collective-permute-start.4 = (f32[8,512]{1,0:T(8,128)S(1)}, f32[8,512]{1,0:T(8,128)S(1)}, u32[]{:S(2)}, u32[]{:S(2)}) collective-permute-start(f32[8,512]{1,0:T(8,128)S(1)} %add_add_fusion), channel_id=1, source_target_pairs={{0,16},{4,20},{8,24},{12,28},{16,0},{20,4},{24,8},{28,12},{1,17},{... | collective-permute-start | bytes 49160 | tf_op jit(solution)/shard_map/ppermute | solution.py:35
  19.9 5.4 %collective-permute-start.6 = (bf16[128,2048]{1,0:T(8,128)(2,1)S(1)}, bf16[128,2048]{1,0:T(8,128)(2,1)S(1)}, u32[]{:S(2)}, u32[]{:S(2)}) collective-permute-start(bf16[128,2048]{1,0:T(8,128)(2,1)S(1)} %collective-permute-done.5.refs_2_), channel_id=1, source_target_pairs={{0,1},{1,0},{2,3},{3,2},{4,5},{5,4},{6,7},{7,6},{8,9},{9,8},{10,11... | collective-permute-start | bytes 1572872 | tf_op jit(solution)/shard_map/ppermute | solution.py:35
  25.3 2.6 %copy-start.1 = (bf16[512,2048]{1,0:T(8,128)(2,1)S(1)}, bf16[512,2048]{1,0:T(8,128)(2,1)}, u32[]{:S(2)}) copy-start(bf16[512,2048]{1,0:T(8,128)(2,1)} %refs_2_) | copy-start | bytes 6291460
  25.3 8.3 %copy-start = (bf16[2048,512]{1,0:T(8,128)(2,1)S(1)}, bf16[2048,512]{1,0:T(8,128)(2,1)}, u32[]{:S(2)}) copy-start(bf16[2048,512]{1,0:T(8,128)(2,1)} %weight.1) | copy-start | bytes 6291460
  27.9 51.9 %collective-permute-start.23 = (bf16[512,2048]{1,0:T(8,128)(2,1)S(1)}, bf16[512,2048]{1,0:T(8,128)(2,1)S(1)}, u32[]{:S(2)}, u32[]{:S(2)}) collective-permute-start(bf16[512,2048]{1,0:T(8,128)(2,1)S(1)} %copy-done.1), channel_id=1, source_target_pairs={{0,2},{1,3},{2,0},{3,1},{4,6},{5,7},{6,4},{7,5},{8,10},{9,11},{10,... | collective-permute-start | bytes 6291464 | tf_op jit(solution)/shard_map/ppermute | solution.py:35
  29.5 9.9 %collective-permute-start.7 = (bf16[288,512]{1,0:T(8,128)(2,1)S(1)}, bf16[288,512]{1,0:T(8,128)(2,1)S(1)}, u32[]{:S(2)}, u32[]{:S(2)}) collective-permute-start(bf16[288,512]{1,0:T(8,128)(2,1)S(1)} %get-tuple-element.60.refs_1_), channel_id=1, source_target_pairs={{0,8},{8,16},{16,24},{24,28},{28,20},{20,12},{12,4},{4,0},{1,9},{9... | collective-permute-start | bytes 884744 | tf_op jit(solution)/shard_map/ppermute | solution.py:465
  31.0 9.9 %collective-permute-start.8 = (bf16[288,512]{1,0:T(8,128)(2,1)S(1)}, bf16[288,512]{1,0:T(8,128)(2,1)S(1)}, u32[]{:S(2)}, u32[]{:S(2)}) collective-permute-start(bf16[288,512]{1,0:T(8,128)(2,1)S(1)} %get-tuple-element.61.refs_2_), channel_id=1, source_target_pairs={{8,0},{16,8},{24,16},{28,24},{20,28},{12,20},{4,12},{0,4},{9,1},{1... | collective-permute-start | bytes 884744 | tf_op jit(solution)/shard_map/ppermute | solution.py:465
  31.5 15.1 %collective-permute-start.11 = (bf16[288,512]{1,0:T(8,128)(2,1)S(1)}, bf16[288,512]{1,0:T(8,128)(2,1)S(1)}, u32[]{:S(2)}, u32[]{:S(2)}) collective-permute-start(bf16[288,512]{1,0:T(8,128)(2,1)S(1)} %get-tuple-element.61.refs_2_), channel_id=1, source_target_pairs={{0,8},{8,16},{16,24},{24,28},{28,20},{20,12},{12,4},{4,0},{1,9},{9... | collective-permute-start | bytes 884744 | tf_op jit(solution)/shard_map/ppermute | solution.py:465
  33.1 14.2 %collective-permute-start.12 = (bf16[288,512]{1,0:T(8,128)(2,1)S(1)}, bf16[288,512]{1,0:T(8,128)(2,1)S(1)}, u32[]{:S(2)}, u32[]{:S(2)}) collective-permute-start(bf16[288,512]{1,0:T(8,128)(2,1)S(1)} %get-tuple-element.60.refs_1_), channel_id=1, source_target_pairs={{8,0},{16,8},{24,16},{28,24},{20,28},{12,20},{4,12},{0,4},{9,1},{1... | collective-permute-start | bytes 884744 | tf_op jit(solution)/shard_map/ppermute | solution.py:465
  40.9 12.6 %collective-permute-start.10 = (bf16[288,512]{1,0:T(8,128)(2,1)S(1)}, bf16[288,512]{1,0:T(8,128)(2,1)S(1)}, u32[]{:S(2)}, u32[]{:S(2)}) collective-permute-start(bf16[288,512]{1,0:T(8,128)(2,1)S(1)} %collective-permute-done.8.refs_2_), channel_id=1, source_target_pairs={{8,0},{16,8},{24,16},{28,24},{20,28},{12,20},{4,12},{0,4},{9,1},{1... | collective-permute-start | bytes 884744 | tf_op jit(solution)/shard_map/ppermute | solution.py:465
  41.4 12.2 %collective-permute-start.9 = (bf16[288,512]{1,0:T(8,128)(2,1)S(1)}, bf16[288,512]{1,0:T(8,128)(2,1)S(1)}, u32[]{:S(2)}, u32[]{:S(2)}) collective-permute-start(bf16[288,512]{1,0:T(8,128)(2,1)S(1)} %collective-permute-done.7.refs_1_), channel_id=1, source_target_pairs={{0,8},{8,16},{16,24},{24,28},{28,20},{20,12},{12,4},{4,0},{1,9},{9... | collective-permute-start | bytes 884744 | tf_op jit(solution)/shard_map/ppermute | solution.py:465
  47.2 12.0 %collective-permute-start.15 = (bf16[288,512]{1,0:T(8,128)(2,1)S(1)}, bf16[288,512]{1,0:T(8,128)(2,1)S(1)}, u32[]{:S(2)}, u32[]{:S(2)}) collective-permute-start(bf16[288,512]{1,0:T(8,128)(2,1)S(1)} %collective-permute-done.11.refs_1_), channel_id=1, source_target_pairs={{0,8},{8,16},{16,24},{24,28},{28,20},{20,12},{12,4},{4,0},{1,9},{9... | collective-permute-start | bytes 884744 | tf_op jit(solution)/shard_map/ppermute | solution.py:465
  48.8 11.1 %collective-permute-start.16 = (bf16[288,512]{1,0:T(8,128)(2,1)S(1)}, bf16[288,512]{1,0:T(8,128)(2,1)S(1)}, u32[]{:S(2)}, u32[]{:S(2)}) collective-permute-start(bf16[288,512]{1,0:T(8,128)(2,1)S(1)} %collective-permute-done.12.refs_2_), channel_id=1, source_target_pairs={{8,0},{16,8},{24,16},{28,24},{20,28},{12,20},{4,12},{0,4},{9,1},{1... | collective-permute-start | bytes 884744 | tf_op jit(solution)/shard_map/ppermute | solution.py:465
  53.6 12.0 %collective-permute-start.13 = (bf16[288,512]{1,0:T(8,128)(2,1)S(1)}, bf16[288,512]{1,0:T(8,128)(2,1)S(1)}, u32[]{:S(2)}, u32[]{:S(2)}) collective-permute-start(bf16[288,512]{1,0:T(8,128)(2,1)S(1)} %collective-permute-done.9.refs_1_), channel_id=1, source_target_pairs={{0,8},{8,16},{16,24},{24,28},{28,20},{20,12},{12,4},{4,0},{1,9},{9... | collective-permute-start | bytes 884744 | tf_op jit(solution)/shard_map/ppermute | solution.py:465
  55.1 11.1 %collective-permute-start.14 = (bf16[288,512]{1,0:T(8,128)(2,1)S(1)}, bf16[288,512]{1,0:T(8,128)(2,1)S(1)}, u32[]{:S(2)}, u32[]{:S(2)}) collective-permute-start(bf16[288,512]{1,0:T(8,128)(2,1)S(1)} %collective-permute-done.10.refs_2_), channel_id=1, source_target_pairs={{8,0},{16,8},{24,16},{28,24},{20,28},{12,20},{4,12},{0,4},{9,1},{1... | collective-permute-start | bytes 884744 | tf_op jit(solution)/shard_map/ppermute | solution.py:465
  59.9 12.0 %collective-permute-start.19 = (bf16[288,512]{1,0:T(8,128)(2,1)S(1)}, bf16[288,512]{1,0:T(8,128)(2,1)S(1)}, u32[]{:S(2)}, u32[]{:S(2)}) collective-permute-start(bf16[288,512]{1,0:T(8,128)(2,1)S(1)} %collective-permute-done.15.refs_1_), channel_id=1, source_target_pairs={{0,8},{8,16},{16,24},{24,28},{28,20},{20,12},{12,4},{4,0},{1,9},{9... | collective-permute-start | bytes 884744 | tf_op jit(solution)/shard_map/ppermute | solution.py:465
  61.5 11.1 %collective-permute-start.20 = (bf16[288,512]{1,0:T(8,128)(2,1)S(1)}, bf16[288,512]{1,0:T(8,128)(2,1)S(1)}, u32[]{:S(2)}, u32[]{:S(2)}) collective-permute-start(bf16[288,512]{1,0:T(8,128)(2,1)S(1)} %collective-permute-done.16.refs_2_), channel_id=1, source_target_pairs={{8,0},{16,8},{24,16},{28,24},{20,28},{12,20},{4,12},{0,4},{9,1},{1... | collective-permute-start | bytes 884744 | tf_op jit(solution)/shard_map/ppermute | solution.py:465
  66.2 10.2 %collective-permute-start.17 = (bf16[288,512]{1,0:T(8,128)(2,1)S(1)}, bf16[288,512]{1,0:T(8,128)(2,1)S(1)}, u32[]{:S(2)}, u32[]{:S(2)}) collective-permute-start(bf16[288,512]{1,0:T(8,128)(2,1)S(1)} %collective-permute-done.13.refs_1_), channel_id=1, source_target_pairs={{0,8},{8,16},{16,24},{24,28},{28,20},{20,12},{12,4},{4,0},{1,9},{9... | collective-permute-start | bytes 884744 | tf_op jit(solution)/shard_map/ppermute | solution.py:465
  67.8 9.9 %collective-permute-start.18 = (bf16[288,512]{1,0:T(8,128)(2,1)S(1)}, bf16[288,512]{1,0:T(8,128)(2,1)S(1)}, u32[]{:S(2)}, u32[]{:S(2)}) collective-permute-start(bf16[288,512]{1,0:T(8,128)(2,1)S(1)} %collective-permute-done.14.refs_2_), channel_id=1, source_target_pairs={{8,0},{16,8},{24,16},{28,24},{20,28},{12,20},{4,12},{0,4},{9,1},{1... | collective-permute-start | bytes 884744 | tf_op jit(solution)/shard_map/ppermute | solution.py:465
  71.9 11.9 %collective-permute-start.26 = (bf16[512,2048]{1,0:T(8,128)(2,1)S(1)}, bf16[512,2048]{1,0:T(8,128)(2,1)S(1)}, u32[]{:S(2)}, u32[]{:S(2)}) collective-permute-start(bf16[512,2048]{1,0:T(8,128)(2,1)S(1)} %copy-done.1), channel_id=1, source_target_pairs={{0,1},{1,0},{2,3},{3,2},{4,5},{5,4},{6,7},{7,6},{8,9},{9,8},{10,11... | collective-permute-start | bytes 6291464 | tf_op jit(solution)/shard_map/ppermute | solution.py:35
  79.7 10.1 %collective-permute-start.24 = (bf16[512,2048]{1,0:T(8,128)(2,1)S(1)}, bf16[512,2048]{1,0:T(8,128)(2,1)S(1)}, u32[]{:S(2)}, u32[]{:S(2)}) collective-permute-start(bf16[512,2048]{1,0:T(8,128)(2,1)S(1)} %collective-permute-done.23.refs_2_), channel_id=1, source_target_pairs={{0,1},{1,0},{2,3},{3,2},{4,5},{5,4},{6,7},{7,6},{8,9},{9,8},{10,11... | collective-permute-start | bytes 6291464 | tf_op jit(solution)/shard_map/ppermute | solution.py:35
  81.8 2.3 %collective-permute-start.25 = (bf16[128,512]{1,0:T(8,128)(2,1)S(1)}, bf16[128,512]{1,0:T(8,128)(2,1)S(1)}, u32[]{:S(2)}, u32[]{:S(2)}) collective-permute-start(bf16[128,512]{1,0:T(8,128)(2,1)S(1)} %get-tuple-element.90), channel_id=1, source_target_pairs={{0,1},{1,0},{2,3},{3,2},{4,5},{5,4},{6,7},{7,6},{8,9},{9,8},{10,11... | collective-permute-start | bytes 393224 | tf_op jit(solution)/shard_map/ppermute | solution.py:35
  82.4 6.4 %collective-permute-start.21 = (bf16[128,512]{1,0:T(8,128)(2,1)S(1)}, bf16[128,512]{1,0:T(8,128)(2,1)S(1)}, u32[]{:S(2)}, u32[]{:S(2)}) collective-permute-start(bf16[128,512]{1,0:T(8,128)(2,1)S(1)} %get-tuple-element.84), channel_id=1, source_target_pairs={{0,2},{1,3},{2,0},{3,1},{4,6},{5,7},{6,4},{7,5},{8,10},{9,11},{10,... | collective-permute-start | bytes 393224 | tf_op jit(solution)/shard_map/ppermute | solution.py:35
  82.9 6.9 %collective-permute-start.22 = (bf16[128,512]{1,0:T(8,128)(2,1)S(1)}, bf16[128,512]{1,0:T(8,128)(2,1)S(1)}, u32[]{:S(2)}, u32[]{:S(2)}) collective-permute-start(bf16[128,512]{1,0:T(8,128)(2,1)S(1)} %get-tuple-element.85), channel_id=1, source_target_pairs={{0,3},{1,2},{2,1},{3,0},{4,7},{5,6},{6,5},{7,4},{8,11},{9,10},{10,... | collective-permute-start | bytes 393224 | tf_op jit(solution)/shard_map/ppermute | solution.py:35

commit v3 on v2

--- a/solution.py
+++ b/solution.py
@@ -97,33 +97,49 @@
     return [h for part in out for h in pieces_of(part, HEAD)]
 
 
-def modulate(x, gain, shift, dest, row):
-    rows = x.shape[0]
-    x = x.astype(F32)
-    inverse = lax.rsqrt(jnp.mean(x * x, axis=1, keepdims=True) + EPSILON)
-    dest[row : row + rows, :] = (x * inverse * gain + shift).astype(BF16)
-
-
-def kv_kernel(count, *refs):
-    pieces = refs[:count]
-    context, mod, gains, weight, cos, sin_e, sin_o = refs[count : count + 7]
-    hidden, first, second = refs[count + 7 :]
-    extra = context.shape[0] // 2
+def normal_kernel(*refs):
+    out = refs[-1]
+    row = 0
+    for ref in refs[:-1]:
+        x = ref[...].astype(F32)
+        inverse = lax.rsqrt(jnp.mean(x * x, axis=1, keepdims=True) + EPSILON)
+        out[row : row + x.shape[0], :] = x * inverse
+        row += x.shape[0]
+
+
+def normal_rows(arrays):
+    rows = sum(x.shape[0] for x in arrays)
+    depth = arrays[0].shape[1]
+    return pl.pallas_call(
+        normal_kernel,
+        in_specs=[IN_VMEM] * len(arrays),
+        out_specs=IN_VMEM,
+        out_shape=jax.ShapeDtypeStruct((rows, depth), F32),
+        compiler_params=pltpu.CompilerParams(vmem_limit_bytes=VMEM_LIMIT),
+        cost_estimate=cost(8 * rows * depth, 6 * rows * depth),
+        name="normal",
+    )(*arrays)
+
+
+def kv_kernel(count, context_rows, *refs):
+    tails = refs[:count]
+    normal, gains, weight, cos, sin_e, sin_o = refs[count : count + 6]
+    hidden, first, second, mod = refs[count + 6 :]
+    extra = context_rows // 2
     half = first.shape[0] - extra
-    norm_gain = gains[:, : context.shape[1]]
-    key_gain = gains[:, context.shape[1] : context.shape[1] + HEAD]
-    parts = mod.shape[0] // 8
+    norm_gain = gains[:, : normal.shape[1]]
+    key_gain = gains[:, normal.shape[1] : normal.shape[1] + HEAD]
+    rank = lax.axis_index("tp")
+    for j, tail in enumerate(tails):
+        mod[jnp.bitwise_xor(rank, j)] = tail[...]
 
     def vector(index):
-        return jnp.concatenate([mod[8 * t + index : 8 * t + index + 1, :] for t in range(parts)], axis=1)
-
-    gain = norm_gain * (1.0 + vector(1))
-    shift = vector(0)
-    row = 0
-    for piece in pieces:
-        modulate(piece[...], gain, shift, hidden, row)
-        row += piece.shape[0]
-    modulate(context[...], norm_gain * (1.0 + vector(4)), vector(3), hidden, row)
+        return jnp.concatenate([mod[t, index : index + 1, :] for t in range(count)], axis=1)
+
+    length = 2 * half
+    gain, context_gain = [norm_gain * (1.0 + vector(i)) for i in (1, 4)]
+    hidden[:length, :] = (normal[:length, :] * gain + vector(0)).astype(BF16)
+    hidden[length:, :] = (normal[length:, :] * context_gain + vector(3)).astype(BF16)
     h = hidden[...]
     width = weight.shape[1] // 2
     keys = dot(h, weight[:, :width])
@@ -139,23 +155,23 @@
         second[half:, lanes] = tile[2 * half + extra :]
 
 
-def keys_values(pieces, context, mod, gains, weight, tables):
-    rows = sum(p.shape[0] for p in pieces) + context.shape[0]
-    depth = context.shape[1]
+def keys_values(normal, context_rows, tails, gains, weight, tables):
+    rows, depth = normal.shape
     width = weight.shape[1] // 2
     return pl.pallas_call(
-        functools.partial(kv_kernel, len(pieces)),
+        functools.partial(kv_kernel, len(tails), context_rows),
         out_shape=(
             jax.ShapeDtypeStruct((rows, depth), BF16),
             jax.ShapeDtypeStruct((rows // 2, 2 * width), BF16),
             jax.ShapeDtypeStruct((rows // 2, 2 * width), BF16),
+            jax.ShapeDtypeStruct((len(tails),) + tails[0].shape, F32),
         ),
-        in_specs=[IN_VMEM] * (len(pieces) + 7),
-        out_specs=(IN_VMEM, IN_VMEM, IN_VMEM),
+        in_specs=[IN_VMEM] * (len(tails) + 6),
+        out_specs=(IN_VMEM,) * 4,
         compiler_params=pltpu.CompilerParams(vmem_limit_bytes=VMEM_LIMIT),
         cost_estimate=cost(4 * rows * depth * width, 4 * rows * depth + 4 * depth * width),
         name="keys_values",
-    )(*pieces, context, mod, gains, weight, *tables)
+    )(*tails, normal, gains, weight, *tables)
 
 
 def query_kernel(hidden, weight, gains, cos, sin_e, sin_o, out):
@@ -336,7 +352,7 @@
             total = term if total is None else total + term
         if rest:
             begun, latent, mod = rest
-            gate = [mod[8 * t + 2 : 8 * t + 3, :] for t in range(mod.shape[0] // 8)]
+            gate = [mod[t, 2:3, :] for t in range(mod.shape[0])]
             gate = jnp.concatenate(gate, axis=1)[:, i : i + step]
             total = latent[:, i : i + step].astype(F32) + gate * (begun[:, i : i + step] + total)
             made, sems = refs[-2:]
@@ -385,6 +401,11 @@
     sine = jnp.sin(angle)
     even = lane % 2 == 0
     return jnp.cos(angle), jnp.where(even, -sine, 0.0), jnp.where(even, 0.0, sine)
+
+
+def far_calls(tp, rows):
+    each = min(tp // 2, max(1, TILE // rows))
+    return each, tp // 2 // each
 
 
 def shards(
@@ -450,10 +471,14 @@
     partial, pieces[tp_bits[0]] = tie(partial, pieces[tp_bits[0]])
     for bit in tp_bits[1:]:
         spread(pieces, bit)
-    mod = lax.all_gather(partial, "tp", axis=0, tiled=True)
-
-    hidden, first, second = keys_values(
-        [pieces[j] for j in range(tp)], context, mod, gains, kv_weight, tables
+    tails = {0: partial}
+    for j in reversed(range(1, tp)):
+        tails[j] = swap(partial, "tp", tp, j)
+
+    normal = normal_rows([pieces[j] for j in range(tp)] + [context])
+    tails = [tails[j] for j in range(tp)]
+    hidden, first, second, mod = keys_values(
+        normal, context_rows, tails, gains, kv_weight, tables
     )
 
     half = length // 2
@@ -481,12 +506,18 @@
         if i < sp - 3:
             flight.append(hop((up, down)))
         waiting = as_blocks((up, down))
-    far = attention(queries, waiting, lifts, state, group, tp // 2, (half, length))
+    far = []
+    each, calls = far_calls(tp, rows)
+    for c in reversed(range(calls)):
+        window = (half + c * each * rows, half + (c + 1) * each * rows)
+        made = attention(queries, waiting, lifts, state, group, each, window)
+        *made, state = tie(*made, state)
+        made = [swap(a, "tp", tp, tp // 2 + c * each + j) for j, a in enumerate(made)]
+        far = made + far
     top_bit = tp_bits[0]
-    weights[top_bit], state, *_ = tie(weights[top_bit], state, *far)
+    weights[top_bit], state = tie(weights[top_bit], state)
     for bit in tp_bits[1:]:
         spread(weights, bit)
-    far = [swap(a, "tp", tp, tp // 2 + j) for j, a in enumerate(far)]
     near = attention(queries, waiting, lifts, state, group, tp // 2, (0, half))
     near = near[:1] + [swap(a, "tp", tp, j) for j, a in enumerate(near) if j]
     weights = [weights[j] for j in range(tp)]

time: 92 us -> 91.6 us (level)
  blocking collectives: 5.34 us -> 0 us
  waiting for transfers between devices: 15.6 us -> 18.6 us
  starting transfers between devices: 27.1 us -> 28.1 us
    all_gather x1 -> x0, blocking collectives: 5.34 us -> none  [shards(): mod = lax.all_gather(partial, 'tp', axis=0, tiled=True)]
    ppermute x13 -> x16, waiting for transfers between devices: 9.2 us -> 13.2 us  [swap(): return lax.ppermute(value, axis, [(i, i ^ mask) for i in range(size)])]
    ppermute x7, waiting for transfers between devices: 6.02 us -> 2.71 us  [hop(): lax.ppermute(pair[1], 'sp', back)]
    ppermute x7, waiting for transfers between devices: 0.36 us -> 2.65 us  [hop(): lax.ppermute(pair[0], 'sp', ahead)]
    ppermute x7, starting transfers between devices: 3.14 us -> 4.26 us  [hop(): lax.ppermute(pair[1], 'sp', back)]
    ppermute x13 -> x16, starting transfers between devices: 12.9 us -> 13.7 us  [swap(): return lax.ppermute(value, axis, [(i, i ^ mask) for i in range(size)])]
    pallas_call x9 -> x10, Pallas kernels: 29.4 us -> 29.9 us  [attention(): pl.pallas_call(functools.partial(attention_kernel, spans, lifted, state i...]
    pallas_call x1 -> x2, Pallas kernels: 2.55 us -> 2.78 us  [the longest x1 2 us: keys_values(): pl.pallas_call(functools.partial(kv_kernel, len(tails), context_rows), ou...]
  transfers between devices with their start and end apart: 27 -> 30, of which waited for: 15 -> 12; matrix products, arithmetic and copies ran while one was open for 5% -> 5% of each run, Pallas kernels for 35% -> 37%
where the time goes in v3:
time: 91.6 us; the launch traced here: 91.1 us
  Pallas kernels  39.2 us (43%)
  starting transfers between devices  28.1 us (31%)
  waiting for transfers between devices  18.6 us (20%)
  other arithmetic  3.75 us (4%)
    pallas_call x10, Pallas kernels, attention(): pl.pallas_call(functools.partial(attention_kernel, spans, lifted, state i...  29.9 us
    ppermute x16, starting transfers between devices, swap(): return lax.ppermute(value, axis, [(i, i ^ mask) for i in range(size)])  13.7 us
    ppermute x16, waiting for transfers between devices, swap(): return lax.ppermute(value, axis, [(i, i ^ mask) for i in range(size)])  13.2 us
    ppermute x7, starting transfers between devices, hop(): lax.ppermute(pair[0], 'sp', ahead)  10.1 us
    ppermute x7, starting transfers between devices, hop(): lax.ppermute(pair[1], 'sp', back)  4.26 us
    ppermute x7, waiting for transfers between devices, hop(): lax.ppermute(pair[1], 'sp', back)  2.71 us
    ppermute x7, waiting for transfers between devices, hop(): lax.ppermute(pair[0], 'sp', ahead)  2.65 us
    pallas_call x2, Pallas kernels, project(): pl.pallas_call(functools.partial(output_kernel, count), in_specs=[IN_VMEM...  2.26 us
  transfers between devices with their start and end apart: 30, of which 12 were waited for; matrix products, arithmetic and copies ran while one was open for 5% of the time, Pallas kernels for 37%

profile of v3, /device:TPU:0, one launch (start us, length us, event | category | flops | bytes accessed | tf_op | source)
XLA Modules:
  0.0 91.1 jit_solution(6312864462120858208)
XLA Ops:
  0.0 2.1 %modulation.1 = f32[8,512]{1,0:T(8,128)} custom-call(f32[1,256]{1,0:T(1,128)} %bitcast.6, f32[1,256]{1,0:T(1,128)} %bitcast.7, bf16[256,512]{1,0:T(8,128)(2,1)} %shift.1, bf16[256,512]{1,0:T(8,128)(2,1)} %scale.1, bf16[256,512]{1,0:T(8,128)(2,1)} %gate.1), custom_call_target="tpu_custom_call" | custom-call | flops 6291456 | bytes 786432 | tf_op jit(solution)/shard_map/modulation/pallas_call | solution.py:59
  2.1 4.0 %collective-permute-start.2 = (f32[8,512]{1,0:T(8,128)}, f32[8,512]{1,0:T(8,128)S(1)}, u32[]{:S(2)}, u32[]{:S(2)}) collective-permute-start(f32[8,512]{1,0:T(8,128)} %modulation.1), channel_id=1, source_target_pairs={{0,12},{4,8},{8,4},{12,0},{16,28},{20,24},{24,20},{28,16},{1,13},{... | collective-permute-start | bytes 49160 | tf_op jit(solution)/shard_map/ppermute | solution.py:35
  6.0 0.4 collective-permute-start.1
  6.5 0.1 collective-permute-start
  6.6 0.0 collective-permute-start.8
  6.6 1.9 %collective-permute-start.4 = (bf16[128,2048]{1,0:T(8,128)(2,1)}, bf16[128,2048]{1,0:T(8,128)(2,1)S(1)}, u32[]{:S(2)}, u32[]{:S(2)}) collective-permute-start(bf16[128,2048]{1,0:T(8,128)(2,1)} %refs_5_.1), channel_id=1, source_target_pairs={{0,2},{1,3},{2,0},{3,1},{4,6},{5,7},{6,4},{7,5},{8,10},{9,11},{10,... | collective-permute-start | bytes 1572872 | tf_op jit(solution)/shard_map/ppermute | solution.py:35
  8.6 1.6 %fusion.13 = (f32[576,128]{1,0:T(8,128)S(1)}, f32[576,128]{1,0:T(8,128)S(1)}, f32[576,128]{1,0:T(8,128)S(1)}) fusion(s32[128]{0:T(128)S(1)} %get-tuple-element.108, s32[128]{0:T(128)S(1)} %get-tuple-element.110, pred[128]{0:T(512)(128)(4,1)S(1)} %get-tuple-element.106, s32[576]{0:T(1024)S(1)} %get-tuple-element.101, s32[576]{0:T(1024)S(1)} %get-tuple-element.102, ...), kind=kLoop, calls=%fused_computation.31 | loop fusion | flops 4792320 | bytes 897992 | tf_op jit(solution)/shard_map/jit(_where)/select_n | solution.py:403
  10.2 0.8 concatenate.6.refs_5_.gains
  11.1 0.7 add_add_fusion
  11.8 0.0 copy-start.3
  11.8 2.7 %collective-permute-start.3 = (f32[8,512]{1,0:T(8,128)S(1)}, f32[8,512]{1,0:T(8,128)S(1)}, u32[]{:S(2)}, u32[]{:S(2)}) collective-permute-start(f32[8,512]{1,0:T(8,128)S(1)} %add_add_fusion), channel_id=1, source_target_pairs={{0,16},{4,20},{8,24},{12,28},{16,0},{20,4},{24,8},{28,12},{1,17},{... | collective-permute-start | bytes 49160 | tf_op jit(solution)/shard_map/ppermute | solution.py:35
  14.5 1.4 %pad_maximum_fusion.refs_6_ = bf16[2048,512]{1,0:T(8,128)(2,1)S(1)} fusion(bf16[2048,256]{1,0:T(8,128)(2,1)S(1)} %copy-done.4, bf16[2048,256]{1,0:T(8,128)(2,1)} %param.24), kind=kLoop, calls=%fused_computation | loop fusion | flops 4194304 | bytes 4194304 | tf_op jit(solution)/shard_map/concatenate | solution.py:452
  15.9 0.7 collective-permute-done.3
  16.5 0.1 broadcast_in_dim.14.refs_3_
  16.6 4.7 %collective-permute-done.4.refs_2_ = bf16[128,2048]{1,0:T(8,128)(2,1)S(1)} collective-permute-done((bf16[128,2048]{1,0:T(8,128)(2,1)}, bf16[128,2048]{1,0:T(8,128)(2,1)S(1)}, u32[]{:S(2)}, u32[]{:S(2)}) %collective-permute-start.4) | collective-permute-done | bytes 524320 | tf_op jit(solution)/shard_map/ppermute | solution.py:35
  21.4 1.9 %collective-permute-start.7 = (f32[8,512]{1,0:T(8,128)S(1)}, f32[8,512]{1,0:T(8,128)S(1)}, u32[]{:S(2)}, u32[]{:S(2)}) collective-permute-start(f32[8,512]{1,0:T(8,128)S(1)} %add.75.refs_0_), channel_id=1, source_target_pairs={{0,3},{1,2},{2,1},{3,0},{4,7},{5,6},{6,5},{7,4},{8,11},{9,10},{10,... | collective-permute-start | bytes 49160 | tf_op jit(solution)/shard_map/ppermute | solution.py:35
  23.2 0.3 collective-permute-start.6
  23.5 0.8 normal.1.refs_4_
  24.3 0.0 copy-start.2
  24.3 0.0 copy-start.1
  24.3 0.3 collective-permute-done.7.refs_3_
  24.7 2.3 %collective-permute-done.6.refs_2_ = f32[8,512]{1,0:T(8,128)S(1)} collective-permute-done((f32[8,512]{1,0:T(8,128)S(1)}, f32[8,512]{1,0:T(8,128)S(1)}, u32[]{:S(2)}, u32[]{:S(2)}) %collective-permute-start.6) | collective-permute-done | bytes 16416 | tf_op jit(solution)/shard_map/ppermute | solution.py:35
  26.9 2.0 %keys_values.1 = (bf16[576,2048]{1,0:T(8,128)(2,1)S(1)}, bf16[288,512]{1,0:T(8,128)(2,1)S(1)}, bf16[288,512]{1,0:T(8,128)(2,1)S(1)}, f32[4,8,512]{2,1,0:T(8,128)S(1)}) custom-call(f32[8,512]{1,0:T(8,128)S(1)} %add.75.refs_0_, f32[8,512]{1,0:T(8,128)S(1)} %collective-permute-done.5.refs_1_, f32[8,512]{1,0:T(8,128)S(1)} %collective-permute-done.6.refs_2_, ...), custom_call_target="tpu_custom_call" | custom-call | flops 1207959552 | bytes 6815744 | tf_op jit(solution)/shard_map/keys_values/pallas_call | solution.py:161
  29.0 1.6 %collective-permute-start.14 = (bf16[288,512]{1,0:T(8,128)(2,1)S(1)}, bf16[288,512]{1,0:T(8,128)(2,1)S(1)}, u32[]{:S(2)}, u32[]{:S(2)}) collective-permute-start(bf16[288,512]{1,0:T(8,128)(2,1)S(1)} %get-tuple-element.64.refs_2_), channel_id=1, source_target_pairs={{0,8},{8,16},{16,24},{24,28},{28,20},{20,12},{12,4},{4,0},{1,9},{9... | collective-permute-start | bytes 884744 | tf_op jit(solution)/shard_map/ppermute | solution.py:490
  30.6 0.4 collective-permute-start.11
  31.0 1.5 %collective-permute-start.15 = (bf16[288,512]{1,0:T(8,128)(2,1)S(1)}, bf16[288,512]{1,0:T(8,128)(2,1)S(1)}, u32[]{:S(2)}, u32[]{:S(2)}) collective-permute-start(bf16[288,512]{1,0:T(8,128)(2,1)S(1)} %get-tuple-element.63.refs_1_), channel_id=1, source_target_pairs={{8,0},{16,8},{24,16},{28,24},{20,28},{12,20},{4,12},{0,4},{9,1},{1... | collective-permute-start | bytes 884744 | tf_op jit(solution)/shard_map/ppermute | solution.py:490
  32.5 0.5 collective-permute-start.10
  33.1 0.3 collective-permute-start.26
  33.4 2.2 %queries.1.refs_0_ = bf16[8,512,128]{2,1,0:T(8,128)(2,1)S(1)} custom-call(bf16[576,2048]{1,0:T(8,128)(2,1)S(1)} %get-tuple-element.62.hidden, bf16[2048,512]{1,0:T(8,128)(2,1)S(1)} %copy-done.1, f32[1,2176]{1,0:T(1,128)S(1)} %concatenate.6.refs_5_.gains, f32[576,128]{1,0:T(8,128)S(1)} %get-tuple-element.59.refs_7_.cos, ...), custom_call_target="tpu_custom_call" | custom-call | flops 1073741824 | bytes 4194304 | tf_op jit(solution)/shard_map/queries/pallas_call | solution.py:189
  35.5 3.5 %attention.10.refs_4_ = f32[8,80,512]{2,1,0:T(8,128)S(1)} custom-call(bf16[8,512,128]{2,1,0:T(8,128)(2,1)S(1)} %queries.1.refs_0_, bf16[288,512]{1,0:T(8,128)(2,1)S(1)} %get-tuple-element.63.refs_1_, bf16[288,512]{1,0:T(8,128)(2,1)S(1)} %get-tuple-element.64.refs_2_, f32[8,8,128]{2,1,0:T(8,128)S(1)} %broadcast_in_dim.14.refs_3_), custom_call_target="tpu_custom_call" | custom-call | flops 2415919104 | bytes 2097152 | tf_op jit(solution)/shard_map/attention/pallas_call | solution.py:322
  39.0 1.4 %collective-permute-done.11.refs_2_ = bf16[288,512]{1,0:T(8,128)(2,1)S(1)} collective-permute-done((bf16[288,512]{1,0:T(8,128)(2,1)S(1)}, bf16[288,512]{1,0:T(8,128)(2,1)S(1)}, u32[]{:S(2)}, u32[]{:S(2)}) %collective-permute-start.11) | collective-permute-done | bytes 294944 | tf_op jit(solution)/shard_map/ppermute | solution.py:490
  40.5 2.6 %collective-permute-done.10.refs_1_ = bf16[288,512]{1,0:T(8,128)(2,1)S(1)} collective-permute-done((bf16[288,512]{1,0:T(8,128)(2,1)S(1)}, bf16[288,512]{1,0:T(8,128)(2,1)S(1)}, u32[]{:S(2)}, u32[]{:S(2)}) %collective-permute-start.10) | collective-permute-done | bytes 294944 | tf_op jit(solution)/shard_map/ppermute | solution.py:490
  43.1 1.6 %collective-permute-start.12 = (bf16[288,512]{1,0:T(8,128)(2,1)S(1)}, bf16[288,512]{1,0:T(8,128)(2,1)S(1)}, u32[]{:S(2)}, u32[]{:S(2)}) collective-permute-start(bf16[288,512]{1,0:T(8,128)(2,1)S(1)} %collective-permute-done.10.refs_1_), channel_id=1, source_target_pairs={{0,8},{8,16},{16,24},{24,28},{28,20},{20,12},{12,4},{4,0},{1,9},{9... | collective-permute-start | bytes 884744 | tf_op jit(solution)/shard_map/ppermute | solution.py:490
  44.7 0.5 collective-permute-start.13
  45.1 3.7 %attention.11.refs_4_ = f32[8,80,512]{2,1,0:T(8,128)S(1)} custom-call(bf16[8,512,128]{2,1,0:T(8,128)(2,1)S(1)} %queries.1.refs_0_, bf16[288,512]{1,0:T(8,128)(2,1)S(1)} %collective-permute-done.10.refs_1_, bf16[288,512]{1,0:T(8,128)(2,1)S(1)} %collective-permute-done.11.refs_2_, f32[8,8,128]{2,1,0:T(8,128)S(1)} %broadcast_in_dim.14.refs_3_, ...), custom_call_target="tpu_custom_call" | custom-call | flops 2415919104 | bytes 2097152 | tf_op jit(solution)/shard_map/attention/pallas_call | solution.py:322
  48.8 1.6 %collective-permute-start.18 = (bf16[288,512]{1,0:T(8,128)(2,1)S(1)}, bf16[288,512]{1,0:T(8,128)(2,1)S(1)}, u32[]{:S(2)}, u32[]{:S(2)}) collective-permute-start(bf16[288,512]{1,0:T(8,128)(2,1)S(1)} %collective-permute-done.14.refs_1_), channel_id=1, source_target_pairs={{0,8},{8,16},{16,24},{24,28},{28,20},{20,12},{12,4},{4,0},{1,9},{9... | collective-permute-start | bytes 884744 | tf_op jit(solution)/shard_map/ppermute | solution.py:490
  50.4 0.5 collective-permute-start.19
  50.9 3.6 %attention.12.refs_4_ = f32[8,80,512]{2,1,0:T(8,128)S(1)} custom-call(bf16[8,512,128]{2,1,0:T(8,128)(2,1)S(1)} %queries.1.refs_0_, bf16[288,512]{1,0:T(8,128)(2,1)S(1)} %collective-permute-done.14.refs_1_, bf16[288,512]{1,0:T(8,128)(2,1)S(1)} %collective-permute-done.15.refs_2_, f32[8,8,128]{2,1,0:T(8,128)S(1)} %broadcast_in_dim.14.refs_3_, ...), custom_call_target="tpu_custom_call" | custom-call | flops 2415919104 | bytes 2097152 | tf_op jit(solution)/shard_map/attention/pallas_call | solution.py:322
  54.5 1.6 %collective-permute-start.16 = (bf16[288,512]{1,0:T(8,128)(2,1)S(1)}, bf16[288,512]{1,0:T(8,128)(2,1)S(1)}, u32[]{:S(2)}, u32[]{:S(2)}) collective-permute-start(bf16[288,512]{1,0:T(8,128)(2,1)S(1)} %collective-permute-done.12.refs_1_), channel_id=1, source_target_pairs={{0,8},{8,16},{16,24},{24,28},{28,20},{20,12},{12,4},{4,0},{1,9},{9... | collective-permute-start | bytes 884744 | tf_op jit(solution)/shard_map/ppermute | solution.py:490
  56.2 0.5 collective-permute-start.17
  56.6 3.6 %attention.13.refs_4_ = f32[8,80,512]{2,1,0:T(8,128)S(1)} custom-call(bf16[8,512,128]{2,1,0:T(8,128)(2,1)S(1)} %queries.1.refs_0_, bf16[288,512]{1,0:T(8,128)(2,1)S(1)} %collective-permute-done.12.refs_1_, bf16[288,512]{1,0:T(8,128)(2,1)S(1)} %collective-permute-done.13.refs_2_, f32[8,8,128]{2,1,0:T(8,128)S(1)} %broadcast_in_dim.14.refs_3_, ...), custom_call_target="tpu_custom_call" | custom-call | flops 2415919104 | bytes 2097152 | tf_op jit(solution)/shard_map/attention/pallas_call | solution.py:322
  60.3 1.6 %collective-permute-start.22 = (bf16[288,512]{1,0:T(8,128)(2,1)S(1)}, bf16[288,512]{1,0:T(8,128)(2,1)S(1)}, u32[]{:S(2)}, u32[]{:S(2)}) collective-permute-start(bf16[288,512]{1,0:T(8,128)(2,1)S(1)} %collective-permute-done.18.refs_1_), channel_id=1, source_target_pairs={{0,8},{8,16},{16,24},{24,28},{28,20},{20,12},{12,4},{4,0},{1,9},{9... | collective-permute-start | bytes 884744 | tf_op jit(solution)/shard_map/ppermute | solution.py:490
  61.9 0.5 collective-permute-start.23
  62.4 3.6 %attention.14.refs_4_ = f32[8,80,512]{2,1,0:T(8,128)S(1)} custom-call(bf16[8,512,128]{2,1,0:T(8,128)(2,1)S(1)} %queries.1.refs_0_, bf16[288,512]{1,0:T(8,128)(2,1)S(1)} %collective-permute-done.18.refs_1_, bf16[288,512]{1,0:T(8,128)(2,1)S(1)} %collective-permute-done.19.refs_2_, f32[8,8,128]{2,1,0:T(8,128)S(1)} %broadcast_in_dim.14.refs_3_, ...), custom_call_target="tpu_custom_call" | custom-call | flops 2415919104 | bytes 2097152 | tf_op jit(solution)/shard_map/attention/pallas_call | solution.py:322
  66.0 0.4 collective-permute-done.17.refs_2_
  66.4 1.6 %collective-permute-start.20 = (bf16[288,512]{1,0:T(8,128)(2,1)S(1)}, bf16[288,512]{1,0:T(8,128)(2,1)S(1)}, u32[]{:S(2)}, u32[]{:S(2)}) collective-permute-start(bf16[288,512]{1,0:T(8,128)(2,1)S(1)} %collective-permute-done.16.refs_1_), channel_id=1, source_target_pairs={{0,8},{8,16},{16,24},{24,28},{28,20},{20,12},{12,4},{4,0},{1,9},{9... | collective-permute-start | bytes 884744 | tf_op jit(solution)/shard_map/ppermute | solution.py:490
  68.0 0.4 collective-permute-start.21
  68.4 3.6 %attention.15.refs_4_ = f32[8,80,512]{2,1,0:T(8,128)S(1)} custom-call(bf16[8,512,128]{2,1,0:T(8,128)(2,1)S(1)} %queries.1.refs_0_, bf16[288,512]{1,0:T(8,128)(2,1)S(1)} %collective-permute-done.16.refs_1_, bf16[288,512]{1,0:T(8,128)(2,1)S(1)} %collective-permute-done.17.refs_2_, f32[8,8,128]{2,1,0:T(8,128)S(1)} %broadcast_in_dim.14.refs_3_, ...), custom_call_target="tpu_custom_call" | custom-call | flops 2415919104 | bytes 2097152 | tf_op jit(solution)/shard_map/attention/pallas_call | solution.py:322
  72.1 0.1 collective-permute-start.29
  72.2 0.6 collective-permute-done.23.refs_2_
  72.7 3.6 %attention.16.refs_4_ = f32[8,80,512]{2,1,0:T(8,128)S(1)} custom-call(bf16[8,512,128]{2,1,0:T(8,128)(2,1)S(1)} %queries.1.refs_0_, bf16[288,512]{1,0:T(8,128)(2,1)S(1)} %collective-permute-done.22.refs_1_, bf16[288,512]{1,0:T(8,128)(2,1)S(1)} %collective-permute-done.23.refs_2_, f32[8,8,128]{2,1,0:T(8,128)S(1)} %broadcast_in_dim.14.refs_3_, ...), custom_call_target="tpu_custom_call" | custom-call | flops 2415919104 | bytes 2097152 | tf_op jit(solution)/shard_map/attention/pallas_call | solution.py:322
  76.4 0.3 collective-permute-done.21.refs_2_
  76.7 1.3 %attention.17 = bf16[128,512]{1,0:T(8,128)(2,1)S(1)} custom-call(bf16[8,512,128]{2,1,0:T(8,128)(2,1)S(1)} %queries.1.refs_0_, bf16[288,512]{1,0:T(8,128)(2,1)S(1)} %collective-permute-done.20.refs_1_, bf16[288,512]{1,0:T(8,128)(2,1)S(1)} %collective-permute-done.21.refs_2_, f32[8,8,128]{2,1,0:T(8,128)S(1)} %broadcast_in_dim.14.refs_3_, ...), custom_call_target="tpu_custom_call" | custom-call | flops 2415919104 | bytes 2097152 | tf_op jit(solution)/shard_map/attention/pallas_call | solution.py:322
  78.0 1.3 %attention.18 = bf16[128,512]{1,0:T(8,128)(2,1)S(1)} custom-call(bf16[8,512,128]{2,1,0:T(8,128)(2,1)S(1)} %queries.1.refs_0_, bf16[288,512]{1,0:T(8,128)(2,1)S(1)} %collective-permute-done.20.refs_1_, bf16[288,512]{1,0:T(8,128)(2,1)S(1)} %collective-permute-done.21.refs_2_, f32[8,8,128]{2,1,0:T(8,128)S(1)} %broadcast_in_dim.14.refs_3_, ...), custom_call_target="tpu_custom_call" | custom-call | flops 2415919104 | bytes 2097152 | tf_op jit(solution)/shard_map/attention/pallas_call | solution.py:322
  79.3 0.1 collective-permute-start.27
  79.4 2.0 %attention.19 = (bf16[128,512]{1,0:T(8,128)(2,1)S(1)}, bf16[128,512]{1,0:T(8,128)(2,1)S(1)}) custom-call(bf16[8,512,128]{2,1,0:T(8,128)(2,1)S(1)} %queries.1.refs_0_, bf16[288,512]{1,0:T(8,128)(2,1)S(1)} %collective-permute-done.20.refs_1_, bf16[288,512]{1,0:T(8,128)(2,1)S(1)} %collective-permute-done.21.refs_2_, f32[8,8,128]{2,1,0:T(8,128)S(1)} %broadcast_in_dim.14.refs_3_, ...), custom_call_target="tpu_custom_call" | custom-call | flops 2415919104 | bytes 2097152 | tf_op jit(solution)/shard_map/attention/pallas_call | solution.py:322
  81.4 0.6 collective-permute-start.28
  82.0 1.3 %collective-permute-start.24 = (bf16[128,512]{1,0:T(8,128)(2,1)S(1)}, bf16[128,512]{1,0:T(8,128)(2,1)S(1)}, u32[]{:S(2)}, u32[]{:S(2)}) collective-permute-start(bf16[128,512]{1,0:T(8,128)(2,1)S(1)} %attention.18), channel_id=1, source_target_pairs={{0,2},{1,3},{2,0},{3,1},{4,6},{5,7},{6,4},{7,5},{8,10},{9,11},{10,... | collective-permute-start | bytes 393224 | tf_op jit(solution)/shard_map/ppermute | solution.py:35
  83.3 0.1 collective-permute-start.25
  83.4 0.3 collective-permute-done.28.refs_1_
  83.7 0.7 output.2.refs_4_
  84.5 3.9 %collective-permute-done.24.refs_0_ = bf16[128,512]{1,0:T(8,128)(2,1)S(1)} collective-permute-done((bf16[128,512]{1,0:T(8,128)(2,1)S(1)}, bf16[128,512]{1,0:T(8,128)(2,1)S(1)}, u32[]{:S(2)}, u32[]{:S(2)}) %collective-permute-start.24) | collective-permute-done | bytes 131104 | tf_op jit(solution)/shard_map/ppermute | solution.py:35
  88.4 1.0 %collective-permute-done.25.refs_1_ = bf16[128,512]{1,0:T(8,128)(2,1)S(1)} collective-permute-done((bf16[128,512]{1,0:T(8,128)(2,1)S(1)}, bf16[128,512]{1,0:T(8,128)(2,1)S(1)}, u32[]{:S(2)}, u32[]{:S(2)}) %collective-permute-start.25) | collective-permute-done | bytes 131104 | tf_op jit(solution)/shard_map/ppermute | solution.py:35
  89.4 1.5 %output.3 = bf16[128,2048]{1,0:T(8,128)(2,1)} custom-call(bf16[128,512]{1,0:T(8,128)(2,1)S(1)} %collective-permute-done.24.refs_0_, bf16[128,512]{1,0:T(8,128)(2,1)S(1)} %collective-permute-done.25.refs_1_, bf16[512,2048]{1,0:T(8,128)(2,1)S(1)} %collective-permute-done.26.refs_2_, bf16[512,2048]{1,0:T(8,128)(2,1)S(1)} %collective-permute-done.27.refs_3_, ...), custom_call_target="tpu_custom_call" | custom-call | flops 536870912 | bytes 4194304 | tf_op jit(solution)/shard_map/output/pallas_call | solution.py:374
  (37 shorter events, 0.1 us)
Async XLA Ops:
  0.0 14.5 %copy-start.4 = (bf16[2048,256]{1,0:T(8,128)(2,1)S(1)}, bf16[2048,256]{1,0:T(8,128)(2,1)}, u32[]{:S(2)}) copy-start(bf16[2048,256]{1,0:T(8,128)(2,1)} %param.25) | copy-start | bytes 3145732
  2.1 9.0 %collective-permute-start.2 = (f32[8,512]{1,0:T(8,128)}, f32[8,512]{1,0:T(8,128)S(1)}, u32[]{:S(2)}, u32[]{:S(2)}) collective-permute-start(f32[8,512]{1,0:T(8,128)} %modulation.1), channel_id=1, source_target_pairs={{0,12},{4,8},{8,4},{12,0},{16,28},{20,24},{24,20},{28,16},{1,13},{... | collective-permute-start | bytes 49160 | tf_op jit(solution)/shard_map/ppermute | solution.py:35
  6.0 5.0 %collective-permute-start.1 = (f32[8,512]{1,0:T(8,128)}, f32[8,512]{1,0:T(8,128)S(1)}, u32[]{:S(2)}, u32[]{:S(2)}) collective-permute-start(f32[8,512]{1,0:T(8,128)} %modulation.1), channel_id=1, source_target_pairs={{0,8},{4,12},{8,0},{12,4},{16,24},{20,28},{24,16},{28,20},{1,9},{5... | collective-permute-start | bytes 49160 | tf_op jit(solution)/shard_map/ppermute | solution.py:35
  6.5 4.6 %collective-permute-start = (f32[8,512]{1,0:T(8,128)}, f32[8,512]{1,0:T(8,128)S(1)}, u32[]{:S(2)}, u32[]{:S(2)}) collective-permute-start(f32[8,512]{1,0:T(8,128)} %modulation.1), channel_id=1, source_target_pairs={{0,4},{4,0},{8,12},{12,8},{16,20},{20,16},{24,28},{28,24},{1,5},{5... | collective-permute-start | bytes 49160 | tf_op jit(solution)/shard_map/ppermute | solution.py:35
  6.6 16.9 %collective-permute-start.8 = (bf16[128,2048]{1,0:T(8,128)(2,1)}, bf16[128,2048]{1,0:T(8,128)(2,1)S(1)}, u32[]{:S(2)}, u32[]{:S(2)}) collective-permute-start(bf16[128,2048]{1,0:T(8,128)(2,1)} %refs_5_.1), channel_id=1, source_target_pairs={{0,1},{1,0},{2,3},{3,2},{4,5},{5,4},{6,7},{7,6},{8,9},{9,8},{10,11... | collective-permute-start | bytes 1572872 | tf_op jit(solution)/shard_map/ppermute | solution.py:35
  6.6 14.7 %collective-permute-start.4 = (bf16[128,2048]{1,0:T(8,128)(2,1)}, bf16[128,2048]{1,0:T(8,128)(2,1)S(1)}, u32[]{:S(2)}, u32[]{:S(2)}) collective-permute-start(bf16[128,2048]{1,0:T(8,128)(2,1)} %refs_5_.1), channel_id=1, source_target_pairs={{0,2},{1,3},{2,0},{3,1},{4,6},{5,7},{6,4},{7,5},{8,10},{9,11},{10,... | collective-permute-start | bytes 1572872 | tf_op jit(solution)/shard_map/ppermute | solution.py:35
  11.8 4.7 %copy-start.5 = (f32[8]{0:T(128)S(1)}, f32[8]{0:T(128)}, u32[]{:S(2)}) copy-start(f32[8]{0:T(128)} %param.28) | copy-start | bytes 100
  11.8 11.7 %copy-start = (bf16[128,2048]{1,0:T(8,128)(2,1)S(1)}, bf16[128,2048]{1,0:T(8,128)(2,1)}, u32[]{:S(2)}) copy-start(bf16[128,2048]{1,0:T(8,128)(2,1)} %refs_5_.1) | copy-start | bytes 1572868
  11.8 11.7 %copy-start.3 = (bf16[64,2048]{1,0:T(8,128)(2,1)S(1)}, bf16[64,2048]{1,0:T(8,128)(2,1)}, u32[]{:S(2)}) copy-start(bf16[64,2048]{1,0:T(8,128)(2,1)} %refs_4_.1) | copy-start | bytes 786436
  11.8 4.7 %collective-permute-start.3 = (f32[8,512]{1,0:T(8,128)S(1)}, f32[8,512]{1,0:T(8,128)S(1)}, u32[]{:S(2)}, u32[]{:S(2)}) collective-permute-start(f32[8,512]{1,0:T(8,128)S(1)} %add_add_fusion), channel_id=1, source_target_pairs={{0,16},{4,20},{8,24},{12,28},{16,0},{20,4},{24,8},{28,12},{1,17},{... | collective-permute-start | bytes 49160 | tf_op jit(solution)/shard_map/ppermute | solution.py:35
  21.3 2.2 %collective-permute-start.9 = (bf16[128,2048]{1,0:T(8,128)(2,1)S(1)}, bf16[128,2048]{1,0:T(8,128)(2,1)S(1)}, u32[]{:S(2)}, u32[]{:S(2)}) collective-permute-start(bf16[128,2048]{1,0:T(8,128)(2,1)S(1)} %collective-permute-done.4.refs_2_), channel_id=1, source_target_pairs={{0,1},{1,0},{2,3},{3,2},{4,5},{5,4},{6,7},{7,6},{8,9},{9,8},{10,11... | collective-permute-start | bytes 1572872 | tf_op jit(solution)/shard_map/ppermute | solution.py:35
  21.4 3.3 %collective-permute-start.7 = (f32[8,512]{1,0:T(8,128)S(1)}, f32[8,512]{1,0:T(8,128)S(1)}, u32[]{:S(2)}, u32[]{:S(2)}) collective-permute-start(f32[8,512]{1,0:T(8,128)S(1)} %add.75.refs_0_), channel_id=1, source_target_pairs={{0,3},{1,2},{2,1},{3,0},{4,7},{5,6},{6,5},{7,4},{8,11},{9,10},{10,... | collective-permute-start | bytes 49160 | tf_op jit(solution)/shard_map/ppermute | solution.py:35
  23.2 3.7 %collective-permute-start.6 = (f32[8,512]{1,0:T(8,128)S(1)}, f32[8,512]{1,0:T(8,128)S(1)}, u32[]{:S(2)}, u32[]{:S(2)}) collective-permute-start(f32[8,512]{1,0:T(8,128)S(1)} %add.75.refs_0_), channel_id=1, source_target_pairs={{0,2},{1,3},{2,0},{3,1},{4,6},{5,7},{6,4},{7,5},{8,10},{9,11},{10,... | collective-permute-start | bytes 49160 | tf_op jit(solution)/shard_map/ppermute | solution.py:35
  23.5 3.5 %collective-permute-start.5 = (f32[8,512]{1,0:T(8,128)S(1)}, f32[8,512]{1,0:T(8,128)S(1)}, u32[]{:S(2)}, u32[]{:S(2)}) collective-permute-start(f32[8,512]{1,0:T(8,128)S(1)} %add.75.refs_0_), channel_id=1, source_target_pairs={{0,1},{1,0},{2,3},{3,2},{4,5},{5,4},{6,7},{7,6},{8,9},{9,8},{10,11... | collective-permute-start | bytes 49160 | tf_op jit(solution)/shard_map/ppermute | solution.py:35
  24.3 8.7 %copy-start.2 = (bf16[512,2048]{1,0:T(8,128)(2,1)S(1)}, bf16[512,2048]{1,0:T(8,128)(2,1)}, u32[]{:S(2)}) copy-start(bf16[512,2048]{1,0:T(8,128)(2,1)} %refs_2_) | copy-start | bytes 6291460
  24.3 9.0 %copy-start.1 = (bf16[2048,512]{1,0:T(8,128)(2,1)S(1)}, bf16[2048,512]{1,0:T(8,128)(2,1)}, u32[]{:S(2)}) copy-start(bf16[2048,512]{1,0:T(8,128)(2,1)} %weight.1) | copy-start | bytes 6291460
  29.0 19.8 %collective-permute-start.14 = (bf16[288,512]{1,0:T(8,128)(2,1)S(1)}, bf16[288,512]{1,0:T(8,128)(2,1)S(1)}, u32[]{:S(2)}, u32[]{:S(2)}) collective-permute-start(bf16[288,512]{1,0:T(8,128)(2,1)S(1)} %get-tuple-element.64.refs_2_), channel_id=1, source_target_pairs={{0,8},{8,16},{16,24},{24,28},{28,20},{20,12},{12,4},{4,0},{1,9},{9... | collective-permute-start | bytes 884744 | tf_op jit(solution)/shard_map/ppermute | solution.py:490
  30.6 9.9 %collective-permute-start.11 = (bf16[288,512]{1,0:T(8,128)(2,1)S(1)}, bf16[288,512]{1,0:T(8,128)(2,1)S(1)}, u32[]{:S(2)}, u32[]{:S(2)}) collective-permute-start(bf16[288,512]{1,0:T(8,128)(2,1)S(1)} %get-tuple-element.64.refs_2_), channel_id=1, source_target_pairs={{8,0},{16,8},{24,16},{28,24},{20,28},{12,20},{4,12},{0,4},{9,1},{1... | collective-permute-start | bytes 884744 | tf_op jit(solution)/shard_map/ppermute | solution.py:490
  31.0 17.8 %collective-permute-start.15 = (bf16[288,512]{1,0:T(8,128)(2,1)S(1)}, bf16[288,512]{1,0:T(8,128)(2,1)S(1)}, u32[]{:S(2)}, u32[]{:S(2)}) collective-permute-start(bf16[288,512]{1,0:T(8,128)(2,1)S(1)} %get-tuple-element.63.refs_1_), channel_id=1, source_target_pairs={{8,0},{16,8},{24,16},{28,24},{20,28},{12,20},{4,12},{0,4},{9,1},{1... | collective-permute-start | bytes 884744 | tf_op jit(solution)/shard_map/ppermute | solution.py:490
  32.5 10.6 %collective-permute-start.10 = (bf16[288,512]{1,0:T(8,128)(2,1)S(1)}, bf16[288,512]{1,0:T(8,128)(2,1)S(1)}, u32[]{:S(2)}, u32[]{:S(2)}) collective-permute-start(bf16[288,512]{1,0:T(8,128)(2,1)S(1)} %get-tuple-element.63.refs_1_), channel_id=1, source_target_pairs={{0,8},{8,16},{16,24},{24,28},{28,20},{20,12},{12,4},{4,0},{1,9},{9... | collective-permute-start | bytes 884744 | tf_op jit(solution)/shard_map/ppermute | solution.py:490
  33.1 46.2 %collective-permute-start.26 = (bf16[512,2048]{1,0:T(8,128)(2,1)S(1)}, bf16[512,2048]{1,0:T(8,128)(2,1)S(1)}, u32[]{:S(2)}, u32[]{:S(2)}) collective-permute-start(bf16[512,2048]{1,0:T(8,128)(2,1)S(1)} %copy-done.2), channel_id=1, source_target_pairs={{0,2},{1,3},{2,0},{3,1},{4,6},{5,7},{6,4},{7,5},{8,10},{9,11},{10,... | collective-permute-start | bytes 6291464 | tf_op jit(solution)/shard_map/ppermute | solution.py:35
  43.1 11.4 %collective-permute-start.12 = (bf16[288,512]{1,0:T(8,128)(2,1)S(1)}, bf16[288,512]{1,0:T(8,128)(2,1)S(1)}, u32[]{:S(2)}, u32[]{:S(2)}) collective-permute-start(bf16[288,512]{1,0:T(8,128)(2,1)S(1)} %collective-permute-done.10.refs_1_), channel_id=1, source_target_pairs={{0,8},{8,16},{16,24},{24,28},{28,20},{20,12},{12,4},{4,0},{1,9},{9... | collective-permute-start | bytes 884744 | tf_op jit(solution)/shard_map/ppermute | solution.py:490
  44.7 9.9 %collective-permute-start.13 = (bf16[288,512]{1,0:T(8,128)(2,1)S(1)}, bf16[288,512]{1,0:T(8,128)(2,1)S(1)}, u32[]{:S(2)}, u32[]{:S(2)}) collective-permute-start(bf16[288,512]{1,0:T(8,128)(2,1)S(1)} %collective-permute-done.11.refs_2_), channel_id=1, source_target_pairs={{8,0},{16,8},{24,16},{28,24},{20,28},{12,20},{4,12},{0,4},{9,1},{1... | collective-permute-start | bytes 884744 | tf_op jit(solution)/shard_map/ppermute | solution.py:490
  48.8 11.5 %collective-permute-start.18 = (bf16[288,512]{1,0:T(8,128)(2,1)S(1)}, bf16[288,512]{1,0:T(8,128)(2,1)S(1)}, u32[]{:S(2)}, u32[]{:S(2)}) collective-permute-start(bf16[288,512]{1,0:T(8,128)(2,1)S(1)} %collective-permute-done.14.refs_1_), channel_id=1, source_target_pairs={{0,8},{8,16},{16,24},{24,28},{28,20},{20,12},{12,4},{4,0},{1,9},{9... | collective-permute-start | bytes 884744 | tf_op jit(solution)/shard_map/ppermute | solution.py:490
  50.4 9.9 %collective-permute-start.19 = (bf16[288,512]{1,0:T(8,128)(2,1)S(1)}, bf16[288,512]{1,0:T(8,128)(2,1)S(1)}, u32[]{:S(2)}, u32[]{:S(2)}) collective-permute-start(bf16[288,512]{1,0:T(8,128)(2,1)S(1)} %collective-permute-done.15.refs_2_), channel_id=1, source_target_pairs={{8,0},{16,8},{24,16},{28,24},{20,28},{12,20},{4,12},{0,4},{9,1},{1... | collective-permute-start | bytes 884744 | tf_op jit(solution)/shard_map/ppermute | solution.py:490
  54.5 11.5 %collective-permute-start.16 = (bf16[288,512]{1,0:T(8,128)(2,1)S(1)}, bf16[288,512]{1,0:T(8,128)(2,1)S(1)}, u32[]{:S(2)}, u32[]{:S(2)}) collective-permute-start(bf16[288,512]{1,0:T(8,128)(2,1)S(1)} %collective-permute-done.12.refs_1_), channel_id=1, source_target_pairs={{0,8},{8,16},{16,24},{24,28},{28,20},{20,12},{12,4},{4,0},{1,9},{9... | collective-permute-start | bytes 884744 | tf_op jit(solution)/shard_map/ppermute | solution.py:490
  56.2 10.3 %collective-permute-start.17 = (bf16[288,512]{1,0:T(8,128)(2,1)S(1)}, bf16[288,512]{1,0:T(8,128)(2,1)S(1)}, u32[]{:S(2)}, u32[]{:S(2)}) collective-permute-start(bf16[288,512]{1,0:T(8,128)(2,1)S(1)} %collective-permute-done.13.refs_2_), channel_id=1, source_target_pairs={{8,0},{16,8},{24,16},{28,24},{20,28},{12,20},{4,12},{0,4},{9,1},{1... | collective-permute-start | bytes 884744 | tf_op jit(solution)/shard_map/ppermute | solution.py:490
  60.3 11.8 %collective-permute-start.22 = (bf16[288,512]{1,0:T(8,128)(2,1)S(1)}, bf16[288,512]{1,0:T(8,128)(2,1)S(1)}, u32[]{:S(2)}, u32[]{:S(2)}) collective-permute-start(bf16[288,512]{1,0:T(8,128)(2,1)S(1)} %collective-permute-done.18.refs_1_), channel_id=1, source_target_pairs={{0,8},{8,16},{16,24},{24,28},{28,20},{20,12},{12,4},{4,0},{1,9},{9... | collective-permute-start | bytes 884744 | tf_op jit(solution)/shard_map/ppermute | solution.py:490
  61.9 10.8 %collective-permute-start.23 = (bf16[288,512]{1,0:T(8,128)(2,1)S(1)}, bf16[288,512]{1,0:T(8,128)(2,1)S(1)}, u32[]{:S(2)}, u32[]{:S(2)}) collective-permute-start(bf16[288,512]{1,0:T(8,128)(2,1)S(1)} %collective-permute-done.19.refs_2_), channel_id=1, source_target_pairs={{8,0},{16,8},{24,16},{28,24},{20,28},{12,20},{4,12},{0,4},{9,1},{1... | collective-permute-start | bytes 884744 | tf_op jit(solution)/shard_map/ppermute | solution.py:490
  66.4 10.0 %collective-permute-start.20 = (bf16[288,512]{1,0:T(8,128)(2,1)S(1)}, bf16[288,512]{1,0:T(8,128)(2,1)S(1)}, u32[]{:S(2)}, u32[]{:S(2)}) collective-permute-start(bf16[288,512]{1,0:T(8,128)(2,1)S(1)} %collective-permute-done.16.refs_1_), channel_id=1, source_target_pairs={{0,8},{8,16},{16,24},{24,28},{28,20},{20,12},{12,4},{4,0},{1,9},{9... | collective-permute-start | bytes 884744 | tf_op jit(solution)/shard_map/ppermute | solution.py:490
  68.0 8.7 %collective-permute-start.21 = (bf16[288,512]{1,0:T(8,128)(2,1)S(1)}, bf16[288,512]{1,0:T(8,128)(2,1)S(1)}, u32[]{:S(2)}, u32[]{:S(2)}) collective-permute-start(bf16[288,512]{1,0:T(8,128)(2,1)S(1)} %collective-permute-done.17.refs_2_), channel_id=1, source_target_pairs={{8,0},{16,8},{24,16},{28,24},{20,28},{12,20},{4,12},{0,4},{9,1},{1... | collective-permute-start | bytes 884744 | tf_op jit(solution)/shard_map/ppermute | solution.py:490
  72.1 11.3 %collective-permute-start.29 = (bf16[512,2048]{1,0:T(8,128)(2,1)S(1)}, bf16[512,2048]{1,0:T(8,128)(2,1)S(1)}, u32[]{:S(2)}, u32[]{:S(2)}) collective-permute-start(bf16[512,2048]{1,0:T(8,128)(2,1)S(1)} %copy-done.2), channel_id=1, source_target_pairs={{0,1},{1,0},{2,3},{3,2},{4,5},{5,4},{6,7},{7,6},{8,9},{9,8},{10,11... | collective-permute-start | bytes 6291464 | tf_op jit(solution)/shard_map/ppermute | solution.py:35
  79.3 10.1 %collective-permute-start.27 = (bf16[512,2048]{1,0:T(8,128)(2,1)S(1)}, bf16[512,2048]{1,0:T(8,128)(2,1)S(1)}, u32[]{:S(2)}, u32[]{:S(2)}) collective-permute-start(bf16[512,2048]{1,0:T(8,128)(2,1)S(1)} %collective-permute-done.26.refs_2_), channel_id=1, source_target_pairs={{0,1},{1,0},{2,3},{3,2},{4,5},{5,4},{6,7},{7,6},{8,9},{9,8},{10,11... | collective-permute-start | bytes 6291464 | tf_op jit(solution)/shard_map/ppermute | solution.py:35
  81.4 2.3 %collective-permute-start.28 = (bf16[128,512]{1,0:T(8,128)(2,1)S(1)}, bf16[128,512]{1,0:T(8,128)(2,1)S(1)}, u32[]{:S(2)}, u32[]{:S(2)}) collective-permute-start(bf16[128,512]{1,0:T(8,128)(2,1)S(1)} %get-tuple-element.95), channel_id=1, source_target_pairs={{0,1},{1,0},{2,3},{3,2},{4,5},{5,4},{6,7},{7,6},{8,9},{9,8},{10,11... | collective-permute-start | bytes 393224 | tf_op jit(solution)/shard_map/ppermute | solution.py:35
  82.0 6.4 %collective-permute-start.24 = (bf16[128,512]{1,0:T(8,128)(2,1)S(1)}, bf16[128,512]{1,0:T(8,128)(2,1)S(1)}, u32[]{:S(2)}, u32[]{:S(2)}) collective-permute-start(bf16[128,512]{1,0:T(8,128)(2,1)S(1)} %attention.18), channel_id=1, source_target_pairs={{0,2},{1,3},{2,0},{3,1},{4,6},{5,7},{6,4},{7,5},{8,10},{9,11},{10,... | collective-permute-start | bytes 393224 | tf_op jit(solution)/shard_map/ppermute | solution.py:35
  83.3 6.1 %collective-permute-start.25 = (bf16[128,512]{1,0:T(8,128)(2,1)S(1)}, bf16[128,512]{1,0:T(8,128)(2,1)S(1)}, u32[]{:S(2)}, u32[]{:S(2)}) collective-permute-start(bf16[128,512]{1,0:T(8,128)(2,1)S(1)} %attention.17), channel_id=1, source_target_pairs={{0,3},{1,2},{2,1},{3,0},{4,7},{5,6},{6,5},{7,4},{8,11},{9,10},{10,... | collective-permute-start | bytes 393224 | tf_op jit(solution)/shard_map/ppermute | solution.py:35
